TPU v7x, 32 devices: a whole 2x2x4 slice. The times are simulated.
32 devices in a mesh: dp: 4 (over y, x), kv: 4 (over z), tp: 2 (over core).
Axes of the slice: x: 2, y: 2, z: 4, core: 2. Of those that a mesh axis runs over, the one named last changes fastest.
Arguments:
- tokens: bfloat16 [256, 2048], P('dp', ('kv', 'tp')), parts along dimension 0, may hold values from -64 to 64, as said below
- lengths: int32 [32], P(('dp', 'kv', 'tp')), parts along dimension 0, may hold values from 1 to 8, 28 in all
- state: float32 [32, 16, 128, 128], P(('dp', 'kv', 'tp')), parts along dimension 0, may hold values from -1.8 to 1.8
- gain_first: float32 [2048], replicated, may hold values from 0.1 to 1.9
- first_gate: bfloat16 [2048, 5632], P(None, 'kv'), may hold values from -0.125 to 0.125
- first_up: bfloat16 [2048, 5632], P(None, 'kv'), may hold values from -0.125 to 0.125
- first_down: bfloat16 [5632, 2048], P('kv'), may hold values from -0.109375 to 0.109375
- gain_mix: float32 [2048], replicated, may hold values from 0.1 to 1.9
- query_weight: bfloat16 [2048, 2048], P(None, ('kv', 'tp')), may hold values from -0.125 to 0.125
- key_weight: bfloat16 [2048, 2048], P(None, ('kv', 'tp')), may hold values from -0.125 to 0.125
- value_weight: bfloat16 [2048, 2048], P(None, ('kv', 'tp')), may hold values from -0.125 to 0.125
- gating_weight: bfloat16 [2048, 2048], P(None, ('kv', 'tp')), may hold values from -0.125 to 0.125
- write_weight: bfloat16 [2048, 16], replicated, may hold values from -0.125 to 0.125
- forget_weight: bfloat16 [2048, 16], replicated, may hold values from -0.125 to 0.125
- forget_rate: float32 [16], replicated, may hold values from -4 to 1.5
- out_weight: bfloat16 [2048, 2048], P(None, ('kv', 'tp')), may hold values from -0.125 to 0.125
- gain_second: float32 [2048], replicated, may hold values from 0.1 to 1.9
- second_gate: bfloat16 [2048, 5632], P(None, 'kv'), may hold values from -0.125 to 0.125
- second_up: bfloat16 [2048, 5632], P(None, 'kv'), may hold values from -0.125 to 0.125
- second_down: bfloat16 [5632, 2048], P('kv'), may hold values from -0.109375 to 0.109375
Outputs:
- mixed_out: bfloat16 [256, 2048], P('dp', ('kv', 'tp')), parts along dimension 0
- new_state: float32 [32, 16, 128, 128], P(('dp', 'kv', 'tp')), parts along dimension 0
There are 4 independent parts, one for each index of `dp`. A program takes and returns all parts, laid end to end along the dimension named above; an argument that names none is the same for every part. Nothing has to cross between parts.
Inputs may be any that keep to these rules, and one draw needn't show every extreme that they name: Activations of the new tokens. `lengths`: the live new tokens of each sequence; within each independent group of 8 sequences (one part along dp) they sum to seven halves of 8, rounded down, and some sequence of each group has all 8 live.
All inputs are finite; a program needn't handle non-finite values.
Results may differ from a plain program's by a relative error of at most 0.0058.
Values may be sent and summed in bfloat16 or wider, within the bound.
No kernel may reach another device: no remote copies, remote signals or barrier semaphores. Data moves between devices by JAX's collectives and lax.ppermute only.
A program may use at most 128 MiB of HBM per device.

v0:
```python
import math

import jax
import jax.numpy as jnp
from jax import lax
from jax.sharding import PartitionSpec as P

HEADS = 16
HEAD = 128
BLK = 8


EPSILON = 1e-06


def fold_step(gain, gate_cols, up_cols, portion):
    values = portion.astype(jnp.float32)
    scaled = (values * gain).astype(jnp.bfloat16)
    gate_acc = jnp.dot(scaled, gate_cols, preferred_element_type=jnp.float32)
    up_acc = jnp.dot(scaled, up_cols, preferred_element_type=jnp.float32)
    squares = jnp.sum(values * values, axis=1)
    return (gate_acc, up_acc, squares)


def finish_units(gate_acc, up_acc, squares, channels, down_rows):
    row_scale = lax.rsqrt(squares / channels + EPSILON)[:, None]
    hidden = (jax.nn.silu(gate_acc * row_scale) * (up_acc * row_scale)).astype(jnp.bfloat16)
    return jnp.dot(hidden, down_rows, preferred_element_type=jnp.float32)


def feed_forward(hidden_in, gain, w_gate, w_up, w_down):
    channels = gain.shape[0]
    paired = lax.all_to_all(hidden_in, "tp", split_axis=0, concat_axis=1, tiled=True)
    gate_acc, up_acc, squares = fold_step(
        gain, w_gate, w_up, lax.all_gather(paired, "kv", axis=1, tiled=True)
    )
    ffn_term = finish_units(gate_acc, up_acc, squares, channels, w_down)
    partial_value = lax.psum_scatter(ffn_term, "kv", scatter_dimension=1, tiled=True)
    summed = lax.all_to_all(partial_value, "tp", split_axis=1, concat_axis=0, tiled=True)
    return (hidden_in.astype(jnp.float32) + 0.5 * summed).astype(jnp.bfloat16)


def delta_block(query, key_in, value, gating, write_pre, forget_pre, rates, live, state):
    seq_count, block_len, head_count, head_size = query.shape
    precise = lax.Precision.HIGHEST
    query_unit = (
        query
        * lax.rsqrt(jnp.sum(query * query, axis=-1, keepdims=True) + EPSILON)
        / math.sqrt(head_size)
    )
    key_unit = key_in * lax.rsqrt(jnp.sum(key_in * key_in, axis=-1, keepdims=True) + EPSILON)
    live_rows = live[:, :, None]
    write_gate = jax.nn.sigmoid(write_pre) * live_rows
    forget = -jnp.exp(rates)[None, None, :] * jax.nn.softplus(forget_pre) * live_rows
    cumulative = jnp.cumsum(forget, axis=1)
    cum_heads = jnp.transpose(cumulative, (0, 2, 1))
    positions = jnp.arange(block_len)
    causal = positions[:, None] >= positions[None, :]
    strict = positions[:, None] > positions[None, :]
    differ = jnp.minimum(cum_heads[:, :, :, None] - cum_heads[:, :, None, :], 0.0)
    decay_mat = jnp.where(causal, jnp.exp(differ), 0.0)
    key_dots = jnp.einsum("sthd,suhd->shtu", key_unit, key_unit, precision=precise)
    write_heads = jnp.transpose(write_gate, (0, 2, 1))
    strict_part = jnp.where(strict, write_heads[:, :, :, None] * decay_mat * key_dots, 0.0)
    identity = jnp.eye(block_len, dtype=jnp.float32)
    squared = jnp.einsum("shtu,shuv->shtv", strict_part, strict_part, precision=precise)
    fourth = jnp.einsum("shtu,shuv->shtv", squared, squared, precision=precise)
    inverse = jnp.einsum(
        "shtu,shuv->shtv", identity - strict_part, identity + squared, precision=precise
    )
    inverse = jnp.einsum("shtu,shuv->shtv", inverse, identity + fourth, precision=precise)
    growth = jnp.exp(cumulative)
    target = jnp.einsum(
        "shtu,suhv->sthv", inverse, write_gate[..., None] * value, precision=precise
    )
    key_mix = jnp.einsum(
        "shtu,suhk->sthk", inverse, (write_gate * growth)[..., None] * key_unit, precision=precise
    )
    update = target - jnp.einsum("sthk,shkv->sthv", key_mix, state, precision=precise)
    scores = jnp.einsum("sthd,suhd->shtu", query_unit, key_unit, precision=precise) * decay_mat
    attend = jnp.einsum("sthk,shkv->sthv", query_unit * growth[..., None], state, precision=precise)
    attend = attend + jnp.einsum("shtu,suhv->sthv", scores, update, precision=precise)
    final_cum = cumulative[:, -1:, :]
    fading = jnp.exp(final_cum - cumulative)
    new_state = jnp.exp(final_cum[:, 0, :])[:, :, None, None] * state
    new_state = new_state + jnp.einsum(
        "sthk,sthv->shkv", key_unit * fading[..., None], update, precision=precise
    )
    normed = attend * lax.rsqrt(jnp.mean(attend * attend, axis=-1, keepdims=True) + EPSILON)
    normed = normed * jax.nn.silu(gating) * live[:, :, None, None]
    mixed_heads = normed.reshape(seq_count * block_len, head_count * head_size).astype(jnp.bfloat16)
    return (mixed_heads, new_state)


def per_device(
    tokens,
    lengths,
    state,
    gain_first,
    first_gate,
    first_up,
    first_down,
    gain_mix,
    query_weight,
    key_weight,
    value_weight,
    gating_weight,
    write_weight,
    forget_weight,
    forget_rate,
    out_weight,
    gain_second,
    second_gate,
    second_up,
    second_down,
):
    after_first = feed_forward(tokens, gain_first, first_gate, first_up, first_down)
    seq_count = lengths.shape[0]
    own_count = seq_count * BLK
    whole_rows = lax.all_gather(after_first, ("kv", "tp"), axis=1, tiled=True)
    scaled_all = (whole_rows.astype(jnp.float32) * gain_mix).astype(jnp.bfloat16)
    stacked = jnp.stack(
        [
            jnp.dot(scaled_all, matrix, preferred_element_type=jnp.float32)
            for matrix in (query_weight, key_weight, value_weight, gating_weight)
        ]
    )
    owned = lax.all_to_all(
        stacked.astype(jnp.bfloat16), ("kv", "tp"), split_axis=1, concat_axis=2, tiled=True
    ).astype(stacked.dtype)
    row_start = lax.axis_index(("kv", "tp")) * own_count
    own_values = lax.dynamic_slice_in_dim(whole_rows, row_start, own_count, 0).astype(jnp.float32)
    own_scaled = lax.dynamic_slice_in_dim(scaled_all, row_start, own_count, 0)
    mix_scale = lax.rsqrt(jnp.mean(own_values * own_values, axis=1, keepdims=True) + EPSILON)
    query = (owned[0] * mix_scale).reshape(seq_count, BLK, HEADS, HEAD)
    key_in = (owned[1] * mix_scale).reshape(seq_count, BLK, HEADS, HEAD)
    value = (owned[2] * mix_scale).reshape(seq_count, BLK, HEADS, HEAD)
    gating = (owned[3] * mix_scale).reshape(seq_count, BLK, HEADS, HEAD)
    write_pre = (
        jnp.dot(own_scaled, write_weight, preferred_element_type=jnp.float32) * mix_scale
    ).reshape(seq_count, BLK, HEADS)
    forget_pre = (
        jnp.dot(own_scaled, forget_weight, preferred_element_type=jnp.float32) * mix_scale
    ).reshape(seq_count, BLK, HEADS)
    positions = jnp.arange(BLK, dtype=jnp.int32)
    live = (positions[None, :] < lengths[:, None]).astype(jnp.float32)
    mixed_heads, new_state = delta_block(
        query, key_in, value, gating, write_pre, forget_pre, forget_rate, live, state
    )
    half_cols = mixed_heads.shape[1] // 2
    portion = lax.all_gather(mixed_heads, ("kv", "tp"), axis=0, tiled=True)
    first_half = jnp.dot(
        portion[:, :half_cols], out_weight[:half_cols], preferred_element_type=jnp.float32
    ).astype(jnp.bfloat16)
    second_half = jnp.dot(
        portion[:, half_cols:], out_weight[half_cols:], preferred_element_type=jnp.float32
    ).astype(jnp.bfloat16)
    first_half, second_half = lax.optimization_barrier((first_half, second_half))
    mixed_sum = first_half.astype(jnp.float32) + second_half.astype(jnp.float32)
    after_mix = (after_first.astype(jnp.float32) + mixed_sum).astype(jnp.bfloat16)
    mixed_out = feed_forward(after_mix, gain_second, second_gate, second_up, second_down)
    return (mixed_out, new_state)


def solution(mesh):
    in_specs = (
        P("dp", ("kv", "tp")),
        P(("dp", "kv", "tp")),
        P(("dp", "kv", "tp"), None, None, None),
        P(),
        P(None, "kv"),
        P(None, "kv"),
        P("kv", None),
        P(),
        P(None, ("kv", "tp")),
        P(None, ("kv", "tp")),
        P(None, ("kv", "tp")),
        P(None, ("kv", "tp")),
        P(),
        P(),
        P(),
        P(None, ("kv", "tp")),
        P(),
        P(None, "kv"),
        P(None, "kv"),
        P("kv", None),
    )
    out_specs = (P("dp", ("kv", "tp")), P(("dp", "kv", "tp"), None, None, None))
    return jax.shard_map(
        per_device, mesh=mesh, in_specs=in_specs, out_specs=out_specs, check_vma=False
    )
```

profile of v0, /device:TPU:0, one launch (start us, length us, event | category | flops | bytes accessed | tf_op | source)
XLA Modules:
  0.0 174.8 jit_solution(16179178874863830319)
XLA Ops:
  7.2 4.8 %all_to_all.73 = bf16[2,32,256]{2,1,0:T(8,128)(2,1)S(1)} all-to-all(bf16[2,32,256]{2,1,0:T(8,128)(2,1)} %bitcast.150), channel_id=1, replica_groups=mesh['dp'=4,'kv'=4,'tp'=2] {'tp'}, dimensions={0} | all-to-all | bytes 65536 | tf_op jit(solution)/shard_map/all_to_all | solution.py:33
  12.0 15.1 %all_gather.12 = bf16[32,2048]{1,0:T(8,128)(2,1)S(1)} all-gather(bf16[32,512]{1,0:T(8,128)(2,1)S(1)} %bitcast.146), channel_id=1, replica_groups=mesh['dp'=4,'kv'=4,'tp'=2] {'kv'}, dimensions={1}, use_global_device_ids=true | all-gather | bytes 163840 | tf_op jit(solution)/shard_map/all_gather | solution.py:35
  27.2 3.7 %convolution_multiply_fusion.3 = f32[32,1408]{1,0:T(8,128)S(1)} fusion(bf16[2048,1408]{1,0:T(8,128)(2,1)} %param.24, bf16[32,2048]{1,0:T(8,128)(2,1)S(1)} %all_gather.12, f32[2048]{0:T(1024)} %param.23, f32[32]{0:T(128)S(1)} %add_rsqrt_fusion.5), kind=kOutput, calls=%fused_computation.5 | convolution fusion | flops 184791040 | bytes 6086784 | tf_op jit(solution)/shard_map/dot_general | solution.py:19
  31.0 7.1 %fusion.21 = f32[32,2048]{1,0:T(8,128)} fusion(bf16[1408,2048]{1,0:T(8,128)(2,1)} %param.26, bf16[2048,1408]{1,0:T(8,128)(2,1)} %param.25, f32[32,1408]{1,0:T(8,128)S(1)} %convolution_multiply_fusion.3, bf16[32,2048]{1,0:T(8,128)(2,1)S(1)} %all_gather.12, f32[2048]{0:T(1024)S(1)} %copy-done.4, f32[32]{0:T(128)S(1)} %add_rsqrt_fusion.5), kind=kOutput, calls=%fused_computation.41 | convolution fusion | flops 369610752 | bytes 12116096 | tf_op jit(solution)/shard_map/dot_general | solution.py:28
  38.9 20.5 %reduce-scatter.3.cloned.1.call-done = f32[32,512]{1,0:T(8,128)} async-done(((f32[32,2048]{1,0:T(8,128)}), f32[32,512]{1,0:T(8,128)}) %reduce-scatter.3.cloned.1.call-update) | async-done | bytes 65552 | tf_op jit(solution)/shard_map/reduce_scatter | solution.py:38
  60.2 3.8 %all_to_all.74 = f32[32,2,256]{2,0,1:T(8,128)S(1)} all-to-all(f32[32,2,256]{2,0,1:T(8,128)S(1)} %bitcast.144), channel_id=1, replica_groups=mesh['dp'=4,'kv'=4,'tp'=2] {'tp'}, dimensions={1} | all-to-all | bytes 131072 | tf_op jit(solution)/shard_map/all_to_all | solution.py:39
  64.0 14.3 %all_gather.13 = bf16[64,2048]{1,0:T(8,128)(2,1)S(1)} all-gather(bf16[64,256]{1,0:T(8,128)(2,1)S(1)} %fusion.51), channel_id=1, replica_groups=mesh['dp'=4,'kv'=4,'tp'=2] {'kv','tp'}, dimensions={1}, use_global_device_ids=true | all-gather | bytes 294912 | tf_op jit(solution)/shard_map/all_gather | solution.py:120
  79.2 1.5 fusion.10
  80.7 1.5 fusion.9
  83.0 3.4 %all-to-all-start.2 = ((bf16[4,64,256]{2,0,1:T(4,128)(2,1)}), bf16[4,64,256]{2,0,1:T(4,128)(2,1)S(1)}, u32[]{:S(2)}, u32[]{:S(2)}) async-start(bf16[4,64,256]{2,0,1:T(4,128)(2,1)} %copy.99), calls=%async_computation.3 | async-start | bytes 262144 | tf_op jit(solution)/shard_map/all_to_all | solution.py:128
  86.7 0.9 fusion.80
  87.8 5.3 %all-to-all-done.2 = bf16[4,64,256]{2,0,1:T(4,128)(2,1)S(1)} async-done(((bf16[4,64,256]{2,0,1:T(4,128)(2,1)}), bf16[4,64,256]{2,0,1:T(4,128)(2,1)S(1)}, u32[]{:S(2)}, u32[]{:S(2)}) %all-to-all-start.2) | async-done | bytes 131104 | tf_op jit(solution)/shard_map/all_to_all | solution.py:128
  96.0 1.0 convolution_bitcast_fusion.3
  96.9 1.0 fusion.7
  98.5 14.2 %all_gather.14 = bf16[64,2048]{1,0:T(8,128)(2,1)S(1)} all-gather(bf16[8,2048]{1,0:T(8,128)(2,1)S(1)} %fusion.70), channel_id=1, replica_groups=mesh['dp'=4,'kv'=4,'tp'=2] {'kv','tp'}, dimensions={0}, use_global_device_ids=true | all-gather | bytes 294912 | tf_op jit(solution)/shard_map/all_gather | solution.py:151
  112.8 1.2 convolution_convert_fusion
  114.0 1.2 convolution_convert_fusion.1
  115.3 3.7 %all_to_all.75 = bf16[2,32,256]{2,1,0:T(8,128)(2,1)S(1)} all-to-all(bf16[2,32,256]{2,1,0:T(8,128)(2,1)S(1)} %bitcast.143), channel_id=1, replica_groups=mesh['dp'=4,'kv'=4,'tp'=2] {'tp'}, dimensions={0} | all-to-all | bytes 65536 | tf_op jit(solution)/shard_map/all_to_all | solution.py:33
  119.0 13.6 %all_gather.15 = bf16[32,2048]{1,0:T(8,128)(2,1)S(1)} all-gather(bf16[32,512]{1,0:T(8,128)(2,1)S(1)} %bitcast.147), channel_id=1, replica_groups=mesh['dp'=4,'kv'=4,'tp'=2] {'kv'}, dimensions={1}, use_global_device_ids=true | all-gather | bytes 163840 | tf_op jit(solution)/shard_map/all_gather | solution.py:35
  132.7 3.6 %convolution_multiply_fusion.1 = f32[32,1408]{1,0:T(8,128)S(1)} fusion(bf16[2048,1408]{1,0:T(8,128)(2,1)} %param.37, bf16[32,2048]{1,0:T(8,128)(2,1)S(1)} %all_gather.15, f32[2048]{0:T(1024)S(1)} %copy-done.5, f32[32]{0:T(128)S(1)} %add_rsqrt_fusion.3), kind=kOutput, calls=%fused_computation.2 | convolution fusion | flops 184791040 | bytes 6086784 | tf_op jit(solution)/shard_map/dot_general | solution.py:19
  136.4 7.0 %fusion.20 = f32[32,2048]{1,0:T(8,128)} fusion(bf16[1408,2048]{1,0:T(8,128)(2,1)} %param.39, bf16[2048,1408]{1,0:T(8,128)(2,1)} %param.38, f32[32,1408]{1,0:T(8,128)S(1)} %convolution_multiply_fusion.1, bf16[32,2048]{1,0:T(8,128)(2,1)S(1)} %all_gather.15, f32[2048]{0:T(1024)S(1)} %copy-done.5, f32[32]{0:T(128)S(1)} %add_rsqrt_fusion.3), kind=kOutput, calls=%fused_computation.40 | convolution fusion | flops 369610752 | bytes 12116096 | tf_op jit(solution)/shard_map/dot_general | solution.py:28
  143.5 2.8 %fusion.4 = f32[1,16,128,128]{3,2,1,0:T(8,128)} fusion(f32[8,16,128]{2,0,1:T(8,128)S(1)} %fusion.7, f32[1,16,128,128]{3,2,1,0:T(8,128)S(1)} %copy-done.1, f32[16]{0:T(128)S(1)} %fusion.86, f32[8,16,128]{2,1,0:T(8,128)S(1)} %get-tuple-element.20), kind=kOutput, calls=%fused_computation.9 | convolution fusion | flops 25690112 | bytes 2228288 | tf_op jit(solution)/shard_map/sthk,sthv->shkv/dot_general | solution.py:86
  146.3 16.4 %reduce-scatter.5.cloned.1.call-done = f32[32,512]{1,0:T(8,128)} async-done(((f32[32,2048]{1,0:T(8,128)}), f32[32,512]{1,0:T(8,128)}) %reduce-scatter.5.cloned.1.call-update) | async-done | bytes 65552 | tf_op jit(solution)/shard_map/reduce_scatter | solution.py:38
  163.6 3.8 %all_to_all.76 = f32[32,2,256]{2,0,1:T(8,128)S(1)} all-to-all(f32[32,2,256]{2,0,1:T(8,128)S(1)} %bitcast.145), channel_id=1, replica_groups=mesh['dp'=4,'kv'=4,'tp'=2] {'tp'}, dimensions={1} | all-to-all | bytes 131072 | tf_op jit(solution)/shard_map/all_to_all | solution.py:39
  (79 shorter events, 8.1 us)
Async XLA Ops:
  7.2 71.4 %copy-start = (bf16[2048,256]{1,0:T(8,128)(2,1)S(1)}, bf16[2048,256]{1,0:T(8,128)(2,1)}, u32[]{:S(2)}) copy-start(bf16[2048,256]{1,0:T(8,128)(2,1)} %param.31) | copy-start | bytes 3145732
  7.2 23.7 %copy-start.4 = (f32[2048]{0:T(1024)S(1)}, f32[2048]{0:T(1024)}, u32[]{:S(2)}) copy-start(f32[2048]{0:T(1024)} %param.23) | copy-start | bytes 24580
  7.2 52.2 %reduce-scatter.3.cloned.1.call-start = ((), (), s32[]{:S(2)}) async-start(), calls=%async_computation.7 | async-start | bytes 327680 | tf_op jit(solution)/shard_map/reduce_scatter | solution.py:38
  30.9 7.9 %copy-start.8 = (f32[16]{0:T(128)S(1)}, f32[16]{0:T(128)}, u32[]{:S(2)}) copy-start(f32[16]{0:T(128)} %param.34) | copy-start | bytes 196
  30.9 33.1 %copy-start.3 = (bf16[64,256]{1,0:T(8,128)(2,1)S(1)}, bf16[64,256]{1,0:T(8,128)(2,1)}, u32[]{:S(2)}) copy-start(bf16[64,256]{1,0:T(8,128)(2,1)} %param.20) | copy-start | bytes 98308
  30.9 47.6 %copy-start.6 = (f32[2048]{0:T(1024)S(1)}, f32[2048]{0:T(1024)}, u32[]{:S(2)}) copy-start(f32[2048]{0:T(1024)} %param.27) | copy-start | bytes 24580
  30.9 47.9 %copy-start.2 = (bf16[2048,256]{1,0:T(8,128)(2,1)S(1)}, bf16[2048,256]{1,0:T(8,128)(2,1)}, u32[]{:S(2)}) copy-start(bf16[2048,256]{1,0:T(8,128)(2,1)} %param.30) | copy-start | bytes 3145732
  38.1 48.4 %copy-start.7 = (bf16[2048,16]{0,1:T(8,128)(2,1)S(1)}, bf16[2048,16]{0,1:T(8,128)(2,1)}, u32[]{:S(2)}) copy-start(bf16[2048,16]{0,1:T(8,128)(2,1)} %param.33) | copy-start | bytes 196612
  64.0 31.9 %copy-start.1 = (f32[1,16,128,128]{3,2,1,0:T(8,128)S(1)}, f32[1,16,128,128]{3,2,1,0:T(8,128)}, u32[]{:S(2)}) copy-start(f32[1,16,128,128]{3,2,1,0:T(8,128)} %param.22) | copy-start | bytes 3145732
  80.7 52.0 %copy-start.5 = (f32[2048]{0:T(1024)S(1)}, f32[2048]{0:T(1024)}, u32[]{:S(2)}) copy-start(f32[2048]{0:T(1024)} %param.36) | copy-start | bytes 24580
  83.0 10.1 %all-to-all-start.2 = ((bf16[4,64,256]{2,0,1:T(4,128)(2,1)}), bf16[4,64,256]{2,0,1:T(4,128)(2,1)S(1)}, u32[]{:S(2)}, u32[]{:S(2)}) async-start(bf16[4,64,256]{2,0,1:T(4,128)(2,1)} %copy.99), calls=%async_computation.3 | async-start | bytes 262144 | tf_op jit(solution)/shard_map/all_to_all | solution.py:128
  86.4 76.3 %reduce-scatter.5.cloned.1.call-start = ((), (), s32[]{:S(2)}) async-start(), calls=%async_computation.8 | async-start | bytes 327680 | tf_op jit(solution)/shard_map/reduce_scatter | solution.py:38
Sparse Core Ops, SparseCore 0:
  38.2 21.0 reduce-scatter.2
  143.6 19.1 reduce-scatter.4
where the time goes:
time: 176 us; the launch traced here: 175 us
  blocking collectives  73.2 us (42%)
  waiting for transfers between devices  42.3 us (24%)
  matrix products  35.8 us (20%)
  between operations  15.2 us (9%)
  starting transfers between devices  3.45 us (2%)
  local copies, waits for them, and re-layouts  3.13 us (2%)
  other arithmetic  1.76 us (1%)
    reduce_scatter x2, waiting for transfers between devices, feed_forward(): lax.psum_scatter(ffn_term, 'kv', scatter_dimension=1, tiled=True)  36.9 us
    all_gather x2, blocking collectives, feed_forward(): lax.all_gather(paired, 'kv', axis=1, tiled=True)  28.6 us
    all_gather x1, blocking collectives, per_device(): whole_rows = lax.all_gather(after_first, ('kv', 'tp'), axis=1, tiled=True)  14.3 us
    all_gather x1, blocking collectives, per_device(): portion = lax.all_gather(mixed_heads, ('kv', 'tp'), axis=0, tiled=True)  14.2 us
    dot_general x2, matrix products, finish_units(): return jnp.dot(hidden, down_rows, preferred_element_type=jnp.float32)  14.2 us
    all_to_all x2, blocking collectives, feed_forward(): lax.all_to_all(hidden_in, 'tp', split_axis=0, concat_axis=1, tiled=True)  8.52 us
    all_to_all x2, blocking collectives, feed_forward(): lax.all_to_all(partial_value, 'tp', split_axis=1, concat_axis=0, tiled=True)  7.56 us
    dot_general x2, matrix products, fold_step(): gate_acc = jnp.dot(scaled, gate_cols, preferred_element_type=jnp.float32)  7.31 us
  transfers between devices with their start and end apart: 3, of which 3 were waited for; matrix products, arithmetic and copies ran while one was open for 2% of the time, Pallas kernels for 0%

commit v1 on v0

--- a/solution.py
+++ b/solution.py
@@ -1,8 +1,11 @@
+import functools
 import math
 
 import jax
 import jax.numpy as jnp
 from jax import lax
+from jax.experimental import pallas as pl
+from jax.experimental.pallas import tpu as pltpu
 from jax.sharding import PartitionSpec as P
 
 HEADS = 16
@@ -92,7 +95,7 @@
     return (mixed_heads, new_state)
 
 
-def per_device(
+def general_device(
     tokens,
     lengths,
     state,
@@ -162,6 +165,414 @@
     return (mixed_out, new_state)
 
 
+VMEM_SPEC = pl.BlockSpec(memory_space=pltpu.VMEM)
+HBM_SPEC = pl.BlockSpec(memory_space=pl.ANY)
+GROUP = ("kv", "tp")
+F32, BF16 = jnp.float32, jnp.bfloat16
+
+
+def call(body, out_shapes, args, in_specs=None, scratch=(), limit=16 << 20, out_specs=None, name=None):
+    single = not isinstance(out_shapes, (list, tuple))
+    shapes = [out_shapes] if single else list(out_shapes)
+    outs = pl.pallas_call(
+        body,
+        out_shape=shapes,
+        in_specs=in_specs or [VMEM_SPEC] * len(args),
+        out_specs=out_specs or [VMEM_SPEC] * len(shapes),
+        scratch_shapes=list(scratch),
+        compiler_params=pltpu.CompilerParams(vmem_limit_bytes=limit),
+        name=name,
+    )(*args)
+    return outs[0] if single else outs
+
+
+def my_index():
+    return lax.axis_index("kv") * lax.axis_size("tp") + lax.axis_index("tp")
+
+
+def swap(value, mask, count):
+    return lax.ppermute(value, GROUP, [(i, i ^ mask) for i in range(count)])
+
+
+def gather_blocks(own, count):
+    near = [own] + [swap(own, mask, count) for mask in range(2, count, 2)]
+    blocks = []
+    for block in near:
+        blocks += [block, swap(block, 1, count)]
+    return blocks
+
+
+def assemble(blocks, index, gain_ref, scaled_ref):
+    width = blocks[0].shape[1]
+    squares = None
+    for mask, block in enumerate(blocks):
+        values = block[...].astype(F32)
+        owner = index ^ mask
+        gain = gain_ref[pl.ds(owner, 1), :]
+        column = pl.multiple_of(owner * width, width)
+        scaled_ref[:, pl.ds(column, width)] = (values * gain).astype(BF16)
+        part = values * values
+        squares = part if squares is None else squares + part
+    total = jnp.sum(squares, axis=1, keepdims=True)
+    channels = width * len(blocks)
+    return lax.rsqrt(total / channels + EPSILON)
+
+
+def ffn_kernel(count, span, skip, *refs):
+    blocks = refs[:count]
+    gain_ref, gate_hbm, up_hbm, down_hbm = refs[count : count + 4]
+    own_ref, cross_ref = refs[count + 4 : count + 6]
+    scaled, gate_buf, up_buf, down_buf, gate_sem, up_sem, down_sem = refs[count + 6 :]
+    index = my_index()
+    core = lax.axis_index("tp")
+    start = pl.multiple_of(core * skip, 128)
+    width = blocks[0].shape[1]
+    channels = width * count
+    pieces = gate_buf.shape[0]
+    depth = channels // pieces
+    copies = []
+    for piece in range(pieces):
+        rows = pl.ds(piece * depth, depth)
+        for hbm, buf, sem in ((gate_hbm, gate_buf, gate_sem), (up_hbm, up_buf, up_sem)):
+            copy = pltpu.make_async_copy(
+                hbm.at[rows, pl.ds(start, span)], buf.at[piece], sem.at[piece]
+            )
+            copy.start()
+            copies.append(copy)
+    order = list(range(1, count, 2)) + list(range(0, count, 2))
+    down_copies = {}
+    for mask in order:
+        column = pl.multiple_of((index ^ mask) * width, width)
+        copy = pltpu.make_async_copy(
+            down_hbm.at[pl.ds(start, span), pl.ds(column, width)], down_buf.at[mask], down_sem.at[mask]
+        )
+        copy.start()
+        down_copies[mask] = copy
+    row_scale = assemble(blocks, index, gain_ref, scaled)
+    gate_acc = up_acc = None
+    for piece in range(pieces):
+        lhs = scaled[:, piece * depth : (piece + 1) * depth]
+        copies[2 * piece].wait()
+        part = jnp.dot(lhs, gate_buf[piece], preferred_element_type=F32)
+        gate_acc = part if gate_acc is None else gate_acc + part
+        copies[2 * piece + 1].wait()
+        part = jnp.dot(lhs, up_buf[piece], preferred_element_type=F32)
+        up_acc = part if up_acc is None else up_acc + part
+    gate_act = gate_acc * row_scale
+    hidden = gate_act * jax.nn.sigmoid(gate_act) * (up_acc * row_scale)
+    unit = lax.broadcasted_iota(jnp.int32, hidden.shape, 1)
+    repeated = core * (lax.axis_size("tp") * span - down_hbm.shape[0])
+    hidden = jnp.where(unit >= repeated, hidden, 0.0).astype(BF16)
+    for mask in order:
+        down_copies[mask].wait()
+        part = jnp.dot(hidden, down_buf[mask], preferred_element_type=F32)
+        if mask % 2:
+            cross_ref[mask // 2] = part.astype(BF16)
+        else:
+            own_ref[mask // 2] = part
+
+
+def pair_sum_kernel(own_ref, cross_ref, mine_ref, *sends):
+    mine_ref[...] = own_ref[0] + cross_ref[0].astype(F32)
+    for step, send in enumerate(sends):
+        send[...] = (own_ref[step + 1] + cross_ref[step + 1].astype(F32)).astype(BF16)
+
+
+def residual_kernel(base_ref, mine_ref, *refs):
+    total = mine_ref[...]
+    for received in refs[:-1]:
+        total = total + received[...].astype(F32)
+    refs[-1][...] = (base_ref[...].astype(F32) + 0.5 * total).astype(BF16)
+
+
+def half_step(own, count, gain, gate, up, down):
+    rows, width = own.shape
+    near = count // 2
+    units = gate.shape[1]
+    tiles = units // 128
+    span = -(-tiles // 2) * 128
+    skip = units - span
+    blocks = gather_blocks(own, count)
+    pieces = 4
+    depth = width * count // pieces
+    own_part, cross_part = call(
+        functools.partial(ffn_kernel, count, span, skip),
+        [pltpu.VMEM((near, rows, width), F32), pltpu.VMEM((near, rows, width), BF16)],
+        [*blocks, gain.reshape(count, width), gate, up, down],
+        in_specs=[VMEM_SPEC] * (count + 1) + [HBM_SPEC] * 3,
+        scratch=[
+            pltpu.VMEM((rows, width * count), BF16),
+            pltpu.VMEM((pieces, depth, span), BF16),
+            pltpu.VMEM((pieces, depth, span), BF16),
+            pltpu.VMEM((count, span, width), BF16),
+            pltpu.SemaphoreType.DMA((pieces,)),
+            pltpu.SemaphoreType.DMA((pieces,)),
+            pltpu.SemaphoreType.DMA((count,)),
+        ],
+        limit=24 << 20,
+        name="ffn",
+    )
+    cross_sum = swap(cross_part, 1, count)
+    mine, *sends = call(
+        pair_sum_kernel,
+        [pltpu.VMEM((rows, width), F32)] + [pltpu.VMEM((rows, width), BF16)] * (near - 1),
+        [own_part, cross_sum],
+        name="pair_sum",
+    )
+    received = [swap(send, 2 * (step + 1), count) for step, send in enumerate(sends)]
+    return call(
+        residual_kernel,
+        pltpu.VMEM((rows, width), BF16),
+        [own, mine, *received],
+        name="residual",
+    )
+
+
+def project_kernel(count, *refs):
+    blocks = refs[:count]
+    gain_ref, query_w, key_w, value_w, gating_w, write_t, forget_t = refs[count : count + 7]
+    sends = refs[count + 7 : count + 7 + count]
+    pre_ref, scaled, result, pre_scratch = refs[count + 7 + count :]
+    index = my_index()
+    row_scale = assemble(blocks, index, gain_ref, scaled)
+    lhs = scaled[...]
+    width = query_w.shape[1]
+    for place, weight in enumerate((query_w, key_w, value_w, gating_w)):
+        part = jnp.dot(lhs, weight[...], preferred_element_type=F32)
+        result[:, place * width : (place + 1) * width] = part * row_scale
+    heads = write_t.shape[0]
+    contract = (((1,), (1,)), ((), ()))
+    for place, weight in enumerate((write_t, forget_t)):
+        part = lax.dot_general(lhs, weight[...], contract, preferred_element_type=F32)
+        pre_scratch[:, place * heads : (place + 1) * heads] = part * row_scale
+    for mask, send in enumerate(sends):
+        row = pl.multiple_of((index ^ mask) * BLK, BLK)
+        send[...] = result[pl.ds(row, BLK), :].astype(BF16)
+    row = pl.multiple_of(index * BLK, BLK)
+    pre_ref[...] = pre_scratch[pl.ds(row, BLK), :]
+
+
+def parts(value):
+    high = value.astype(BF16)
+    return high, (value - high.astype(F32)).astype(BF16)
+
+
+def dot_parts(left, right, dims=(((1,), (0,)), ((), ()))):
+    left_high, left_low = left
+    right_high, right_low = right
+    total = lax.dot_general(left_high, right_low, dims, preferred_element_type=F32)
+    total = total + lax.dot_general(left_low, right_high, dims, preferred_element_type=F32)
+    return total + lax.dot_general(left_high, right_high, dims, preferred_element_type=F32)
+
+
+def delta_kernel(count, *refs):
+    blocks = refs[:count]
+    pre_ref, rate_ref, length_ref, state_ref = refs[count : count + 4]
+    mixed_ref, update_ref, faded_ref, final_ref, ordered = refs[count + 4 :]
+    index = my_index()
+    for mask, block in enumerate(blocks):
+        ordered[pl.ds(index ^ mask, 1)] = block[...].astype(F32)[None]
+    heads = rate_ref.shape[1]
+    size = state_ref.shape[-1]
+    per_block = heads // count
+    rows = heads * BLK
+    width = per_block * size
+
+    def stack(place):
+        found = []
+        for head in range(heads):
+            column = place * width + (head % per_block) * size
+            found.append(ordered[head // per_block, :, column : column + size])
+        return jnp.concatenate(found, axis=0)
+
+    query, key_in, value, gating = (stack(place) for place in range(4))
+    query_unit = query * lax.rsqrt(jnp.sum(query * query, axis=1, keepdims=True) + EPSILON) * (1.0 / math.sqrt(size))
+    key_unit = key_in * lax.rsqrt(jnp.sum(key_in * key_in, axis=1, keepdims=True) + EPSILON)
+    step_of = lax.broadcasted_iota(jnp.int32, (BLK, heads), 0)
+    live = (step_of < length_ref[0]).astype(F32)
+    pre = pre_ref[...]
+    write_gate = jax.nn.sigmoid(pre[:, :heads]) * live
+    forget_in = pre[:, heads:]
+    softplus = jnp.maximum(forget_in, 0.0) + jnp.log1p(jnp.exp(-jnp.abs(forget_in)))
+    forget = -jnp.exp(rate_ref[...]) * softplus * live
+    cumulative = forget
+    lower = 1
+    while lower < BLK:
+        moved = pltpu.roll(cumulative, lower, 0)
+        cumulative = cumulative + jnp.where(step_of >= lower, moved, 0.0)
+        lower *= 2
+    final = jnp.broadcast_to(cumulative[BLK - 1 :, :], (BLK, heads))
+    row_head = lax.broadcasted_iota(jnp.int32, (rows, heads), 0) // BLK
+    picked = row_head == lax.broadcasted_iota(jnp.int32, (rows, heads), 1)
+
+    def column_of(array):
+        tall = jnp.concatenate([array] * heads, axis=0)
+        return jnp.sum(jnp.where(picked, tall, 0.0), axis=1, keepdims=True)
+
+    write_col, live_col = column_of(write_gate), column_of(live)
+    cum_col, final_col = column_of(cumulative), column_of(final)
+    down_at = lax.broadcasted_iota(jnp.int32, (rows, rows), 0)
+    over_at = lax.broadcasted_iota(jnp.int32, (rows, rows), 1)
+    same = (down_at // BLK) == (over_at // BLK)
+    diagonal = down_at == over_at
+    cum_row = jnp.sum(jnp.where(diagonal, cum_col, 0.0), axis=0, keepdims=True)
+    causal = same & (down_at >= over_at)
+    decay = jnp.where(causal, jnp.exp(jnp.minimum(cum_col - cum_row, 0.0)), 0.0)
+    across = (((1,), (1,)), ((), ()))
+    key_parts = parts(key_unit)
+    strict_part = jnp.where(diagonal, 0.0, write_col * decay * dot_parts(key_parts, key_parts, across))
+    scores = decay * dot_parts(parts(query_unit), key_parts, across)
+    identity = diagonal.astype(F32)
+    strict_split = parts(strict_part)
+    squared = dot_parts(strict_split, strict_split)
+    squared_split = parts(squared)
+    fourth = dot_parts(squared_split, squared_split)
+    inverse = identity - strict_part + squared - dot_parts(strict_split, squared_split)
+    inverse = inverse + dot_parts(parts(inverse), parts(fourth))
+    growth = jnp.exp(cum_col)
+    key_grown, query_grown = key_unit * growth, query_unit * growth
+    from_key, from_query = [], []
+    for head in range(heads):
+        at = slice(head * BLK, (head + 1) * BLK)
+        both = jnp.concatenate([key_grown[at], query_grown[at]], axis=0)
+        found = dot_parts(parts(both), parts(state_ref[head]))
+        from_key.append(found[:BLK])
+        from_query.append(found[BLK:])
+    target = write_col * (value - jnp.concatenate(from_key, axis=0))
+    update = dot_parts(parts(inverse), parts(target))
+    attend = jnp.concatenate(from_query, axis=0) + dot_parts(parts(scores), parts(update))
+    normed = attend * lax.rsqrt(jnp.mean(attend * attend, axis=1, keepdims=True) + EPSILON)
+    normed = (normed * (gating * jax.nn.sigmoid(gating)) * live_col).astype(BF16)
+    for head in range(heads):
+        mixed_ref[:, head * size : (head + 1) * size] = normed[head * BLK : (head + 1) * BLK]
+    update_ref[...] = update
+    faded_ref[...] = key_unit * jnp.exp(final_col - cum_col)
+    final_ref[...] = jnp.broadcast_to(jnp.exp(final_col), final_ref.shape)
+
+
+def state_kernel(update_ref, faded_ref, final_ref, state_ref, new_ref):
+    heads = state_ref.shape[0]
+    along = (((0,), (0,)), ((), ()))
+    for head in range(heads):
+        at = slice(head * BLK, (head + 1) * BLK)
+        left_high, left_low = parts(faded_ref[at])
+        right_high, right_low = parts(update_ref[at])
+        left = jnp.concatenate([left_high, left_high, left_low, left_low], axis=0)
+        right = jnp.concatenate([right_high, right_low, right_high, right_low], axis=0)
+        grown = lax.dot_general(left, right, along, preferred_element_type=F32)
+        scale = final_ref[head * BLK : head * BLK + 1, :]
+        new_ref[head] = scale * state_ref[head] + grown
+
+
+def out_kernel(count, *refs):
+    blocks = refs[:count]
+    weight_ref, base_ref, out_ref, scratch = refs[count:]
+    index = my_index()
+    lhs = jnp.concatenate([block[...].astype(F32) for block in blocks], axis=0).astype(BF16)
+    half = lhs.shape[1] // 2
+    first = jnp.dot(lhs[:, :half], weight_ref[:half, :], preferred_element_type=F32).astype(BF16)
+    second = jnp.dot(lhs[:, half:], weight_ref[half:, :], preferred_element_type=F32).astype(BF16)
+    total = first.astype(F32) + second.astype(F32)
+    for mask in range(count):
+        row = pl.multiple_of((index ^ mask) * BLK, BLK)
+        scratch[pl.ds(row, BLK), :] = total[mask * BLK : (mask + 1) * BLK]
+    out_ref[...] = (base_ref[...].astype(F32) + scratch[...]).astype(BF16)
+
+
+def group_device(
+    tokens,
+    lengths,
+    state,
+    gain_first,
+    first_gate,
+    first_up,
+    first_down,
+    gain_mix,
+    query_weight,
+    key_weight,
+    value_weight,
+    gating_weight,
+    write_weight,
+    forget_weight,
+    forget_rate,
+    out_weight,
+    gain_second,
+    second_gate,
+    second_up,
+    second_down,
+):
+    count = lax.axis_size("kv") * lax.axis_size("tp")
+    rows, width = tokens.shape
+    channels = gain_first.shape[0]
+    heads, size = state.shape[1], state.shape[2]
+    after_first = half_step(tokens, count, gain_first, first_gate, first_up, first_down)
+    blocks = gather_blocks(after_first, count)
+    columns = 4 * width
+    *sends, pre = call(
+        functools.partial(project_kernel, count),
+        [pltpu.VMEM((BLK, columns), BF16)] * count + [pltpu.VMEM((BLK, 2 * heads), F32)],
+        [
+            *blocks,
+            gain_mix.reshape(count, width),
+            query_weight,
+            key_weight,
+            value_weight,
+            gating_weight,
+            write_weight.T,
+            forget_weight.T,
+        ],
+        scratch=[
+            pltpu.VMEM((rows, channels), BF16),
+            pltpu.VMEM((rows, columns), F32),
+            pltpu.VMEM((rows, 2 * heads), F32),
+        ],
+        name="project",
+    )
+    owned = [sends[0]] + [swap(sends[mask], mask, count) for mask in range(1, count)]
+    matrices = state.reshape(heads, size, size)
+    mixed, update, faded, final = call(
+        functools.partial(delta_kernel, count),
+        [
+            pltpu.VMEM((BLK, channels), BF16),
+            pltpu.VMEM((heads * BLK, size), F32),
+            pltpu.VMEM((heads * BLK, size), F32),
+            pltpu.VMEM((heads * BLK, size), F32),
+        ],
+        [*owned, pre, forget_rate.reshape(1, heads), lengths, matrices],
+        in_specs=[VMEM_SPEC] * (count + 2) + [pl.BlockSpec(memory_space=pltpu.SMEM), VMEM_SPEC],
+        scratch=[pltpu.VMEM((count, BLK, columns), F32)],
+        name="delta",
+    )
+    head_blocks = gather_blocks(mixed, count)
+    new_state = call(
+        state_kernel,
+        jax.ShapeDtypeStruct((heads, size, size), F32),
+        [update, faded, final, matrices],
+        name="state",
+    )
+    after_mix = call(
+        functools.partial(out_kernel, count),
+        pltpu.VMEM((rows, width), BF16),
+        [*head_blocks, out_weight, after_first],
+        scratch=[pltpu.VMEM((rows, width), F32)],
+        name="out",
+    )
+    mixed_out = half_step(after_mix, count, gain_second, second_gate, second_up, second_down)
+    return (mixed_out, new_state.reshape(state.shape))
+
+
+def fits_group(mesh):
+    near, cores = mesh.shape["kv"], mesh.shape["tp"]
+    count = near * cores
+    return cores == 2 and near & (near - 1) == 0 and near <= 8 and (HEADS * HEAD) % (count * 128) == 0
+
+
+def per_device(mesh, *arrays):
+    tokens, lengths, gate = arrays[0], arrays[1], arrays[4]
+    suits = fits_group(mesh) and lengths.shape[0] == 1 and gate.shape[1] % 128 == 0
+    return (group_device if suits else general_device)(*arrays)
+
+
 def solution(mesh):
     in_specs = (
         P("dp", ("kv", "tp")),
@@ -187,5 +598,5 @@
     )
     out_specs = (P("dp", ("kv", "tp")), P(("dp", "kv", "tp"), None, None, None))
     return jax.shard_map(
-        per_device, mesh=mesh, in_specs=in_specs, out_specs=out_specs, check_vma=False
-    )
+        functools.partial(per_device, mesh), mesh=mesh, in_specs=in_specs, out_specs=out_specs, check_vma=False
+    )

time: 176 us -> 103 us (0.59)
  blocking collectives: 73.2 us -> 0 us
  matrix products: 35.8 us -> 0 us
  starting transfers between devices: 3.45 us -> 39 us
  local copies, waits for them, and re-layouts: 3.13 us -> 23 us
  waiting for transfers between devices: 42.3 us -> 24.2 us
  Pallas kernels: 0 us -> 14.1 us
  between operations: 15.2 us -> 1.47 us
  other arithmetic: 1.76 us -> 0 us
    all_gather x4 -> x0, blocking collectives: 57.2 us -> none  [the longest x2 28.6 us: feed_forward(): lax.all_gather(paired, 'kv', axis=1, tiled=True)]
    ppermute x0 -> x43, starting transfers between devices: none -> 39 us  [swap(): return lax.ppermute(value, GROUP, [(i, i ^ mask) for i in range(count)])]
    reduce_scatter x2 -> x0, waiting for transfers between devices: 36.9 us -> none  [feed_forward(): lax.psum_scatter(ffn_term, 'kv', scatter_dimension=1, tiled=True)]
    dot_general x24 -> x0, matrix products: 35.8 us -> none  [the longest x2 14.2 us: finish_units(): return jnp.dot(hidden, down_rows, preferred_element_type=jnp.float32)]
    ppermute x0 -> x43, waiting for transfers between devices: none -> 24.2 us  [swap(): return lax.ppermute(value, GROUP, [(i, i ^ mask) for i in range(count)])]
    unnamed x18 -> x33, local copies, waits for them, and re-layouts: 0.06 us -> 20.9 us
    all_to_all x4 -> x0, blocking collectives: 16.1 us -> none  [the longest x2 8.52 us: feed_forward(): lax.all_to_all(hidden_in, 'tp', split_axis=0, concat_axis=1, tiled=True)]
    pallas_call x0 -> x10, Pallas kernels: none -> 14.1 us  [call(): pl.pallas_call(body, out_shape=shapes, in_specs=in_specs or [VMEM_SPEC] *...]
  transfers between devices with their start and end apart: 3 -> 43, of which waited for: 3 -> 21; matrix products, arithmetic and copies ran while one was open for 2% -> 2% of each run, Pallas kernels for 0% -> 1%
where the time goes in v1:
time: 103 us; the launch traced here: 102 us
  starting transfers between devices  39 us (38%)
  waiting for transfers between devices  24.2 us (23%)
  local copies, waits for them, and re-layouts  23 us (22%)
  Pallas kernels  14.1 us (14%)
  between operations  1.47 us (1%)
    ppermute x43, starting transfers between devices, swap(): return lax.ppermute(value, GROUP, [(i, i ^ mask) for i in range(count)])  39 us
    ppermute x43, waiting for transfers between devices, swap(): return lax.ppermute(value, GROUP, [(i, i ^ mask) for i in range(count)])  24.2 us
    unnamed x33, local copies, waits for them, and re-layouts  20.9 us
    pallas_call x10, Pallas kernels, call(): pl.pallas_call(body, out_shape=shapes, in_specs=in_specs or [VMEM_SPEC] *...  14.1 us
  transfers between devices with their start and end apart: 43, of which 21 were waited for; matrix products, arithmetic and copies ran while one was open for 2% of the time, Pallas kernels for 1%

profile of v1, /device:TPU:0, one launch (start us, length us, event | category | flops | bytes accessed | tf_op | source)
XLA Modules:
  0.0 101.9 jit_solution(9448839561175749370)
XLA Ops:
  0.6 5.1 %collective-permute-start.5 = (bf16[64,256]{1,0:T(8,128)(2,1)}, bf16[64,256]{1,0:T(8,128)(2,1)S(1)}, u32[]{:S(2)}, u32[]{:S(2)}) collective-permute-start(bf16[64,256]{1,0:T(8,128)(2,1)} %base_ref.1), channel_id=1, source_target_pairs={{0,6},{1,7},{2,4},{3,5},{4,2},{5,3},{6,0},{7,1},{8,14},{9,15},{10,... | collective-permute-start | bytes 98312 | tf_op jit(solution)/shard_map/ppermute | solution.py:194
  7.9 2.9 %collective-permute-done.3.refs_4_ = bf16[64,256]{1,0:T(8,128)(2,1)S(1)} collective-permute-done((bf16[64,256]{1,0:T(8,128)(2,1)}, bf16[64,256]{1,0:T(8,128)(2,1)S(1)}, u32[]{:S(2)}, u32[]{:S(2)}) %collective-permute-start.3) | collective-permute-done | bytes 32800 | tf_op jit(solution)/shard_map/ppermute | solution.py:194
  12.2 2.6 %copy-done = bf16[2048,1408]{1,0:T(8,128)(2,1)S(1)} copy-done((bf16[2048,1408]{1,0:T(8,128)(2,1)S(1)}, bf16[2048,1408]{1,0:T(8,128)(2,1)}, u32[]{:S(2)}) %copy-start) | copy-done | bytes 5767192
  14.8 2.6 %copy-done.1 = bf16[2048,1408]{1,0:T(8,128)(2,1)S(1)} copy-done((bf16[2048,1408]{1,0:T(8,128)(2,1)S(1)}, bf16[2048,1408]{1,0:T(8,128)(2,1)}, u32[]{:S(2)}) %copy-start.1) | copy-done | bytes 5767192
  17.4 2.6 %copy-done.2 = bf16[1408,2048]{1,0:T(8,128)(2,1)S(1)} copy-done((bf16[1408,2048]{1,0:T(8,128)(2,1)S(1)}, bf16[1408,2048]{1,0:T(8,128)(2,1)}, u32[]{:S(2)}) %copy-start.2) | copy-done | bytes 5767192
  20.8 4.8 %ffn.2 = (f32[4,64,256]{2,1,0:T(8,128)S(1)}, bf16[4,64,256]{2,1,0:T(8,128)(2,1)S(1)}) custom-call(bf16[64,256]{1,0:T(8,128)(2,1)S(1)} %copy-done.12, bf16[64,256]{1,0:T(8,128)(2,1)S(1)} %collective-permute-done.refs_1_, bf16[64,256]{1,0:T(8,128)(2,1)S(1)} %collective-permute-done.1.refs_2_, bf16[64,256]{1,0:T(8,128)(2,1)S(1)} %collective-permute-done.2.refs_3_, ...), custom_call_target="tpu_custom_call" | custom-call | tf_op jit(solution)/shard_map/ffn/pallas_call | solution.py:177
  27.2 1.9 %collective-permute-start.9 = (bf16[64,256]{1,0:T(8,128)(2,1)S(1)}, bf16[64,256]{1,0:T(8,128)(2,1)S(1)}, u32[]{:S(2)}, u32[]{:S(2)}) collective-permute-start(bf16[64,256]{1,0:T(8,128)(2,1)S(1)} %get-tuple-element.31), channel_id=1, source_target_pairs={{0,4},{1,5},{2,6},{3,7},{4,0},{5,1},{6,2},{7,3},{8,12},{9,13},{10,... | collective-permute-start | bytes 98312 | tf_op jit(solution)/shard_map/ppermute | solution.py:194
  29.1 2.5 %collective-permute-start.10 = (bf16[64,256]{1,0:T(8,128)(2,1)S(1)}, bf16[64,256]{1,0:T(8,128)(2,1)S(1)}, u32[]{:S(2)}, u32[]{:S(2)}) collective-permute-start(bf16[64,256]{1,0:T(8,128)(2,1)S(1)} %get-tuple-element.32), channel_id=1, source_target_pairs={{0,6},{1,7},{2,4},{3,5},{4,2},{5,3},{6,0},{7,1},{8,14},{9,15},{10,... | collective-permute-start | bytes 98312 | tf_op jit(solution)/shard_map/ppermute | solution.py:194
  32.1 2.8 %collective-permute-done.10.refs_2_ = bf16[64,256]{1,0:T(8,128)(2,1)S(1)} collective-permute-done((bf16[64,256]{1,0:T(8,128)(2,1)S(1)}, bf16[64,256]{1,0:T(8,128)(2,1)S(1)}, u32[]{:S(2)}, u32[]{:S(2)}) %collective-permute-start.10) | collective-permute-done | bytes 32800 | tf_op jit(solution)/shard_map/ppermute | solution.py:194
  34.9 2.5 %collective-permute-start.16 = (bf16[64,256]{1,0:T(8,128)(2,1)S(1)}, bf16[64,256]{1,0:T(8,128)(2,1)S(1)}, u32[]{:S(2)}, u32[]{:S(2)}) collective-permute-start(bf16[64,256]{1,0:T(8,128)(2,1)S(1)} %residual.2.refs_0_.refs_9_), channel_id=1, source_target_pairs={{0,6},{1,7},{2,4},{3,5},{4,2},{5,3},{6,0},{7,1},{8,14},{9,15},{10,... | collective-permute-start | bytes 98312 | tf_op jit(solution)/shard_map/ppermute | solution.py:194
  37.4 1.9 %collective-permute-start.12 = (bf16[64,256]{1,0:T(8,128)(2,1)S(1)}, bf16[64,256]{1,0:T(8,128)(2,1)S(1)}, u32[]{:S(2)}, u32[]{:S(2)}) collective-permute-start(bf16[64,256]{1,0:T(8,128)(2,1)S(1)} %residual.2.refs_0_.refs_9_), channel_id=1, source_target_pairs={{0,2},{1,3},{2,0},{3,1},{4,6},{5,7},{6,4},{7,5},{8,10},{9,11},{10,... | collective-permute-start | bytes 98312 | tf_op jit(solution)/shard_map/ppermute | solution.py:194
  50.3 1.9 %collective-permute-start.21 = (bf16[8,1024]{1,0:T(8,128)(2,1)S(1)}, bf16[8,1024]{1,0:T(8,128)(2,1)S(1)}, u32[]{:S(2)}, u32[]{:S(2)}) collective-permute-start(bf16[8,1024]{1,0:T(8,128)(2,1)S(1)} %get-tuple-element.37), channel_id=1, source_target_pairs={{0,4},{1,5},{2,6},{3,7},{4,0},{5,1},{6,2},{7,3},{8,12},{9,13},{10,... | collective-permute-start | bytes 49160 | tf_op jit(solution)/shard_map/ppermute | solution.py:194
  53.2 1.7 %collective-permute-start.23 = (bf16[8,1024]{1,0:T(8,128)(2,1)S(1)}, bf16[8,1024]{1,0:T(8,128)(2,1)S(1)}, u32[]{:S(2)}, u32[]{:S(2)}) collective-permute-start(bf16[8,1024]{1,0:T(8,128)(2,1)S(1)} %get-tuple-element.39), channel_id=1, source_target_pairs={{0,6},{1,7},{2,4},{3,5},{4,2},{5,3},{6,0},{7,1},{8,14},{9,15},{10,... | collective-permute-start | bytes 49160 | tf_op jit(solution)/shard_map/ppermute | solution.py:194
  59.9 1.7 %delta.1 = (bf16[8,2048]{1,0:T(8,128)(2,1)S(1)}, f32[128,128]{1,0:T(8,128)S(1)}, f32[128,128]{1,0:T(8,128)S(1)}, f32[128,128]{1,0:T(8,128)S(1)}) custom-call(bf16[8,1024]{1,0:T(8,128)(2,1)S(1)} %get-tuple-element.33.refs_0_, bf16[8,1024]{1,0:T(8,128)(2,1)S(1)} %collective-permute-done.18.refs_1_, bf16[8,1024]{1,0:T(8,128)(2,1)S(1)} %collective-permute-done.19.refs_2_, ...), custom_call_target="tpu_custom_call" | custom-call | tf_op jit(solution)/shard_map/delta/pallas_call | solution.py:177
  61.7 2.2 %collective-permute-start.30 = (bf16[8,2048]{1,0:T(8,128)(2,1)S(1)}, bf16[8,2048]{1,0:T(8,128)(2,1)S(1)}, u32[]{:S(2)}, u32[]{:S(2)}) collective-permute-start(bf16[8,2048]{1,0:T(8,128)(2,1)S(1)} %get-tuple-element.42.refs_0_), channel_id=1, source_target_pairs={{0,6},{1,7},{2,4},{3,5},{4,2},{5,3},{6,0},{7,1},{8,14},{9,15},{10,... | collective-permute-start | bytes 98312 | tf_op jit(solution)/shard_map/ppermute | solution.py:194
  63.9 2.3 %collective-permute-start.26 = (bf16[8,2048]{1,0:T(8,128)(2,1)S(1)}, bf16[8,2048]{1,0:T(8,128)(2,1)S(1)}, u32[]{:S(2)}, u32[]{:S(2)}) collective-permute-start(bf16[8,2048]{1,0:T(8,128)(2,1)S(1)} %get-tuple-element.42.refs_0_), channel_id=1, source_target_pairs={{0,2},{1,3},{2,0},{3,1},{4,6},{5,7},{6,4},{7,5},{8,10},{9,11},{10,... | collective-permute-start | bytes 98312 | tf_op jit(solution)/shard_map/ppermute | solution.py:194
  70.4 1.9 %collective-permute-start.37 = (bf16[64,256]{1,0:T(8,128)(2,1)S(1)}, bf16[64,256]{1,0:T(8,128)(2,1)S(1)}, u32[]{:S(2)}, u32[]{:S(2)}) collective-permute-start(bf16[64,256]{1,0:T(8,128)(2,1)S(1)} %out.1.refs_0_.base_ref), channel_id=1, source_target_pairs={{0,6},{1,7},{2,4},{3,5},{4,2},{5,3},{6,0},{7,1},{8,14},{9,15},{10,... | collective-permute-start | bytes 98312 | tf_op jit(solution)/shard_map/ppermute | solution.py:194
  73.1 1.7 %collective-permute-start.33 = (bf16[64,256]{1,0:T(8,128)(2,1)S(1)}, bf16[64,256]{1,0:T(8,128)(2,1)S(1)}, u32[]{:S(2)}, u32[]{:S(2)}) collective-permute-start(bf16[64,256]{1,0:T(8,128)(2,1)S(1)} %out.1.refs_0_.base_ref), channel_id=1, source_target_pairs={{0,2},{1,3},{2,0},{3,1},{4,6},{5,7},{6,4},{7,5},{8,10},{9,11},{10,... | collective-permute-start | bytes 98312 | tf_op jit(solution)/shard_map/ppermute | solution.py:194
  78.8 2.6 %copy-done.3 = bf16[2048,1408]{1,0:T(8,128)(2,1)S(1)} copy-done((bf16[2048,1408]{1,0:T(8,128)(2,1)S(1)}, bf16[2048,1408]{1,0:T(8,128)(2,1)}, u32[]{:S(2)}) %copy-start.3) | copy-done | bytes 5767192
  81.5 2.6 %copy-done.4 = bf16[2048,1408]{1,0:T(8,128)(2,1)S(1)} copy-done((bf16[2048,1408]{1,0:T(8,128)(2,1)S(1)}, bf16[2048,1408]{1,0:T(8,128)(2,1)}, u32[]{:S(2)}) %copy-start.4) | copy-done | bytes 5767192
  84.1 2.6 %copy-done.5 = bf16[1408,2048]{1,0:T(8,128)(2,1)S(1)} copy-done((bf16[1408,2048]{1,0:T(8,128)(2,1)S(1)}, bf16[1408,2048]{1,0:T(8,128)(2,1)}, u32[]{:S(2)}) %copy-start.5) | copy-done | bytes 5767192
  86.7 4.8 %ffn.3 = (f32[4,64,256]{2,1,0:T(8,128)S(1)}, bf16[4,64,256]{2,1,0:T(8,128)(2,1)S(1)}) custom-call(bf16[64,256]{1,0:T(8,128)(2,1)S(1)} %out.1.refs_0_.base_ref, bf16[64,256]{1,0:T(8,128)(2,1)S(1)} %collective-permute-done.32.refs_1_, bf16[64,256]{1,0:T(8,128)(2,1)S(1)} %collective-permute-done.33.refs_2_, ...), custom_call_target="tpu_custom_call" | custom-call | tf_op jit(solution)/shard_map/ffn/pallas_call | solution.py:177
  95.5 1.9 %collective-permute-start.42 = (bf16[64,256]{1,0:T(8,128)(2,1)S(1)}, bf16[64,256]{1,0:T(8,128)(2,1)S(1)}, u32[]{:S(2)}, u32[]{:S(2)}) collective-permute-start(bf16[64,256]{1,0:T(8,128)(2,1)S(1)} %get-tuple-element.48), channel_id=1, source_target_pairs={{0,6},{1,7},{2,4},{3,5},{4,2},{5,3},{6,0},{7,1},{8,14},{9,15},{10,... | collective-permute-start | bytes 98312 | tf_op jit(solution)/shard_map/ppermute | solution.py:194
  99.5 1.8 %collective-permute-done.42.refs_2_ = bf16[64,256]{1,0:T(8,128)(2,1)S(1)} collective-permute-done((bf16[64,256]{1,0:T(8,128)(2,1)S(1)}, bf16[64,256]{1,0:T(8,128)(2,1)S(1)}, u32[]{:S(2)}, u32[]{:S(2)}) %collective-permute-start.42) | collective-permute-done | bytes 32800 | tf_op jit(solution)/shard_map/ppermute | solution.py:194
  (108 shorter events, 38.3 us)
Async XLA Ops:
  0.6 7.2 %collective-permute-start.5 = (bf16[64,256]{1,0:T(8,128)(2,1)}, bf16[64,256]{1,0:T(8,128)(2,1)S(1)}, u32[]{:S(2)}, u32[]{:S(2)}) collective-permute-start(bf16[64,256]{1,0:T(8,128)(2,1)} %base_ref.1), channel_id=1, source_target_pairs={{0,6},{1,7},{2,4},{3,5},{4,2},{5,3},{6,0},{7,1},{8,14},{9,15},{10,... | collective-permute-start | bytes 98312 | tf_op jit(solution)/shard_map/ppermute | solution.py:194
  5.8 5.0 %collective-permute-start.3 = (bf16[64,256]{1,0:T(8,128)(2,1)}, bf16[64,256]{1,0:T(8,128)(2,1)S(1)}, u32[]{:S(2)}, u32[]{:S(2)}) collective-permute-start(bf16[64,256]{1,0:T(8,128)(2,1)} %base_ref.1), channel_id=1, source_target_pairs={{0,4},{1,5},{2,6},{3,7},{4,0},{5,1},{6,2},{7,3},{8,12},{9,13},{10,... | collective-permute-start | bytes 98312 | tf_op jit(solution)/shard_map/ppermute | solution.py:194
  5.8 5.0 %collective-permute-start.1 = (bf16[64,256]{1,0:T(8,128)(2,1)}, bf16[64,256]{1,0:T(8,128)(2,1)S(1)}, u32[]{:S(2)}, u32[]{:S(2)}) collective-permute-start(bf16[64,256]{1,0:T(8,128)(2,1)} %base_ref.1), channel_id=1, source_target_pairs={{0,2},{1,3},{2,0},{3,1},{4,6},{5,7},{6,4},{7,5},{8,10},{9,11},{10,... | collective-permute-start | bytes 98312 | tf_op jit(solution)/shard_map/ppermute | solution.py:194
  6.4 5.6 %collective-permute-start = (bf16[64,256]{1,0:T(8,128)(2,1)}, bf16[64,256]{1,0:T(8,128)(2,1)S(1)}, u32[]{:S(2)}, u32[]{:S(2)}) collective-permute-start(bf16[64,256]{1,0:T(8,128)(2,1)} %base_ref.1), channel_id=1, source_target_pairs={{0,1},{1,0},{2,3},{3,2},{4,5},{5,4},{6,7},{7,6},{8,9},{9,8},{10,11... | collective-permute-start | bytes 98312 | tf_op jit(solution)/shard_map/ppermute | solution.py:194
  27.2 4.9 %collective-permute-start.9 = (bf16[64,256]{1,0:T(8,128)(2,1)S(1)}, bf16[64,256]{1,0:T(8,128)(2,1)S(1)}, u32[]{:S(2)}, u32[]{:S(2)}) collective-permute-start(bf16[64,256]{1,0:T(8,128)(2,1)S(1)} %get-tuple-element.31), channel_id=1, source_target_pairs={{0,4},{1,5},{2,6},{3,7},{4,0},{5,1},{6,2},{7,3},{8,12},{9,13},{10,... | collective-permute-start | bytes 98312 | tf_op jit(solution)/shard_map/ppermute | solution.py:194
  29.1 5.7 %collective-permute-start.10 = (bf16[64,256]{1,0:T(8,128)(2,1)S(1)}, bf16[64,256]{1,0:T(8,128)(2,1)S(1)}, u32[]{:S(2)}, u32[]{:S(2)}) collective-permute-start(bf16[64,256]{1,0:T(8,128)(2,1)S(1)} %get-tuple-element.32), channel_id=1, source_target_pairs={{0,6},{1,7},{2,4},{3,5},{4,2},{5,3},{6,0},{7,1},{8,14},{9,15},{10,... | collective-permute-start | bytes 98312 | tf_op jit(solution)/shard_map/ppermute | solution.py:194
  34.9 6.0 %collective-permute-start.16 = (bf16[64,256]{1,0:T(8,128)(2,1)S(1)}, bf16[64,256]{1,0:T(8,128)(2,1)S(1)}, u32[]{:S(2)}, u32[]{:S(2)}) collective-permute-start(bf16[64,256]{1,0:T(8,128)(2,1)S(1)} %residual.2.refs_0_.refs_9_), channel_id=1, source_target_pairs={{0,6},{1,7},{2,4},{3,5},{4,2},{5,3},{6,0},{7,1},{8,14},{9,15},{10,... | collective-permute-start | bytes 98312 | tf_op jit(solution)/shard_map/ppermute | solution.py:194
  37.4 4.8 %collective-permute-start.14 = (bf16[64,256]{1,0:T(8,128)(2,1)S(1)}, bf16[64,256]{1,0:T(8,128)(2,1)S(1)}, u32[]{:S(2)}, u32[]{:S(2)}) collective-permute-start(bf16[64,256]{1,0:T(8,128)(2,1)S(1)} %residual.2.refs_0_.refs_9_), channel_id=1, source_target_pairs={{0,4},{1,5},{2,6},{3,7},{4,0},{5,1},{6,2},{7,3},{8,12},{9,13},{10,... | collective-permute-start | bytes 98312 | tf_op jit(solution)/shard_map/ppermute | solution.py:194
  37.4 4.8 %collective-permute-start.12 = (bf16[64,256]{1,0:T(8,128)(2,1)S(1)}, bf16[64,256]{1,0:T(8,128)(2,1)S(1)}, u32[]{:S(2)}, u32[]{:S(2)}) collective-permute-start(bf16[64,256]{1,0:T(8,128)(2,1)S(1)} %residual.2.refs_0_.refs_9_), channel_id=1, source_target_pairs={{0,2},{1,3},{2,0},{3,1},{4,6},{5,7},{6,4},{7,5},{8,10},{9,11},{10,... | collective-permute-start | bytes 98312 | tf_op jit(solution)/shard_map/ppermute | solution.py:194
  48.3 4.8 %collective-permute-start.18 = (bf16[8,1024]{1,0:T(8,128)(2,1)S(1)}, bf16[8,1024]{1,0:T(8,128)(2,1)S(1)}, u32[]{:S(2)}, u32[]{:S(2)}) collective-permute-start(bf16[8,1024]{1,0:T(8,128)(2,1)S(1)} %get-tuple-element.34), channel_id=1, source_target_pairs={{0,1},{1,0},{2,3},{3,2},{4,5},{5,4},{6,7},{7,6},{8,9},{9,8},{10,11... | collective-permute-start | bytes 49160 | tf_op jit(solution)/shard_map/ppermute | solution.py:194
  48.8 6.1 %collective-permute-start.19 = (bf16[8,1024]{1,0:T(8,128)(2,1)S(1)}, bf16[8,1024]{1,0:T(8,128)(2,1)S(1)}, u32[]{:S(2)}, u32[]{:S(2)}) collective-permute-start(bf16[8,1024]{1,0:T(8,128)(2,1)S(1)} %get-tuple-element.35), channel_id=1, source_target_pairs={{0,2},{1,3},{2,0},{3,1},{4,6},{5,7},{6,4},{7,5},{8,10},{9,11},{10,... | collective-permute-start | bytes 49160 | tf_op jit(solution)/shard_map/ppermute | solution.py:194
  49.4 7.7 %collective-permute-start.20 = (bf16[8,1024]{1,0:T(8,128)(2,1)S(1)}, bf16[8,1024]{1,0:T(8,128)(2,1)S(1)}, u32[]{:S(2)}, u32[]{:S(2)}) collective-permute-start(bf16[8,1024]{1,0:T(8,128)(2,1)S(1)} %get-tuple-element.36), channel_id=1, source_target_pairs={{0,3},{1,2},{2,1},{3,0},{4,7},{5,6},{6,5},{7,4},{8,11},{9,10},{10,... | collective-permute-start | bytes 49160 | tf_op jit(solution)/shard_map/ppermute | solution.py:194
  50.3 6.9 %collective-permute-start.21 = (bf16[8,1024]{1,0:T(8,128)(2,1)S(1)}, bf16[8,1024]{1,0:T(8,128)(2,1)S(1)}, u32[]{:S(2)}, u32[]{:S(2)}) collective-permute-start(bf16[8,1024]{1,0:T(8,128)(2,1)S(1)} %get-tuple-element.37), channel_id=1, source_target_pairs={{0,4},{1,5},{2,6},{3,7},{4,0},{5,1},{6,2},{7,3},{8,12},{9,13},{10,... | collective-permute-start | bytes 49160 | tf_op jit(solution)/shard_map/ppermute | solution.py:194
  52.1 5.0 %collective-permute-start.22 = (bf16[8,1024]{1,0:T(8,128)(2,1)S(1)}, bf16[8,1024]{1,0:T(8,128)(2,1)S(1)}, u32[]{:S(2)}, u32[]{:S(2)}) collective-permute-start(bf16[8,1024]{1,0:T(8,128)(2,1)S(1)} %get-tuple-element.38), channel_id=1, source_target_pairs={{0,5},{1,4},{2,7},{3,6},{4,1},{5,0},{6,3},{7,2},{8,13},{9,12},{10,... | collective-permute-start | bytes 49160 | tf_op jit(solution)/shard_map/ppermute | solution.py:194
  53.2 5.5 %collective-permute-start.23 = (bf16[8,1024]{1,0:T(8,128)(2,1)S(1)}, bf16[8,1024]{1,0:T(8,128)(2,1)S(1)}, u32[]{:S(2)}, u32[]{:S(2)}) collective-permute-start(bf16[8,1024]{1,0:T(8,128)(2,1)S(1)} %get-tuple-element.39), channel_id=1, source_target_pairs={{0,6},{1,7},{2,4},{3,5},{4,2},{5,3},{6,0},{7,1},{8,14},{9,15},{10,... | collective-permute-start | bytes 49160 | tf_op jit(solution)/shard_map/ppermute | solution.py:194
  54.9 5.1 %collective-permute-start.24 = (bf16[8,1024]{1,0:T(8,128)(2,1)S(1)}, bf16[8,1024]{1,0:T(8,128)(2,1)S(1)}, u32[]{:S(2)}, u32[]{:S(2)}) collective-permute-start(bf16[8,1024]{1,0:T(8,128)(2,1)S(1)} %get-tuple-element.40), channel_id=1, source_target_pairs={{0,7},{1,6},{2,5},{3,4},{4,3},{5,2},{6,1},{7,0},{8,15},{9,14},{10,... | collective-permute-start | bytes 49160 | tf_op jit(solution)/shard_map/ppermute | solution.py:194
  61.7 5.8 %collective-permute-start.30 = (bf16[8,2048]{1,0:T(8,128)(2,1)S(1)}, bf16[8,2048]{1,0:T(8,128)(2,1)S(1)}, u32[]{:S(2)}, u32[]{:S(2)}) collective-permute-start(bf16[8,2048]{1,0:T(8,128)(2,1)S(1)} %get-tuple-element.42.refs_0_), channel_id=1, source_target_pairs={{0,6},{1,7},{2,4},{3,5},{4,2},{5,3},{6,0},{7,1},{8,14},{9,15},{10,... | collective-permute-start | bytes 98312 | tf_op jit(solution)/shard_map/ppermute | solution.py:194
  63.9 4.8 %collective-permute-start.28 = (bf16[8,2048]{1,0:T(8,128)(2,1)S(1)}, bf16[8,2048]{1,0:T(8,128)(2,1)S(1)}, u32[]{:S(2)}, u32[]{:S(2)}) collective-permute-start(bf16[8,2048]{1,0:T(8,128)(2,1)S(1)} %get-tuple-element.42.refs_0_), channel_id=1, source_target_pairs={{0,4},{1,5},{2,6},{3,7},{4,0},{5,1},{6,2},{7,3},{8,12},{9,13},{10,... | collective-permute-start | bytes 98312 | tf_op jit(solution)/shard_map/ppermute | solution.py:194
  63.9 4.8 %collective-permute-start.26 = (bf16[8,2048]{1,0:T(8,128)(2,1)S(1)}, bf16[8,2048]{1,0:T(8,128)(2,1)S(1)}, u32[]{:S(2)}, u32[]{:S(2)}) collective-permute-start(bf16[8,2048]{1,0:T(8,128)(2,1)S(1)} %get-tuple-element.42.refs_0_), channel_id=1, source_target_pairs={{0,2},{1,3},{2,0},{3,1},{4,6},{5,7},{6,4},{7,5},{8,10},{9,11},{10,... | collective-permute-start | bytes 98312 | tf_op jit(solution)/shard_map/ppermute | solution.py:194
  70.4 6.1 %collective-permute-start.37 = (bf16[64,256]{1,0:T(8,128)(2,1)S(1)}, bf16[64,256]{1,0:T(8,128)(2,1)S(1)}, u32[]{:S(2)}, u32[]{:S(2)}) collective-permute-start(bf16[64,256]{1,0:T(8,128)(2,1)S(1)} %out.1.refs_0_.base_ref), channel_id=1, source_target_pairs={{0,6},{1,7},{2,4},{3,5},{4,2},{5,3},{6,0},{7,1},{8,14},{9,15},{10,... | collective-permute-start | bytes 98312 | tf_op jit(solution)/shard_map/ppermute | solution.py:194
  72.3 5.2 %collective-permute-start.35 = (bf16[64,256]{1,0:T(8,128)(2,1)S(1)}, bf16[64,256]{1,0:T(8,128)(2,1)S(1)}, u32[]{:S(2)}, u32[]{:S(2)}) collective-permute-start(bf16[64,256]{1,0:T(8,128)(2,1)S(1)} %out.1.refs_0_.base_ref), channel_id=1, source_target_pairs={{0,4},{1,5},{2,6},{3,7},{4,0},{5,1},{6,2},{7,3},{8,12},{9,13},{10,... | collective-permute-start | bytes 98312 | tf_op jit(solution)/shard_map/ppermute | solution.py:194
  93.0 5.8 %collective-permute-start.40 = (bf16[64,256]{1,0:T(8,128)(2,1)S(1)}, bf16[64,256]{1,0:T(8,128)(2,1)S(1)}, u32[]{:S(2)}, u32[]{:S(2)}) collective-permute-start(bf16[64,256]{1,0:T(8,128)(2,1)S(1)} %get-tuple-element.46), channel_id=1, source_target_pairs={{0,2},{1,3},{2,0},{3,1},{4,6},{5,7},{6,4},{7,5},{8,10},{9,11},{10,... | collective-permute-start | bytes 98312 | tf_op jit(solution)/shard_map/ppermute | solution.py:194
  94.2 5.3 %collective-permute-start.41 = (bf16[64,256]{1,0:T(8,128)(2,1)S(1)}, bf16[64,256]{1,0:T(8,128)(2,1)S(1)}, u32[]{:S(2)}, u32[]{:S(2)}) collective-permute-start(bf16[64,256]{1,0:T(8,128)(2,1)S(1)} %get-tuple-element.47), channel_id=1, source_target_pairs={{0,4},{1,5},{2,6},{3,7},{4,0},{5,1},{6,2},{7,3},{8,12},{9,13},{10,... | collective-permute-start | bytes 98312 | tf_op jit(solution)/shard_map/ppermute | solution.py:194
  95.5 5.7 %collective-permute-start.42 = (bf16[64,256]{1,0:T(8,128)(2,1)S(1)}, bf16[64,256]{1,0:T(8,128)(2,1)S(1)}, u32[]{:S(2)}, u32[]{:S(2)}) collective-permute-start(bf16[64,256]{1,0:T(8,128)(2,1)S(1)} %get-tuple-element.48), channel_id=1, source_target_pairs={{0,6},{1,7},{2,4},{3,5},{4,2},{5,3},{6,0},{7,1},{8,14},{9,15},{10,... | collective-permute-start | bytes 98312 | tf_op jit(solution)/shard_map/ppermute | solution.py:194
  (35 other events, 259.5 us)

commit v2 on v1

--- a/solution.py
+++ b/solution.py
@@ -7,6 +7,7 @@
 from jax.experimental import pallas as pl
 from jax.experimental.pallas import tpu as pltpu
 from jax.sharding import PartitionSpec as P
+
 
 HEADS = 16
 HEAD = 128
@@ -166,12 +167,12 @@
 
 
 VMEM_SPEC = pl.BlockSpec(memory_space=pltpu.VMEM)
-HBM_SPEC = pl.BlockSpec(memory_space=pl.ANY)
+HBM_SPEC = pl.BlockSpec(memory_space=pltpu.HBM)
 GROUP = ("kv", "tp")
 F32, BF16 = jnp.float32, jnp.bfloat16
 
 
-def call(body, out_shapes, args, in_specs=None, scratch=(), limit=16 << 20, out_specs=None, name=None):
+def call(body, out_shapes, args, in_specs=None, scratch=(), limit=5 << 20, out_specs=None):
     single = not isinstance(out_shapes, (list, tuple))
     shapes = [out_shapes] if single else list(out_shapes)
     outs = pl.pallas_call(
@@ -181,7 +182,6 @@
         out_specs=out_specs or [VMEM_SPEC] * len(shapes),
         scratch_shapes=list(scratch),
         compiler_params=pltpu.CompilerParams(vmem_limit_bytes=limit),
-        name=name,
     )(*args)
     return outs[0] if single else outs
 
@@ -194,12 +194,47 @@
     return lax.ppermute(value, GROUP, [(i, i ^ mask) for i in range(count)])
 
 
-def gather_blocks(own, count):
-    near = [own] + [swap(own, mask, count) for mask in range(2, count, 2)]
+def far_swaps(sends, count):
+    received = []
+    for step, send in enumerate(sends):
+        received.append(swap(send, 2 * (step + 1), count))
+    return received
+
+
+def pair_up(near, count):
     blocks = []
     for block in near:
         blocks += [block, swap(block, 1, count)]
     return blocks
+
+
+def gather_blocks(own, count):
+    near = [own] + far_swaps([own] * (count // 2 - 1), count)
+    return pair_up(near, count)
+
+
+def entry_kernel(tokens_hbm, gate_hbm, up_hbm, down_hbm, tokens_ref, sem):
+    copy = pltpu.make_async_copy(tokens_hbm, tokens_ref, sem)
+    copy.start()
+    copy.wait()
+
+
+def enter(tokens, *weights):
+    arrays = [pltpu.with_memory_space_constraint(a, pltpu.HBM) for a in (tokens, *weights)]
+    return call(
+        entry_kernel,
+        pltpu.VMEM(tokens.shape, tokens.dtype),
+        arrays,
+        in_specs=[HBM_SPEC] * len(arrays),
+        scratch=[pltpu.SemaphoreType.DMA],
+        limit=1 << 20,
+    )
+
+
+def core_span(units):
+    tiles = units // 128
+    span = -(-tiles // 2) * 128
+    return span, units - span
 
 
 def assemble(blocks, index, gain_ref, scaled_ref):
@@ -208,8 +243,8 @@
     for mask, block in enumerate(blocks):
         values = block[...].astype(F32)
         owner = index ^ mask
-        gain = gain_ref[pl.ds(owner, 1), :]
         column = pl.multiple_of(owner * width, width)
+        gain = gain_ref[:, pl.ds(column, width)]
         scaled_ref[:, pl.ds(column, width)] = (values * gain).astype(BF16)
         part = values * values
         squares = part if squares is None else squares + part
@@ -220,52 +255,28 @@
 
 def ffn_kernel(count, span, skip, *refs):
     blocks = refs[:count]
-    gain_ref, gate_hbm, up_hbm, down_hbm = refs[count : count + 4]
-    own_ref, cross_ref = refs[count + 4 : count + 6]
-    scaled, gate_buf, up_buf, down_buf, gate_sem, up_sem, down_sem = refs[count + 6 :]
+    gain_ref, gate_ref, up_ref, down_ref = refs[count : count + 4]
+    own_ref, cross_ref, scaled, hidden_ref = refs[count + 4 :]
     index = my_index()
     core = lax.axis_index("tp")
     start = pl.multiple_of(core * skip, 128)
     width = blocks[0].shape[1]
-    channels = width * count
-    pieces = gate_buf.shape[0]
-    depth = channels // pieces
-    copies = []
-    for piece in range(pieces):
-        rows = pl.ds(piece * depth, depth)
-        for hbm, buf, sem in ((gate_hbm, gate_buf, gate_sem), (up_hbm, up_buf, up_sem)):
-            copy = pltpu.make_async_copy(
-                hbm.at[rows, pl.ds(start, span)], buf.at[piece], sem.at[piece]
-            )
-            copy.start()
-            copies.append(copy)
-    order = list(range(1, count, 2)) + list(range(0, count, 2))
-    down_copies = {}
-    for mask in order:
+    row_scale = assemble(blocks, index, gain_ref, scaled)
+    lhs = scaled[...]
+    repeated = core * (lax.axis_size("tp") * span - down_ref.shape[0])
+    for first in range(0, span, 256):
+        size = min(256, span - first)
+        columns = pl.ds(pl.multiple_of(start + first, 128), size)
+        gate_act = jnp.dot(lhs, gate_ref[:, columns], preferred_element_type=F32) * row_scale
+        up_act = jnp.dot(lhs, up_ref[:, columns], preferred_element_type=F32) * row_scale
+        hidden = gate_act * jax.nn.sigmoid(gate_act) * up_act
+        unit = lax.broadcasted_iota(jnp.int32, hidden.shape, 1) + first
+        hidden_ref[:, first : first + size] = jnp.where(unit >= repeated, hidden, 0.0).astype(BF16)
+    hidden = hidden_ref[...]
+    for mask in list(range(1, count, 2)) + list(range(0, count, 2)):
         column = pl.multiple_of((index ^ mask) * width, width)
-        copy = pltpu.make_async_copy(
-            down_hbm.at[pl.ds(start, span), pl.ds(column, width)], down_buf.at[mask], down_sem.at[mask]
-        )
-        copy.start()
-        down_copies[mask] = copy
-    row_scale = assemble(blocks, index, gain_ref, scaled)
-    gate_acc = up_acc = None
-    for piece in range(pieces):
-        lhs = scaled[:, piece * depth : (piece + 1) * depth]
-        copies[2 * piece].wait()
-        part = jnp.dot(lhs, gate_buf[piece], preferred_element_type=F32)
-        gate_acc = part if gate_acc is None else gate_acc + part
-        copies[2 * piece + 1].wait()
-        part = jnp.dot(lhs, up_buf[piece], preferred_element_type=F32)
-        up_acc = part if up_acc is None else up_acc + part
-    gate_act = gate_acc * row_scale
-    hidden = gate_act * jax.nn.sigmoid(gate_act) * (up_acc * row_scale)
-    unit = lax.broadcasted_iota(jnp.int32, hidden.shape, 1)
-    repeated = core * (lax.axis_size("tp") * span - down_hbm.shape[0])
-    hidden = jnp.where(unit >= repeated, hidden, 0.0).astype(BF16)
-    for mask in order:
-        down_copies[mask].wait()
-        part = jnp.dot(hidden, down_buf[mask], preferred_element_type=F32)
+        weight = down_ref[pl.ds(start, span), pl.ds(column, width)]
+        part = jnp.dot(hidden, weight, preferred_element_type=F32)
         if mask % 2:
             cross_ref[mask // 2] = part.astype(BF16)
         else:
@@ -285,54 +296,32 @@
     refs[-1][...] = (base_ref[...].astype(F32) + 0.5 * total).astype(BF16)
 
 
-def half_step(own, count, gain, gate, up, down):
+def half_step(own, count, gain, gate, up, down, last=False):
     rows, width = own.shape
     near = count // 2
-    units = gate.shape[1]
-    tiles = units // 128
-    span = -(-tiles // 2) * 128
-    skip = units - span
+    span, skip = core_span(down.shape[0])
     blocks = gather_blocks(own, count)
-    pieces = 4
-    depth = width * count // pieces
     own_part, cross_part = call(
         functools.partial(ffn_kernel, count, span, skip),
         [pltpu.VMEM((near, rows, width), F32), pltpu.VMEM((near, rows, width), BF16)],
-        [*blocks, gain.reshape(count, width), gate, up, down],
-        in_specs=[VMEM_SPEC] * (count + 1) + [HBM_SPEC] * 3,
-        scratch=[
-            pltpu.VMEM((rows, width * count), BF16),
-            pltpu.VMEM((pieces, depth, span), BF16),
-            pltpu.VMEM((pieces, depth, span), BF16),
-            pltpu.VMEM((count, span, width), BF16),
-            pltpu.SemaphoreType.DMA((pieces,)),
-            pltpu.SemaphoreType.DMA((pieces,)),
-            pltpu.SemaphoreType.DMA((count,)),
-        ],
-        limit=24 << 20,
-        name="ffn",
+        [*blocks, gain.reshape(1, count * width), gate, up, down],
+        scratch=[pltpu.VMEM((rows, width * count), BF16), pltpu.VMEM((rows, span), BF16)],
     )
     cross_sum = swap(cross_part, 1, count)
     mine, *sends = call(
         pair_sum_kernel,
         [pltpu.VMEM((rows, width), F32)] + [pltpu.VMEM((rows, width), BF16)] * (near - 1),
         [own_part, cross_sum],
-        name="pair_sum",
-    )
-    received = [swap(send, 2 * (step + 1), count) for step, send in enumerate(sends)]
-    return call(
-        residual_kernel,
-        pltpu.VMEM((rows, width), BF16),
-        [own, mine, *received],
-        name="residual",
-    )
+    )
+    received = far_swaps(sends, count)
+    shape = jax.ShapeDtypeStruct if last else pltpu.VMEM
+    return call(residual_kernel, shape((rows, width), BF16), [own, mine, *received])
 
 
 def project_kernel(count, *refs):
     blocks = refs[:count]
     gain_ref, query_w, key_w, value_w, gating_w, write_t, forget_t = refs[count : count + 7]
-    sends = refs[count + 7 : count + 7 + count]
-    pre_ref, scaled, result, pre_scratch = refs[count + 7 + count :]
+    *sends, pre_ref, scaled, result, pre_scratch = refs[count + 7 :]
     index = my_index()
     row_scale = assemble(blocks, index, gain_ref, scaled)
     lhs = scaled[...]
@@ -345,9 +334,10 @@
     for place, weight in enumerate((write_t, forget_t)):
         part = lax.dot_general(lhs, weight[...], contract, preferred_element_type=F32)
         pre_scratch[:, place * heads : (place + 1) * heads] = part * row_scale
-    for mask, send in enumerate(sends):
-        row = pl.multiple_of((index ^ mask) * BLK, BLK)
-        send[...] = result[pl.ds(row, BLK), :].astype(BF16)
+    for step, send in enumerate(sends):
+        rows = send.shape[0]
+        row = pl.multiple_of((lax.axis_index("kv") ^ step) * rows, rows)
+        send[...] = result[pl.ds(row, rows), :].astype(BF16)
     row = pl.multiple_of(index * BLK, BLK)
     pre_ref[...] = pre_scratch[pl.ds(row, BLK), :]
 
@@ -370,8 +360,10 @@
     pre_ref, rate_ref, length_ref, state_ref = refs[count : count + 4]
     mixed_ref, update_ref, faded_ref, final_ref, ordered = refs[count + 4 :]
     index = my_index()
+    first_core = lax.axis_index("tp") == 0
     for mask, block in enumerate(blocks):
-        ordered[pl.ds(index ^ mask, 1)] = block[...].astype(F32)[None]
+        both = block[...].astype(F32)
+        ordered[pl.ds(index ^ mask, 1)] = jnp.where(first_core, both[:BLK], both[BLK:])[None]
     heads = rate_ref.shape[1]
     size = state_ref.shape[-1]
     per_block = heads // count
@@ -505,30 +497,23 @@
     rows, width = tokens.shape
     channels = gain_first.shape[0]
     heads, size = state.shape[1], state.shape[2]
+    tokens = enter(tokens, first_gate, first_up, first_down)
     after_first = half_step(tokens, count, gain_first, first_gate, first_up, first_down)
     blocks = gather_blocks(after_first, count)
+    weights = (query_weight, key_weight, value_weight, gating_weight)
     columns = 4 * width
+    near = count // 2
     *sends, pre = call(
         functools.partial(project_kernel, count),
-        [pltpu.VMEM((BLK, columns), BF16)] * count + [pltpu.VMEM((BLK, 2 * heads), F32)],
-        [
-            *blocks,
-            gain_mix.reshape(count, width),
-            query_weight,
-            key_weight,
-            value_weight,
-            gating_weight,
-            write_weight.T,
-            forget_weight.T,
-        ],
+        [pltpu.VMEM((rows // near, columns), BF16)] * near + [pltpu.VMEM((BLK, 2 * heads), F32)],
+        [*blocks, gain_mix.reshape(1, channels), *weights, write_weight.T, forget_weight.T],
         scratch=[
             pltpu.VMEM((rows, channels), BF16),
             pltpu.VMEM((rows, columns), F32),
             pltpu.VMEM((rows, 2 * heads), F32),
         ],
-        name="project",
-    )
-    owned = [sends[0]] + [swap(sends[mask], mask, count) for mask in range(1, count)]
+    )
+    owned = pair_up([sends[0]] + far_swaps(sends[1:], count), count)
     matrices = state.reshape(heads, size, size)
     mixed, update, faded, final = call(
         functools.partial(delta_kernel, count),
@@ -541,23 +526,22 @@
         [*owned, pre, forget_rate.reshape(1, heads), lengths, matrices],
         in_specs=[VMEM_SPEC] * (count + 2) + [pl.BlockSpec(memory_space=pltpu.SMEM), VMEM_SPEC],
         scratch=[pltpu.VMEM((count, BLK, columns), F32)],
-        name="delta",
     )
     head_blocks = gather_blocks(mixed, count)
     new_state = call(
         state_kernel,
         jax.ShapeDtypeStruct((heads, size, size), F32),
         [update, faded, final, matrices],
-        name="state",
     )
     after_mix = call(
         functools.partial(out_kernel, count),
         pltpu.VMEM((rows, width), BF16),
         [*head_blocks, out_weight, after_first],
         scratch=[pltpu.VMEM((rows, width), F32)],
-        name="out",
-    )
-    mixed_out = half_step(after_mix, count, gain_second, second_gate, second_up, second_down)
+    )
+    mixed_out = half_step(
+        after_mix, count, gain_second, second_gate, second_up, second_down, last=True
+    )
     return (mixed_out, new_state.reshape(state.shape))
 
 
@@ -568,9 +552,11 @@
 
 
 def per_device(mesh, *arrays):
-    tokens, lengths, gate = arrays[0], arrays[1], arrays[4]
+    lengths, gate = arrays[1], arrays[4]
     suits = fits_group(mesh) and lengths.shape[0] == 1 and gate.shape[1] % 128 == 0
-    return (group_device if suits else general_device)(*arrays)
+    if not suits:
+        return general_device(*arrays)
+    return group_device(*arrays)
 
 
 def solution(mesh):
@@ -598,5 +584,9 @@
     )
     out_specs = (P("dp", ("kv", "tp")), P(("dp", "kv", "tp"), None, None, None))
     return jax.shard_map(
-        functools.partial(per_device, mesh), mesh=mesh, in_specs=in_specs, out_specs=out_specs, check_vma=False
-    )
+        functools.partial(per_device, mesh),
+        mesh=mesh,
+        in_specs=in_specs,
+        out_specs=out_specs,
+        check_vma=False,
+    )

time: 103 us -> 74.5 us (0.72)
  local copies, waits for them, and re-layouts: 23 us -> 0.1 us
  Pallas kernels: 14.1 us -> 9.74 us
  starting transfers between devices: 39 us -> 35.9 us
  waiting for transfers between devices: 24.2 us -> 27 us
    unnamed x33 -> x42, local copies, waits for them, and re-layouts: 20.9 us -> 0.1 us
    pallas_call x10 -> x11, Pallas kernels: 14.1 us -> 9.74 us  [call(): pl.pallas_call(body, out_shape=shapes, in_specs=in_specs or [VMEM_SPEC] *...]
    ppermute x43, starting transfers between devices: 39 us -> 35.9 us  [swap(): return lax.ppermute(value, GROUP, [(i, i ^ mask) for i in range(count)])]
    ppermute x43, waiting for transfers between devices: 24.2 us -> 27 us  [swap(): return lax.ppermute(value, GROUP, [(i, i ^ mask) for i in range(count)])]
    reshape x3 -> x0, local copies, waits for them, and re-layouts: 2.11 us -> none  [the longest x2 1.41 us: half_step(): gain.reshape(count, width)]
  transfers between devices with their start and end apart: 43 -> 43, of which waited for: 21 -> 25; matrix products, arithmetic and copies ran while one was open for 2% -> 0% of each run, Pallas kernels for 1% -> 2%
where the time goes in v2:
time: 74.5 us; the launch traced here: 74.4 us
  starting transfers between devices  35.9 us (48%)
  waiting for transfers between devices  27 us (36%)
  Pallas kernels  9.74 us (13%)
  between operations  1.66 us (2%)
    ppermute x43, starting transfers between devices, swap(): return lax.ppermute(value, GROUP, [(i, i ^ mask) for i in range(count)])  35.9 us
    ppermute x43, waiting for transfers between devices, swap(): return lax.ppermute(value, GROUP, [(i, i ^ mask) for i in range(count)])  27 us
    pallas_call x11, Pallas kernels, call(): pl.pallas_call(body, out_shape=shapes, in_specs=in_specs or [VMEM_SPEC] *...  9.74 us
  transfers between devices with their start and end apart: 43, of which 25 were waited for; matrix products, arithmetic and copies ran while one was open for 0% of the time, Pallas kernels for 2%

profile of v2, /device:TPU:0, one launch (start us, length us, event | category | flops | bytes accessed | tf_op | source)
XLA Modules:
  0.0 74.4 jit_solution(7032837653840329795)
XLA Ops:
  1.7 5.1 %collective-permute-start.5 = (bf16[64,256]{1,0:T(8,128)(2,1)S(1)}, bf16[64,256]{1,0:T(8,128)(2,1)S(1)}, u32[]{:S(2)}, u32[]{:S(2)}) collective-permute-start(bf16[64,256]{1,0:T(8,128)(2,1)S(1)} %shard_map.203.refs_0_.base_ref), channel_id=1, source_target_pairs={{0,6},{1,7},{2,4},{3,5},{4,2},{5,3},{6,0},{7,1},{8,14},{9,15},{10,... | collective-permute-start | bytes 98312 | tf_op jit(solution)/shard_map/ppermute | solution.py:194
  8.7 2.9 %collective-permute-done.3.refs_4_ = bf16[64,256]{1,0:T(8,128)(2,1)S(1)} collective-permute-done((bf16[64,256]{1,0:T(8,128)(2,1)S(1)}, bf16[64,256]{1,0:T(8,128)(2,1)S(1)}, u32[]{:S(2)}, u32[]{:S(2)}) %collective-permute-start.3) | collective-permute-done | bytes 32800 | tf_op jit(solution)/shard_map/ppermute | solution.py:194
  13.1 1.8 %shard_map.204 = (f32[4,64,256]{2,1,0:T(8,128)S(1)}, bf16[4,64,256]{2,1,0:T(8,128)(2,1)S(1)}) custom-call(bf16[64,256]{1,0:T(8,128)(2,1)S(1)} %shard_map.203.refs_0_.base_ref, bf16[64,256]{1,0:T(8,128)(2,1)S(1)} %collective-permute-done.refs_1_, bf16[64,256]{1,0:T(8,128)(2,1)S(1)} %collective-permute-done.1.refs_2_, ...), custom_call_target="tpu_custom_call" | custom-call | tf_op jit(solution)/shard_map/pallas_call | solution.py:178
  16.5 1.9 %collective-permute-start.9 = (bf16[64,256]{1,0:T(8,128)(2,1)S(1)}, bf16[64,256]{1,0:T(8,128)(2,1)S(1)}, u32[]{:S(2)}, u32[]{:S(2)}) collective-permute-start(bf16[64,256]{1,0:T(8,128)(2,1)S(1)} %get-tuple-element.27), channel_id=1, source_target_pairs={{0,4},{1,5},{2,6},{3,7},{4,0},{5,1},{6,2},{7,3},{8,12},{9,13},{10,... | collective-permute-start | bytes 98312 | tf_op jit(solution)/shard_map/ppermute | solution.py:194
  18.4 2.5 %collective-permute-start.10 = (bf16[64,256]{1,0:T(8,128)(2,1)S(1)}, bf16[64,256]{1,0:T(8,128)(2,1)S(1)}, u32[]{:S(2)}, u32[]{:S(2)}) collective-permute-start(bf16[64,256]{1,0:T(8,128)(2,1)S(1)} %get-tuple-element.28), channel_id=1, source_target_pairs={{0,6},{1,7},{2,4},{3,5},{4,2},{5,3},{6,0},{7,1},{8,14},{9,15},{10,... | collective-permute-start | bytes 98312 | tf_op jit(solution)/shard_map/ppermute | solution.py:194
  21.3 2.8 %collective-permute-done.10.refs_2_ = bf16[64,256]{1,0:T(8,128)(2,1)S(1)} collective-permute-done((bf16[64,256]{1,0:T(8,128)(2,1)S(1)}, bf16[64,256]{1,0:T(8,128)(2,1)S(1)}, u32[]{:S(2)}, u32[]{:S(2)}) %collective-permute-start.10) | collective-permute-done | bytes 32800 | tf_op jit(solution)/shard_map/ppermute | solution.py:194
  24.1 2.5 %collective-permute-start.16 = (bf16[64,256]{1,0:T(8,128)(2,1)S(1)}, bf16[64,256]{1,0:T(8,128)(2,1)S(1)}, u32[]{:S(2)}, u32[]{:S(2)}) collective-permute-start(bf16[64,256]{1,0:T(8,128)(2,1)S(1)} %shard_map.206.refs_0_.refs_9_), channel_id=1, source_target_pairs={{0,6},{1,7},{2,4},{3,5},{4,2},{5,3},{6,0},{7,1},{8,14},{9,15},{10,... | collective-permute-start | bytes 98312 | tf_op jit(solution)/shard_map/ppermute | solution.py:194
  26.6 1.9 %collective-permute-start.12 = (bf16[64,256]{1,0:T(8,128)(2,1)S(1)}, bf16[64,256]{1,0:T(8,128)(2,1)S(1)}, u32[]{:S(2)}, u32[]{:S(2)}) collective-permute-start(bf16[64,256]{1,0:T(8,128)(2,1)S(1)} %shard_map.206.refs_0_.refs_9_), channel_id=1, source_target_pairs={{0,2},{1,3},{2,0},{3,1},{4,6},{5,7},{6,4},{7,5},{8,10},{9,11},{10,... | collective-permute-start | bytes 98312 | tf_op jit(solution)/shard_map/ppermute | solution.py:194
  28.6 1.5 %collective-permute-done.16.refs_6_ = bf16[64,256]{1,0:T(8,128)(2,1)S(1)} collective-permute-done((bf16[64,256]{1,0:T(8,128)(2,1)S(1)}, bf16[64,256]{1,0:T(8,128)(2,1)S(1)}, u32[]{:S(2)}, u32[]{:S(2)}) %collective-permute-start.16) | collective-permute-done | bytes 32800 | tf_op jit(solution)/shard_map/ppermute | solution.py:194
  30.1 1.4 %collective-permute-done.14.refs_4_ = bf16[64,256]{1,0:T(8,128)(2,1)S(1)} collective-permute-done((bf16[64,256]{1,0:T(8,128)(2,1)S(1)}, bf16[64,256]{1,0:T(8,128)(2,1)S(1)}, u32[]{:S(2)}, u32[]{:S(2)}) %collective-permute-start.14) | collective-permute-done | bytes 32800 | tf_op jit(solution)/shard_map/ppermute | solution.py:194
  34.9 1.4 %collective-permute-start.21 = (bf16[16,1024]{1,0:T(8,128)(2,1)S(1)}, bf16[16,1024]{1,0:T(8,128)(2,1)S(1)}, u32[]{:S(2)}, u32[]{:S(2)}) collective-permute-start(bf16[16,1024]{1,0:T(8,128)(2,1)S(1)} %get-tuple-element.31), channel_id=1, source_target_pairs={{0,4},{1,5},{2,6},{3,7},{4,0},{5,1},{6,2},{7,3},{8,12},{9,13},{10,... | collective-permute-start | bytes 98312 | tf_op jit(solution)/shard_map/ppermute | solution.py:194
  36.3 2.1 %collective-permute-start.23 = (bf16[16,1024]{1,0:T(8,128)(2,1)S(1)}, bf16[16,1024]{1,0:T(8,128)(2,1)S(1)}, u32[]{:S(2)}, u32[]{:S(2)}) collective-permute-start(bf16[16,1024]{1,0:T(8,128)(2,1)S(1)} %get-tuple-element.32), channel_id=1, source_target_pairs={{0,6},{1,7},{2,4},{3,5},{4,2},{5,3},{6,0},{7,1},{8,14},{9,15},{10,... | collective-permute-start | bytes 98312 | tf_op jit(solution)/shard_map/ppermute | solution.py:194
  39.0 1.6 %collective-permute-done.21.refs_4_ = bf16[16,1024]{1,0:T(8,128)(2,1)S(1)} collective-permute-done((bf16[16,1024]{1,0:T(8,128)(2,1)S(1)}, bf16[16,1024]{1,0:T(8,128)(2,1)S(1)}, u32[]{:S(2)}, u32[]{:S(2)}) %collective-permute-start.21) | collective-permute-done | bytes 32800 | tf_op jit(solution)/shard_map/ppermute | solution.py:194
  40.5 1.5 %collective-permute-done.23.refs_6_ = bf16[16,1024]{1,0:T(8,128)(2,1)S(1)} collective-permute-done((bf16[16,1024]{1,0:T(8,128)(2,1)S(1)}, bf16[16,1024]{1,0:T(8,128)(2,1)S(1)}, u32[]{:S(2)}, u32[]{:S(2)}) %collective-permute-start.23) | collective-permute-done | bytes 32800 | tf_op jit(solution)/shard_map/ppermute | solution.py:194
  43.3 1.7 %shard_map.208 = (bf16[8,2048]{1,0:T(8,128)(2,1)S(1)}, f32[128,128]{1,0:T(8,128)S(1)}, f32[128,128]{1,0:T(8,128)S(1)}, f32[128,128]{1,0:T(8,128)S(1)}) custom-call(bf16[16,1024]{1,0:T(8,128)(2,1)S(1)} %get-tuple-element.29.refs_0_, bf16[16,1024]{1,0:T(8,128)(2,1)S(1)} %collective-permute-done.18.refs_1_, ...), custom_call_target="tpu_custom_call" | custom-call | tf_op jit(solution)/shard_map/pallas_call | solution.py:178
  45.0 2.2 %collective-permute-start.30 = (bf16[8,2048]{1,0:T(8,128)(2,1)S(1)}, bf16[8,2048]{1,0:T(8,128)(2,1)S(1)}, u32[]{:S(2)}, u32[]{:S(2)}) collective-permute-start(bf16[8,2048]{1,0:T(8,128)(2,1)S(1)} %get-tuple-element.34.refs_0_), channel_id=1, source_target_pairs={{0,6},{1,7},{2,4},{3,5},{4,2},{5,3},{6,0},{7,1},{8,14},{9,15},{10,... | collective-permute-start | bytes 98312 | tf_op jit(solution)/shard_map/ppermute | solution.py:194
  47.2 2.3 %collective-permute-start.26 = (bf16[8,2048]{1,0:T(8,128)(2,1)S(1)}, bf16[8,2048]{1,0:T(8,128)(2,1)S(1)}, u32[]{:S(2)}, u32[]{:S(2)}) collective-permute-start(bf16[8,2048]{1,0:T(8,128)(2,1)S(1)} %get-tuple-element.34.refs_0_), channel_id=1, source_target_pairs={{0,2},{1,3},{2,0},{3,1},{4,6},{5,7},{6,4},{7,5},{8,10},{9,11},{10,... | collective-permute-start | bytes 98312 | tf_op jit(solution)/shard_map/ppermute | solution.py:194
  53.7 2.0 %collective-permute-start.37 = (bf16[64,256]{1,0:T(8,128)(2,1)S(1)}, bf16[64,256]{1,0:T(8,128)(2,1)S(1)}, u32[]{:S(2)}, u32[]{:S(2)}) collective-permute-start(bf16[64,256]{1,0:T(8,128)(2,1)S(1)} %shard_map.209.refs_0_.base_ref), channel_id=1, source_target_pairs={{0,6},{1,7},{2,4},{3,5},{4,2},{5,3},{6,0},{7,1},{8,14},{9,15},{10,... | collective-permute-start | bytes 98312 | tf_op jit(solution)/shard_map/ppermute | solution.py:194
  56.4 1.7 %collective-permute-start.33 = (bf16[64,256]{1,0:T(8,128)(2,1)S(1)}, bf16[64,256]{1,0:T(8,128)(2,1)S(1)}, u32[]{:S(2)}, u32[]{:S(2)}) collective-permute-start(bf16[64,256]{1,0:T(8,128)(2,1)S(1)} %shard_map.209.refs_0_.base_ref), channel_id=1, source_target_pairs={{0,2},{1,3},{2,0},{3,1},{4,6},{5,7},{6,4},{7,5},{8,10},{9,11},{10,... | collective-permute-start | bytes 98312 | tf_op jit(solution)/shard_map/ppermute | solution.py:194
  58.1 1.6 %collective-permute-done.37.refs_6_ = bf16[64,256]{1,0:T(8,128)(2,1)S(1)} collective-permute-done((bf16[64,256]{1,0:T(8,128)(2,1)S(1)}, bf16[64,256]{1,0:T(8,128)(2,1)S(1)}, u32[]{:S(2)}, u32[]{:S(2)}) %collective-permute-start.37) | collective-permute-done | bytes 32800 | tf_op jit(solution)/shard_map/ppermute | solution.py:194
  62.2 1.8 %shard_map.210 = (f32[4,64,256]{2,1,0:T(8,128)S(1)}, bf16[4,64,256]{2,1,0:T(8,128)(2,1)S(1)}) custom-call(bf16[64,256]{1,0:T(8,128)(2,1)S(1)} %shard_map.209.refs_0_.base_ref, bf16[64,256]{1,0:T(8,128)(2,1)S(1)} %collective-permute-done.32.refs_1_, bf16[64,256]{1,0:T(8,128)(2,1)S(1)} %collective-permute-done.33.refs_2_, ...), custom_call_target="tpu_custom_call" | custom-call | tf_op jit(solution)/shard_map/pallas_call | solution.py:178
  66.7 1.4 %collective-permute-start.41 = (bf16[64,256]{1,0:T(8,128)(2,1)S(1)}, bf16[64,256]{1,0:T(8,128)(2,1)S(1)}, u32[]{:S(2)}, u32[]{:S(2)}) collective-permute-start(bf16[64,256]{1,0:T(8,128)(2,1)S(1)} %get-tuple-element.39), channel_id=1, source_target_pairs={{0,4},{1,5},{2,6},{3,7},{4,0},{5,1},{6,2},{7,3},{8,12},{9,13},{10,... | collective-permute-start | bytes 98312 | tf_op jit(solution)/shard_map/ppermute | solution.py:194
  68.0 1.9 %collective-permute-start.42 = (bf16[64,256]{1,0:T(8,128)(2,1)S(1)}, bf16[64,256]{1,0:T(8,128)(2,1)S(1)}, u32[]{:S(2)}, u32[]{:S(2)}) collective-permute-start(bf16[64,256]{1,0:T(8,128)(2,1)S(1)} %get-tuple-element.40), channel_id=1, source_target_pairs={{0,6},{1,7},{2,4},{3,5},{4,2},{5,3},{6,0},{7,1},{8,14},{9,15},{10,... | collective-permute-start | bytes 98312 | tf_op jit(solution)/shard_map/ppermute | solution.py:194
  72.0 1.8 %collective-permute-done.42.refs_2_ = bf16[64,256]{1,0:T(8,128)(2,1)S(1)} collective-permute-done((bf16[64,256]{1,0:T(8,128)(2,1)S(1)}, bf16[64,256]{1,0:T(8,128)(2,1)S(1)}, u32[]{:S(2)}, u32[]{:S(2)}) %collective-permute-start.42) | collective-permute-done | bytes 32800 | tf_op jit(solution)/shard_map/ppermute | solution.py:194
  (118 shorter events, 23.5 us)
Async XLA Ops:
  1.7 7.0 %collective-permute-start.5 = (bf16[64,256]{1,0:T(8,128)(2,1)S(1)}, bf16[64,256]{1,0:T(8,128)(2,1)S(1)}, u32[]{:S(2)}, u32[]{:S(2)}) collective-permute-start(bf16[64,256]{1,0:T(8,128)(2,1)S(1)} %shard_map.203.refs_0_.base_ref), channel_id=1, source_target_pairs={{0,6},{1,7},{2,4},{3,5},{4,2},{5,3},{6,0},{7,1},{8,14},{9,15},{10,... | collective-permute-start | bytes 98312 | tf_op jit(solution)/shard_map/ppermute | solution.py:194
  6.8 4.8 %collective-permute-start.3 = (bf16[64,256]{1,0:T(8,128)(2,1)S(1)}, bf16[64,256]{1,0:T(8,128)(2,1)S(1)}, u32[]{:S(2)}, u32[]{:S(2)}) collective-permute-start(bf16[64,256]{1,0:T(8,128)(2,1)S(1)} %shard_map.203.refs_0_.base_ref), channel_id=1, source_target_pairs={{0,4},{1,5},{2,6},{3,7},{4,0},{5,1},{6,2},{7,3},{8,12},{9,13},{10,... | collective-permute-start | bytes 98312 | tf_op jit(solution)/shard_map/ppermute | solution.py:194
  6.8 4.8 %collective-permute-start.1 = (bf16[64,256]{1,0:T(8,128)(2,1)S(1)}, bf16[64,256]{1,0:T(8,128)(2,1)S(1)}, u32[]{:S(2)}, u32[]{:S(2)}) collective-permute-start(bf16[64,256]{1,0:T(8,128)(2,1)S(1)} %shard_map.203.refs_0_.base_ref), channel_id=1, source_target_pairs={{0,2},{1,3},{2,0},{3,1},{4,6},{5,7},{6,4},{7,5},{8,10},{9,11},{10,... | collective-permute-start | bytes 98312 | tf_op jit(solution)/shard_map/ppermute | solution.py:194
  7.5 4.7 %collective-permute-start = (bf16[64,256]{1,0:T(8,128)(2,1)S(1)}, bf16[64,256]{1,0:T(8,128)(2,1)S(1)}, u32[]{:S(2)}, u32[]{:S(2)}) collective-permute-start(bf16[64,256]{1,0:T(8,128)(2,1)S(1)} %shard_map.203.refs_0_.base_ref), channel_id=1, source_target_pairs={{0,1},{1,0},{2,3},{3,2},{4,5},{5,4},{6,7},{7,6},{8,9},{9,8},{10,11... | collective-permute-start | bytes 98312 | tf_op jit(solution)/shard_map/ppermute | solution.py:194
  16.4 4.5 %collective-permute-start.8 = (bf16[64,256]{1,0:T(8,128)(2,1)S(1)}, bf16[64,256]{1,0:T(8,128)(2,1)S(1)}, u32[]{:S(2)}, u32[]{:S(2)}) collective-permute-start(bf16[64,256]{1,0:T(8,128)(2,1)S(1)} %get-tuple-element.26), channel_id=1, source_target_pairs={{0,2},{1,3},{2,0},{3,1},{4,6},{5,7},{6,4},{7,5},{8,10},{9,11},{10,... | collective-permute-start | bytes 98312 | tf_op jit(solution)/shard_map/ppermute | solution.py:194
  16.5 4.9 %collective-permute-start.9 = (bf16[64,256]{1,0:T(8,128)(2,1)S(1)}, bf16[64,256]{1,0:T(8,128)(2,1)S(1)}, u32[]{:S(2)}, u32[]{:S(2)}) collective-permute-start(bf16[64,256]{1,0:T(8,128)(2,1)S(1)} %get-tuple-element.27), channel_id=1, source_target_pairs={{0,4},{1,5},{2,6},{3,7},{4,0},{5,1},{6,2},{7,3},{8,12},{9,13},{10,... | collective-permute-start | bytes 98312 | tf_op jit(solution)/shard_map/ppermute | solution.py:194
  18.4 5.7 %collective-permute-start.10 = (bf16[64,256]{1,0:T(8,128)(2,1)S(1)}, bf16[64,256]{1,0:T(8,128)(2,1)S(1)}, u32[]{:S(2)}, u32[]{:S(2)}) collective-permute-start(bf16[64,256]{1,0:T(8,128)(2,1)S(1)} %get-tuple-element.28), channel_id=1, source_target_pairs={{0,6},{1,7},{2,4},{3,5},{4,2},{5,3},{6,0},{7,1},{8,14},{9,15},{10,... | collective-permute-start | bytes 98312 | tf_op jit(solution)/shard_map/ppermute | solution.py:194
  24.1 6.0 %collective-permute-start.16 = (bf16[64,256]{1,0:T(8,128)(2,1)S(1)}, bf16[64,256]{1,0:T(8,128)(2,1)S(1)}, u32[]{:S(2)}, u32[]{:S(2)}) collective-permute-start(bf16[64,256]{1,0:T(8,128)(2,1)S(1)} %shard_map.206.refs_0_.refs_9_), channel_id=1, source_target_pairs={{0,6},{1,7},{2,4},{3,5},{4,2},{5,3},{6,0},{7,1},{8,14},{9,15},{10,... | collective-permute-start | bytes 98312 | tf_op jit(solution)/shard_map/ppermute | solution.py:194
  26.6 4.8 %collective-permute-start.14 = (bf16[64,256]{1,0:T(8,128)(2,1)S(1)}, bf16[64,256]{1,0:T(8,128)(2,1)S(1)}, u32[]{:S(2)}, u32[]{:S(2)}) collective-permute-start(bf16[64,256]{1,0:T(8,128)(2,1)S(1)} %shard_map.206.refs_0_.refs_9_), channel_id=1, source_target_pairs={{0,4},{1,5},{2,6},{3,7},{4,0},{5,1},{6,2},{7,3},{8,12},{9,13},{10,... | collective-permute-start | bytes 98312 | tf_op jit(solution)/shard_map/ppermute | solution.py:194
  26.6 4.8 %collective-permute-start.12 = (bf16[64,256]{1,0:T(8,128)(2,1)S(1)}, bf16[64,256]{1,0:T(8,128)(2,1)S(1)}, u32[]{:S(2)}, u32[]{:S(2)}) collective-permute-start(bf16[64,256]{1,0:T(8,128)(2,1)S(1)} %shard_map.206.refs_0_.refs_9_), channel_id=1, source_target_pairs={{0,2},{1,3},{2,0},{3,1},{4,6},{5,7},{6,4},{7,5},{8,10},{9,11},{10,... | collective-permute-start | bytes 98312 | tf_op jit(solution)/shard_map/ppermute | solution.py:194
  34.0 4.5 %collective-permute-start.19 = (bf16[16,1024]{1,0:T(8,128)(2,1)S(1)}, bf16[16,1024]{1,0:T(8,128)(2,1)S(1)}, u32[]{:S(2)}, u32[]{:S(2)}) collective-permute-start(bf16[16,1024]{1,0:T(8,128)(2,1)S(1)} %get-tuple-element.30), channel_id=1, source_target_pairs={{0,2},{1,3},{2,0},{3,1},{4,6},{5,7},{6,4},{7,5},{8,10},{9,11},{10,... | collective-permute-start | bytes 98312 | tf_op jit(solution)/shard_map/ppermute | solution.py:194
  34.9 5.6 %collective-permute-start.21 = (bf16[16,1024]{1,0:T(8,128)(2,1)S(1)}, bf16[16,1024]{1,0:T(8,128)(2,1)S(1)}, u32[]{:S(2)}, u32[]{:S(2)}) collective-permute-start(bf16[16,1024]{1,0:T(8,128)(2,1)S(1)} %get-tuple-element.31), channel_id=1, source_target_pairs={{0,4},{1,5},{2,6},{3,7},{4,0},{5,1},{6,2},{7,3},{8,12},{9,13},{10,... | collective-permute-start | bytes 98312 | tf_op jit(solution)/shard_map/ppermute | solution.py:194
  36.3 5.7 %collective-permute-start.23 = (bf16[16,1024]{1,0:T(8,128)(2,1)S(1)}, bf16[16,1024]{1,0:T(8,128)(2,1)S(1)}, u32[]{:S(2)}, u32[]{:S(2)}) collective-permute-start(bf16[16,1024]{1,0:T(8,128)(2,1)S(1)} %get-tuple-element.32), channel_id=1, source_target_pairs={{0,6},{1,7},{2,4},{3,5},{4,2},{5,3},{6,0},{7,1},{8,14},{9,15},{10,... | collective-permute-start | bytes 98312 | tf_op jit(solution)/shard_map/ppermute | solution.py:194
  38.4 4.3 %collective-permute-start.18 = (bf16[16,1024]{1,0:T(8,128)(2,1)S(1)}, bf16[16,1024]{1,0:T(8,128)(2,1)S(1)}, u32[]{:S(2)}, u32[]{:S(2)}) collective-permute-start(bf16[16,1024]{1,0:T(8,128)(2,1)S(1)} %get-tuple-element.29.refs_0_), channel_id=1, source_target_pairs={{0,1},{1,0},{2,3},{3,2},{4,5},{5,4},{6,7},{7,6},{8,9},{9,8},{10,11... | collective-permute-start | bytes 98312 | tf_op jit(solution)/shard_map/ppermute | solution.py:194
  38.4 4.3 %collective-permute-start.20 = (bf16[16,1024]{1,0:T(8,128)(2,1)S(1)}, bf16[16,1024]{1,0:T(8,128)(2,1)S(1)}, u32[]{:S(2)}, u32[]{:S(2)}) collective-permute-start(bf16[16,1024]{1,0:T(8,128)(2,1)S(1)} %collective-permute-done.19.refs_2_), channel_id=1, source_target_pairs={{0,1},{1,0},{2,3},{3,2},{4,5},{5,4},{6,7},{7,6},{8,9},{9,8},{10,11... | collective-permute-start | bytes 98312 | tf_op jit(solution)/shard_map/ppermute | solution.py:194
  45.0 5.8 %collective-permute-start.30 = (bf16[8,2048]{1,0:T(8,128)(2,1)S(1)}, bf16[8,2048]{1,0:T(8,128)(2,1)S(1)}, u32[]{:S(2)}, u32[]{:S(2)}) collective-permute-start(bf16[8,2048]{1,0:T(8,128)(2,1)S(1)} %get-tuple-element.34.refs_0_), channel_id=1, source_target_pairs={{0,6},{1,7},{2,4},{3,5},{4,2},{5,3},{6,0},{7,1},{8,14},{9,15},{10,... | collective-permute-start | bytes 98312 | tf_op jit(solution)/shard_map/ppermute | solution.py:194
  47.2 4.8 %collective-permute-start.28 = (bf16[8,2048]{1,0:T(8,128)(2,1)S(1)}, bf16[8,2048]{1,0:T(8,128)(2,1)S(1)}, u32[]{:S(2)}, u32[]{:S(2)}) collective-permute-start(bf16[8,2048]{1,0:T(8,128)(2,1)S(1)} %get-tuple-element.34.refs_0_), channel_id=1, source_target_pairs={{0,4},{1,5},{2,6},{3,7},{4,0},{5,1},{6,2},{7,3},{8,12},{9,13},{10,... | collective-permute-start | bytes 98312 | tf_op jit(solution)/shard_map/ppermute | solution.py:194
  47.2 4.8 %collective-permute-start.26 = (bf16[8,2048]{1,0:T(8,128)(2,1)S(1)}, bf16[8,2048]{1,0:T(8,128)(2,1)S(1)}, u32[]{:S(2)}, u32[]{:S(2)}) collective-permute-start(bf16[8,2048]{1,0:T(8,128)(2,1)S(1)} %get-tuple-element.34.refs_0_), channel_id=1, source_target_pairs={{0,2},{1,3},{2,0},{3,1},{4,6},{5,7},{6,4},{7,5},{8,10},{9,11},{10,... | collective-permute-start | bytes 98312 | tf_op jit(solution)/shard_map/ppermute | solution.py:194
  53.7 6.1 %collective-permute-start.37 = (bf16[64,256]{1,0:T(8,128)(2,1)S(1)}, bf16[64,256]{1,0:T(8,128)(2,1)S(1)}, u32[]{:S(2)}, u32[]{:S(2)}) collective-permute-start(bf16[64,256]{1,0:T(8,128)(2,1)S(1)} %shard_map.209.refs_0_.base_ref), channel_id=1, source_target_pairs={{0,6},{1,7},{2,4},{3,5},{4,2},{5,3},{6,0},{7,1},{8,14},{9,15},{10,... | collective-permute-start | bytes 98312 | tf_op jit(solution)/shard_map/ppermute | solution.py:194
  55.6 5.1 %collective-permute-start.35 = (bf16[64,256]{1,0:T(8,128)(2,1)S(1)}, bf16[64,256]{1,0:T(8,128)(2,1)S(1)}, u32[]{:S(2)}, u32[]{:S(2)}) collective-permute-start(bf16[64,256]{1,0:T(8,128)(2,1)S(1)} %shard_map.209.refs_0_.base_ref), channel_id=1, source_target_pairs={{0,4},{1,5},{2,6},{3,7},{4,0},{5,1},{6,2},{7,3},{8,12},{9,13},{10,... | collective-permute-start | bytes 98312 | tf_op jit(solution)/shard_map/ppermute | solution.py:194
  56.4 4.4 %collective-permute-start.33 = (bf16[64,256]{1,0:T(8,128)(2,1)S(1)}, bf16[64,256]{1,0:T(8,128)(2,1)S(1)}, u32[]{:S(2)}, u32[]{:S(2)}) collective-permute-start(bf16[64,256]{1,0:T(8,128)(2,1)S(1)} %shard_map.209.refs_0_.base_ref), channel_id=1, source_target_pairs={{0,2},{1,3},{2,0},{3,1},{4,6},{5,7},{6,4},{7,5},{8,10},{9,11},{10,... | collective-permute-start | bytes 98312 | tf_op jit(solution)/shard_map/ppermute | solution.py:194
  65.5 5.8 %collective-permute-start.40 = (bf16[64,256]{1,0:T(8,128)(2,1)S(1)}, bf16[64,256]{1,0:T(8,128)(2,1)S(1)}, u32[]{:S(2)}, u32[]{:S(2)}) collective-permute-start(bf16[64,256]{1,0:T(8,128)(2,1)S(1)} %get-tuple-element.38), channel_id=1, source_target_pairs={{0,2},{1,3},{2,0},{3,1},{4,6},{5,7},{6,4},{7,5},{8,10},{9,11},{10,... | collective-permute-start | bytes 98312 | tf_op jit(solution)/shard_map/ppermute | solution.py:194
  66.7 5.3 %collective-permute-start.41 = (bf16[64,256]{1,0:T(8,128)(2,1)S(1)}, bf16[64,256]{1,0:T(8,128)(2,1)S(1)}, u32[]{:S(2)}, u32[]{:S(2)}) collective-permute-start(bf16[64,256]{1,0:T(8,128)(2,1)S(1)} %get-tuple-element.39), channel_id=1, source_target_pairs={{0,4},{1,5},{2,6},{3,7},{4,0},{5,1},{6,2},{7,3},{8,12},{9,13},{10,... | collective-permute-start | bytes 98312 | tf_op jit(solution)/shard_map/ppermute | solution.py:194
  68.0 5.7 %collective-permute-start.42 = (bf16[64,256]{1,0:T(8,128)(2,1)S(1)}, bf16[64,256]{1,0:T(8,128)(2,1)S(1)}, u32[]{:S(2)}, u32[]{:S(2)}) collective-permute-start(bf16[64,256]{1,0:T(8,128)(2,1)S(1)} %get-tuple-element.40), channel_id=1, source_target_pairs={{0,6},{1,7},{2,4},{3,5},{4,2},{5,3},{6,0},{7,1},{8,14},{9,15},{10,... | collective-permute-start | bytes 98312 | tf_op jit(solution)/shard_map/ppermute | solution.py:194
  (40 other events, 748.3 us)

commit v3 on v2

--- a/solution.py
+++ b/solution.py
@@ -213,20 +213,17 @@
     return pair_up(near, count)
 
 
-def entry_kernel(tokens_hbm, gate_hbm, up_hbm, down_hbm, tokens_ref, sem):
-    copy = pltpu.make_async_copy(tokens_hbm, tokens_ref, sem)
-    copy.start()
-    copy.wait()
-
-
-def enter(tokens, *weights):
-    arrays = [pltpu.with_memory_space_constraint(a, pltpu.HBM) for a in (tokens, *weights)]
+def entry_kernel(gate_hbm, up_hbm, down_hbm, mark_ref):
+    mark_ref[...] = jnp.zeros_like(mark_ref)
+
+
+def enter(*weights):
+    arrays = [pltpu.with_memory_space_constraint(a, pltpu.HBM) for a in weights]
     return call(
         entry_kernel,
-        pltpu.VMEM(tokens.shape, tokens.dtype),
+        pltpu.VMEM((8, 128), F32),
         arrays,
         in_specs=[HBM_SPEC] * len(arrays),
-        scratch=[pltpu.SemaphoreType.DMA],
         limit=1 << 20,
     )
 
@@ -237,50 +234,103 @@
     return span, units - span
 
 
-def assemble(blocks, index, gain_ref, scaled_ref):
-    width = blocks[0].shape[1]
-    squares = None
-    for mask, block in enumerate(blocks):
-        values = block[...].astype(F32)
+def gained(block, owner, gain_ref):
+    width = block.shape[1]
+    column = pl.multiple_of(owner * width, width)
+    values = block[...].astype(F32)
+    squares = values * values
+    folded = squares[:, :128]
+    for first in range(128, width, 128):
+        folded = folded + squares[:, first : first + 128]
+    return (values * gain_ref[:, pl.ds(column, width)]).astype(BF16), folded
+
+
+def scale_of_rows(folded, channels):
+    return lax.rsqrt(jnp.sum(folded, axis=1, keepdims=True) / channels + EPSILON)
+
+
+def plus(total, part):
+    return part if total is None else total + part
+
+
+def early_masks(count):
+    late = (3, 5) if count > 4 else (3,)
+    return [m for m in range(count) if m not in late], list(late)
+
+
+def entry_kernel(gate_hbm, up_hbm, down_hbm, mark_ref):
+    mark_ref[...] = jnp.zeros_like(mark_ref)
+
+
+def enter(*weights):
+    arrays = [pltpu.with_memory_space_constraint(a, pltpu.HBM) for a in weights]
+    return call(
+        entry_kernel,
+        pltpu.VMEM((8, 128), F32),
+        arrays,
+        in_specs=[HBM_SPEC] * len(arrays),
+        limit=1 << 20,
+    )
+
+
+def core_span(units):
+    tiles = units // 128
+    span = -(-tiles // 2) * 128
+    return span, units - span
+
+
+def units_of(blocks, masks, gain_ref, gate_ref, up_ref, span, skip):
+    index = my_index()
+    start = pl.multiple_of(lax.axis_index("tp") * skip, 128)
+    gate_acc = up_acc = squares = None
+    for mask, block in zip(masks, blocks):
         owner = index ^ mask
-        column = pl.multiple_of(owner * width, width)
-        gain = gain_ref[:, pl.ds(column, width)]
-        scaled_ref[:, pl.ds(column, width)] = (values * gain).astype(BF16)
-        part = values * values
-        squares = part if squares is None else squares + part
-    total = jnp.sum(squares, axis=1, keepdims=True)
-    channels = width * len(blocks)
-    return lax.rsqrt(total / channels + EPSILON)
-
-
-def ffn_kernel(count, span, skip, *refs):
-    blocks = refs[:count]
-    gain_ref, gate_ref, up_ref, down_ref = refs[count : count + 4]
-    own_ref, cross_ref, scaled, hidden_ref = refs[count + 4 :]
+        width = block.shape[1]
+        rows = pl.ds(pl.multiple_of(owner * width, width), width)
+        lhs, folded = gained(block, owner, gain_ref)
+        squares = plus(squares, folded)
+        columns = pl.ds(start, span)
+        gate_acc = plus(gate_acc, jnp.dot(lhs, gate_ref[rows, columns], preferred_element_type=F32))
+        up_acc = plus(up_acc, jnp.dot(lhs, up_ref[rows, columns], preferred_element_type=F32))
+    return gate_acc, up_acc, squares
+
+
+def ffn_early_kernel(masks, span, skip, *refs):
+    blocks = refs[: len(masks)]
+    gain_ref, gate_ref, up_ref, _, _, gate_out, up_out, squares_out = refs[len(masks) :]
+    gate_out[...], up_out[...], squares_out[...] = units_of(
+        blocks, masks, gain_ref, gate_ref, up_ref, span, skip
+    )
+
+
+def ffn_late_kernel(masks, count, span, skip, *refs):
+    blocks = refs[: len(masks)]
+    gain_ref, gate_ref, up_ref, down_ref, gate_in, up_in, squares_in = refs[len(masks) : len(masks) + 7]
+    hidden_ref, cross_ref = refs[len(masks) + 7 :]
+    gate_acc, up_acc, squares = units_of(blocks, masks, gain_ref, gate_ref, up_ref, span, skip)
+    channels = gate_ref.shape[0]
+    row_scale = scale_of_rows(squares + squares_in[...], channels)
+    gate_act = (gate_acc + gate_in[...]) * row_scale
+    hidden = gate_act * jax.nn.sigmoid(gate_act) * ((up_acc + up_in[...]) * row_scale)
+    repeated = lax.axis_index("tp") * (lax.axis_size("tp") * span - down_ref.shape[0])
+    unit = lax.broadcasted_iota(jnp.int32, hidden.shape, 1)
+    hidden_ref[...] = jnp.where(unit >= repeated, hidden, 0.0).astype(BF16)
+    hidden = hidden_ref[...]
+    down_products(hidden, down_ref, range(1, count, 2), cross_ref, skip)
+
+
+def down_products(hidden, down_ref, masks, out_ref, skip):
     index = my_index()
-    core = lax.axis_index("tp")
-    start = pl.multiple_of(core * skip, 128)
-    width = blocks[0].shape[1]
-    row_scale = assemble(blocks, index, gain_ref, scaled)
-    lhs = scaled[...]
-    repeated = core * (lax.axis_size("tp") * span - down_ref.shape[0])
-    for first in range(0, span, 256):
-        size = min(256, span - first)
-        columns = pl.ds(pl.multiple_of(start + first, 128), size)
-        gate_act = jnp.dot(lhs, gate_ref[:, columns], preferred_element_type=F32) * row_scale
-        up_act = jnp.dot(lhs, up_ref[:, columns], preferred_element_type=F32) * row_scale
-        hidden = gate_act * jax.nn.sigmoid(gate_act) * up_act
-        unit = lax.broadcasted_iota(jnp.int32, hidden.shape, 1) + first
-        hidden_ref[:, first : first + size] = jnp.where(unit >= repeated, hidden, 0.0).astype(BF16)
-    hidden = hidden_ref[...]
-    for mask in list(range(1, count, 2)) + list(range(0, count, 2)):
+    start = pl.multiple_of(lax.axis_index("tp") * skip, 128)
+    span, width = hidden.shape[1], out_ref.shape[2]
+    for place, mask in enumerate(masks):
         column = pl.multiple_of((index ^ mask) * width, width)
         weight = down_ref[pl.ds(start, span), pl.ds(column, width)]
-        part = jnp.dot(hidden, weight, preferred_element_type=F32)
-        if mask % 2:
-            cross_ref[mask // 2] = part.astype(BF16)
-        else:
-            own_ref[mask // 2] = part
+        out_ref[place] = jnp.dot(hidden, weight, preferred_element_type=F32).astype(out_ref.dtype)
+
+
+def ffn_own_kernel(count, skip, hidden_ref, down_ref, own_ref):
+    down_products(hidden_ref[...], down_ref, range(0, count, 2), own_ref, skip)
 
 
 def pair_sum_kernel(own_ref, cross_ref, mine_ref, *sends):
@@ -296,18 +346,29 @@
     refs[-1][...] = (base_ref[...].astype(F32) + 0.5 * total).astype(BF16)
 
 
-def half_step(own, count, gain, gate, up, down, last=False):
+def half_step(own, mark, count, gain, gate, up, down, last=False):
     rows, width = own.shape
     near = count // 2
     span, skip = core_span(down.shape[0])
     blocks = gather_blocks(own, count)
-    own_part, cross_part = call(
-        functools.partial(ffn_kernel, count, span, skip),
-        [pltpu.VMEM((near, rows, width), F32), pltpu.VMEM((near, rows, width), BF16)],
-        [*blocks, gain.reshape(1, count * width), gate, up, down],
-        scratch=[pltpu.VMEM((rows, width * count), BF16), pltpu.VMEM((rows, span), BF16)],
+    gain = gain.reshape(1, count * width)
+    early, late = early_masks(count)
+    parts_early = call(
+        functools.partial(ffn_early_kernel, early, span, skip),
+        [pltpu.VMEM((rows, span), F32)] * 2 + [pltpu.VMEM((rows, 128), F32)],
+        [*(blocks[m] for m in early), gain, gate, up, down, mark],
+    )
+    hidden, cross_part = call(
+        functools.partial(ffn_late_kernel, late, count, span, skip),
+        [pltpu.VMEM((rows, span), BF16), pltpu.VMEM((near, rows, width), BF16)],
+        [*(blocks[m] for m in late), gain, gate, up, down, *parts_early],
     )
     cross_sum = swap(cross_part, 1, count)
+    own_part = call(
+        functools.partial(ffn_own_kernel, count, skip),
+        pltpu.VMEM((near, rows, width), F32),
+        [hidden, down],
+    )
     mine, *sends = call(
         pair_sum_kernel,
         [pltpu.VMEM((rows, width), F32)] + [pltpu.VMEM((rows, width), BF16)] * (near - 1),
@@ -318,27 +379,59 @@
     return call(residual_kernel, shape((rows, width), BF16), [own, mine, *received])
 
 
-def project_kernel(count, *refs):
-    blocks = refs[:count]
-    gain_ref, query_w, key_w, value_w, gating_w, write_t, forget_t = refs[count : count + 7]
-    *sends, pre_ref, scaled, result, pre_scratch = refs[count + 7 :]
+def mixes_of(blocks, masks, gain_ref, weights, thin):
     index = my_index()
-    row_scale = assemble(blocks, index, gain_ref, scaled)
-    lhs = scaled[...]
-    width = query_w.shape[1]
-    for place, weight in enumerate((query_w, key_w, value_w, gating_w)):
-        part = jnp.dot(lhs, weight[...], preferred_element_type=F32)
-        result[:, place * width : (place + 1) * width] = part * row_scale
-    heads = write_t.shape[0]
-    contract = (((1,), (1,)), ((), ()))
-    for place, weight in enumerate((write_t, forget_t)):
-        part = lax.dot_general(lhs, weight[...], contract, preferred_element_type=F32)
-        pre_scratch[:, place * heads : (place + 1) * heads] = part * row_scale
+    wide = [None] * len(weights)
+    narrow = [None] * len(thin)
+    squares = None
+    across = (((1,), (1,)), ((), ()))
+    for mask, block in zip(masks, blocks):
+        owner = index ^ mask
+        width = block.shape[1]
+        rows = pl.ds(pl.multiple_of(owner * width, width), width)
+        lhs, folded = gained(block, owner, gain_ref)
+        squares = plus(squares, folded)
+        for place, weight in enumerate(weights):
+            wide[place] = plus(wide[place], jnp.dot(lhs, weight[rows, :], preferred_element_type=F32))
+        for place, weight in enumerate(thin):
+            part = lax.dot_general(lhs, weight[:, rows], across, preferred_element_type=F32)
+            narrow[place] = plus(narrow[place], part)
+    return wide, narrow, squares
+
+
+def project_early_kernel(masks, *refs):
+    blocks = refs[: len(masks)]
+    gain_ref, *weights = refs[len(masks) : len(masks) + 7]
+    result, pre, squares_out = refs[len(masks) + 7 :]
+    wide, narrow, squares_out[...] = mixes_of(blocks, masks, gain_ref, weights[:4], weights[4:])
+    for place, part in enumerate(wide):
+        width = part.shape[1]
+        result[:, place * width : (place + 1) * width] = part
+    for place, part in enumerate(narrow):
+        width = part.shape[1]
+        pre[:, place * width : (place + 1) * width] = part
+
+
+def project_late_kernel(masks, *refs):
+    blocks = refs[: len(masks)]
+    gain_ref, *weights = refs[len(masks) : len(masks) + 7]
+    result_in, pre_in, squares_in = refs[len(masks) + 7 : len(masks) + 10]
+    *sends, pre_ref, result, pre_scratch = refs[len(masks) + 10 :]
+    wide, narrow, squares = mixes_of(blocks, masks, gain_ref, weights[:4], weights[4:])
+    row_scale = scale_of_rows(squares + squares_in[...], weights[0].shape[0])
+    for place, part in enumerate(wide):
+        width = part.shape[1]
+        columns = slice(place * width, (place + 1) * width)
+        result[:, columns] = (part + result_in[:, columns]) * row_scale
+    for place, part in enumerate(narrow):
+        width = part.shape[1]
+        columns = slice(place * width, (place + 1) * width)
+        pre_scratch[:, columns] = (part + pre_in[:, columns]) * row_scale
     for step, send in enumerate(sends):
         rows = send.shape[0]
         row = pl.multiple_of((lax.axis_index("kv") ^ step) * rows, rows)
         send[...] = result[pl.ds(row, rows), :].astype(BF16)
-    row = pl.multiple_of(index * BLK, BLK)
+    row = pl.multiple_of(my_index() * BLK, BLK)
     pre_ref[...] = pre_scratch[pl.ds(row, BLK), :]
 
 
@@ -381,7 +474,7 @@
     query_unit = query * lax.rsqrt(jnp.sum(query * query, axis=1, keepdims=True) + EPSILON) * (1.0 / math.sqrt(size))
     key_unit = key_in * lax.rsqrt(jnp.sum(key_in * key_in, axis=1, keepdims=True) + EPSILON)
     step_of = lax.broadcasted_iota(jnp.int32, (BLK, heads), 0)
-    live = (step_of < length_ref[0]).astype(F32)
+    live = (step_of < length_ref[...]).astype(F32)
     pre = pre_ref[...]
     write_gate = jax.nn.sigmoid(pre[:, :heads]) * live
     forget_in = pre[:, heads:]
@@ -497,21 +590,35 @@
     rows, width = tokens.shape
     channels = gain_first.shape[0]
     heads, size = state.shape[1], state.shape[2]
-    tokens = enter(tokens, first_gate, first_up, first_down)
-    after_first = half_step(tokens, count, gain_first, first_gate, first_up, first_down)
+    mark = enter(first_gate, first_up, first_down)
+    after_first = half_step(tokens, mark, count, gain_first, first_gate, first_up, first_down)
     blocks = gather_blocks(after_first, count)
-    weights = (query_weight, key_weight, value_weight, gating_weight)
     columns = 4 * width
     near = count // 2
-    *sends, pre = call(
-        functools.partial(project_kernel, count),
-        [pltpu.VMEM((rows // near, columns), BF16)] * near + [pltpu.VMEM((BLK, 2 * heads), F32)],
-        [*blocks, gain_mix.reshape(1, channels), *weights, write_weight.T, forget_weight.T],
-        scratch=[
-            pltpu.VMEM((rows, channels), BF16),
+    early, late = early_masks(count)
+    mixers = [
+        gain_mix.reshape(1, channels),
+        query_weight,
+        key_weight,
+        value_weight,
+        gating_weight,
+        write_weight.T,
+        forget_weight.T,
+    ]
+    parts_early = call(
+        functools.partial(project_early_kernel, early),
+        [
             pltpu.VMEM((rows, columns), F32),
             pltpu.VMEM((rows, 2 * heads), F32),
+            pltpu.VMEM((rows, 128), F32),
         ],
+        [*(blocks[m] for m in early), *mixers],
+    )
+    *sends, pre = call(
+        functools.partial(project_late_kernel, late),
+        [pltpu.VMEM((rows // near, columns), BF16)] * near + [pltpu.VMEM((BLK, 2 * heads), F32)],
+        [*(blocks[m] for m in late), *mixers, *parts_early],
+        scratch=[pltpu.VMEM((rows, columns), F32), pltpu.VMEM((rows, 2 * heads), F32)],
     )
     owned = pair_up([sends[0]] + far_swaps(sends[1:], count), count)
     matrices = state.reshape(heads, size, size)
@@ -523,8 +630,7 @@
             pltpu.VMEM((heads * BLK, size), F32),
             pltpu.VMEM((heads * BLK, size), F32),
         ],
-        [*owned, pre, forget_rate.reshape(1, heads), lengths, matrices],
-        in_specs=[VMEM_SPEC] * (count + 2) + [pl.BlockSpec(memory_space=pltpu.SMEM), VMEM_SPEC],
+        [*owned, pre, forget_rate.reshape(1, heads), lengths.reshape(1, 1), matrices],
         scratch=[pltpu.VMEM((count, BLK, columns), F32)],
     )
     head_blocks = gather_blocks(mixed, count)
@@ -540,7 +646,7 @@
         scratch=[pltpu.VMEM((rows, width), F32)],
     )
     mixed_out = half_step(
-        after_mix, count, gain_second, second_gate, second_up, second_down, last=True
+        after_mix, mark, count, gain_second, second_gate, second_up, second_down, last=True
     )
     return (mixed_out, new_state.reshape(state.shape))
 

time: 74.5 us -> 72.7 us (0.976)
  waiting for transfers between devices: 27 us -> 24.2 us
  local copies, waits for them, and re-layouts: 0.1 us -> 1.58 us
    ppermute x43, waiting for transfers between devices: 27 us -> 24.2 us  [swap(): return lax.ppermute(value, GROUP, [(i, i ^ mask) for i in range(count)])]
    unnamed x42 -> x46, local copies, waits for them, and re-layouts: 0.1 us -> 1.58 us
    pallas_call x11 -> x16, Pallas kernels: 9.74 us -> 9.59 us  [call(): pl.pallas_call(body, out_shape=shapes, in_specs=in_specs or [VMEM_SPEC] *...]
  transfers between devices with their start and end apart: 43 -> 43, of which waited for: 25 -> 19; matrix products, arithmetic and copies ran while one was open for 0% -> 0% of each run, Pallas kernels for 2% -> 7%
where the time goes in v3:
time: 72.7 us; the launch traced here: 72.5 us
  starting transfers between devices  35.3 us (49%)
  waiting for transfers between devices  24.2 us (33%)
  Pallas kernels  9.59 us (13%)
  between operations  1.77 us (2%)
  local copies, waits for them, and re-layouts  1.58 us (2%)
    ppermute x43, starting transfers between devices, swap(): return lax.ppermute(value, GROUP, [(i, i ^ mask) for i in range(count)])  35.3 us
    ppermute x43, waiting for transfers between devices, swap(): return lax.ppermute(value, GROUP, [(i, i ^ mask) for i in range(count)])  24.2 us
    pallas_call x16, Pallas kernels, call(): pl.pallas_call(body, out_shape=shapes, in_specs=in_specs or [VMEM_SPEC] *...  9.59 us
    unnamed x46, local copies, waits for them, and re-layouts  1.58 us
  transfers between devices with their start and end apart: 43, of which 19 were waited for; matrix products, arithmetic and copies ran while one was open for 0% of the time, Pallas kernels for 7%

profile of v3, /device:TPU:0, one launch (start us, length us, event | category | flops | bytes accessed | tf_op | source)
XLA Modules:
  0.0 72.5 jit_solution(12354728562961710655)
XLA Ops:
  0.7 5.1 %collective-permute-start.5 = (bf16[64,256]{1,0:T(8,128)(2,1)}, bf16[64,256]{1,0:T(8,128)(2,1)S(1)}, u32[]{:S(2)}, u32[]{:S(2)}) collective-permute-start(bf16[64,256]{1,0:T(8,128)(2,1)} %base_ref.1), channel_id=1, source_target_pairs={{0,6},{1,7},{2,4},{3,5},{4,2},{5,3},{6,0},{7,1},{8,14},{9,15},{10,... | collective-permute-start | bytes 98312 | tf_op jit(solution)/shard_map/ppermute | solution.py:194
  6.5 1.5 %collective-permute-done.5.refs_4_ = bf16[64,256]{1,0:T(8,128)(2,1)S(1)} collective-permute-done((bf16[64,256]{1,0:T(8,128)(2,1)}, bf16[64,256]{1,0:T(8,128)(2,1)S(1)}, u32[]{:S(2)}, u32[]{:S(2)}) %collective-permute-start.5) | collective-permute-done | bytes 32800 | tf_op jit(solution)/shard_map/ppermute | solution.py:194
  7.9 2.9 %collective-permute-done.2.refs_3_ = bf16[64,256]{1,0:T(8,128)(2,1)S(1)} collective-permute-done((bf16[64,256]{1,0:T(8,128)(2,1)}, bf16[64,256]{1,0:T(8,128)(2,1)S(1)}, u32[]{:S(2)}, u32[]{:S(2)}) %collective-permute-start.2) | collective-permute-done | bytes 32800 | tf_op jit(solution)/shard_map/ppermute | solution.py:194
  16.2 2.1 %collective-permute-start.9 = (bf16[64,256]{1,0:T(8,128)(2,1)S(1)}, bf16[64,256]{1,0:T(8,128)(2,1)S(1)}, u32[]{:S(2)}, u32[]{:S(2)}) collective-permute-start(bf16[64,256]{1,0:T(8,128)(2,1)S(1)} %get-tuple-element.39), channel_id=1, source_target_pairs={{0,4},{1,5},{2,6},{3,7},{4,0},{5,1},{6,2},{7,3},{8,12},{9,13},{10,... | collective-permute-start | bytes 98312 | tf_op jit(solution)/shard_map/ppermute | solution.py:194
  18.3 2.3 %collective-permute-start.10 = (bf16[64,256]{1,0:T(8,128)(2,1)S(1)}, bf16[64,256]{1,0:T(8,128)(2,1)S(1)}, u32[]{:S(2)}, u32[]{:S(2)}) collective-permute-start(bf16[64,256]{1,0:T(8,128)(2,1)S(1)} %get-tuple-element.40), channel_id=1, source_target_pairs={{0,6},{1,7},{2,4},{3,5},{4,2},{5,3},{6,0},{7,1},{8,14},{9,15},{10,... | collective-permute-start | bytes 98312 | tf_op jit(solution)/shard_map/ppermute | solution.py:194
  21.2 2.9 %collective-permute-done.10.refs_2_ = bf16[64,256]{1,0:T(8,128)(2,1)S(1)} collective-permute-done((bf16[64,256]{1,0:T(8,128)(2,1)S(1)}, bf16[64,256]{1,0:T(8,128)(2,1)S(1)}, u32[]{:S(2)}, u32[]{:S(2)}) %collective-permute-start.10) | collective-permute-done | bytes 32800 | tf_op jit(solution)/shard_map/ppermute | solution.py:194
  24.1 2.3 %collective-permute-start.16 = (bf16[64,256]{1,0:T(8,128)(2,1)S(1)}, bf16[64,256]{1,0:T(8,128)(2,1)S(1)}, u32[]{:S(2)}, u32[]{:S(2)}) collective-permute-start(bf16[64,256]{1,0:T(8,128)(2,1)S(1)} %shard_map.208.refs_0_.refs_9_), channel_id=1, source_target_pairs={{0,6},{1,7},{2,4},{3,5},{4,2},{5,3},{6,0},{7,1},{8,14},{9,15},{10,... | collective-permute-start | bytes 98312 | tf_op jit(solution)/shard_map/ppermute | solution.py:194
  26.4 2.1 %collective-permute-start.11 = (bf16[64,256]{1,0:T(8,128)(2,1)S(1)}, bf16[64,256]{1,0:T(8,128)(2,1)S(1)}, u32[]{:S(2)}, u32[]{:S(2)}) collective-permute-start(bf16[64,256]{1,0:T(8,128)(2,1)S(1)} %shard_map.208.refs_0_.refs_9_), channel_id=1, source_target_pairs={{0,2},{1,3},{2,0},{3,1},{4,6},{5,7},{6,4},{7,5},{8,10},{9,11},{10,... | collective-permute-start | bytes 98312 | tf_op jit(solution)/shard_map/ppermute | solution.py:194
  28.5 1.4 %collective-permute-done.16.refs_4_ = bf16[64,256]{1,0:T(8,128)(2,1)S(1)} collective-permute-done((bf16[64,256]{1,0:T(8,128)(2,1)S(1)}, bf16[64,256]{1,0:T(8,128)(2,1)S(1)}, u32[]{:S(2)}, u32[]{:S(2)}) %collective-permute-start.16) | collective-permute-done | bytes 32800 | tf_op jit(solution)/shard_map/ppermute | solution.py:194
  29.9 1.3 %collective-permute-done.13.refs_3_ = bf16[64,256]{1,0:T(8,128)(2,1)S(1)} collective-permute-done((bf16[64,256]{1,0:T(8,128)(2,1)S(1)}, bf16[64,256]{1,0:T(8,128)(2,1)S(1)}, u32[]{:S(2)}, u32[]{:S(2)}) %collective-permute-start.13) | collective-permute-done | bytes 32800 | tf_op jit(solution)/shard_map/ppermute | solution.py:194
  34.1 1.4 %collective-permute-start.21 = (bf16[16,1024]{1,0:T(8,128)(2,1)S(1)}, bf16[16,1024]{1,0:T(8,128)(2,1)S(1)}, u32[]{:S(2)}, u32[]{:S(2)}) collective-permute-start(bf16[16,1024]{1,0:T(8,128)(2,1)S(1)} %get-tuple-element.46), channel_id=1, source_target_pairs={{0,4},{1,5},{2,6},{3,7},{4,0},{5,1},{6,2},{7,3},{8,12},{9,13},{10,... | collective-permute-start | bytes 98312 | tf_op jit(solution)/shard_map/ppermute | solution.py:194
  35.5 2.1 %collective-permute-start.23 = (bf16[16,1024]{1,0:T(8,128)(2,1)S(1)}, bf16[16,1024]{1,0:T(8,128)(2,1)S(1)}, u32[]{:S(2)}, u32[]{:S(2)}) collective-permute-start(bf16[16,1024]{1,0:T(8,128)(2,1)S(1)} %get-tuple-element.47), channel_id=1, source_target_pairs={{0,6},{1,7},{2,4},{3,5},{4,2},{5,3},{6,0},{7,1},{8,14},{9,15},{10,... | collective-permute-start | bytes 98312 | tf_op jit(solution)/shard_map/ppermute | solution.py:194
  39.2 2.0 %collective-permute-done.23.refs_6_ = bf16[16,1024]{1,0:T(8,128)(2,1)S(1)} collective-permute-done((bf16[16,1024]{1,0:T(8,128)(2,1)S(1)}, bf16[16,1024]{1,0:T(8,128)(2,1)S(1)}, u32[]{:S(2)}, u32[]{:S(2)}) %collective-permute-start.23) | collective-permute-done | bytes 32800 | tf_op jit(solution)/shard_map/ppermute | solution.py:194
  42.4 1.7 %shard_map.211 = (bf16[8,2048]{1,0:T(8,128)(2,1)S(1)}, f32[128,128]{1,0:T(8,128)S(1)}, f32[128,128]{1,0:T(8,128)S(1)}, f32[128,128]{1,0:T(8,128)S(1)}) custom-call(bf16[16,1024]{1,0:T(8,128)(2,1)S(1)} %get-tuple-element.44.refs_0_, bf16[16,1024]{1,0:T(8,128)(2,1)S(1)} %collective-permute-done.18.refs_1_, ...), custom_call_target="tpu_custom_call" | custom-call | tf_op jit(solution)/shard_map/pallas_call | solution.py:178
  44.1 2.2 %collective-permute-start.30 = (bf16[8,2048]{1,0:T(8,128)(2,1)S(1)}, bf16[8,2048]{1,0:T(8,128)(2,1)S(1)}, u32[]{:S(2)}, u32[]{:S(2)}) collective-permute-start(bf16[8,2048]{1,0:T(8,128)(2,1)S(1)} %get-tuple-element.49.refs_0_), channel_id=1, source_target_pairs={{0,6},{1,7},{2,4},{3,5},{4,2},{5,3},{6,0},{7,1},{8,14},{9,15},{10,... | collective-permute-start | bytes 98312 | tf_op jit(solution)/shard_map/ppermute | solution.py:194
  46.3 2.3 %collective-permute-start.26 = (bf16[8,2048]{1,0:T(8,128)(2,1)S(1)}, bf16[8,2048]{1,0:T(8,128)(2,1)S(1)}, u32[]{:S(2)}, u32[]{:S(2)}) collective-permute-start(bf16[8,2048]{1,0:T(8,128)(2,1)S(1)} %get-tuple-element.49.refs_0_), channel_id=1, source_target_pairs={{0,2},{1,3},{2,0},{3,1},{4,6},{5,7},{6,4},{7,5},{8,10},{9,11},{10,... | collective-permute-start | bytes 98312 | tf_op jit(solution)/shard_map/ppermute | solution.py:194
  48.6 1.3 %collective-permute-done.30.refs_6_ = bf16[8,2048]{1,0:T(8,128)(2,1)S(1)} collective-permute-done((bf16[8,2048]{1,0:T(8,128)(2,1)S(1)}, bf16[8,2048]{1,0:T(8,128)(2,1)S(1)}, u32[]{:S(2)}, u32[]{:S(2)}) %collective-permute-start.30) | collective-permute-done | bytes 32800 | tf_op jit(solution)/shard_map/ppermute | solution.py:194
  52.8 2.0 %collective-permute-start.37 = (bf16[64,256]{1,0:T(8,128)(2,1)S(1)}, bf16[64,256]{1,0:T(8,128)(2,1)S(1)}, u32[]{:S(2)}, u32[]{:S(2)}) collective-permute-start(bf16[64,256]{1,0:T(8,128)(2,1)S(1)} %shard_map.212.refs_0_.base_ref), channel_id=1, source_target_pairs={{0,6},{1,7},{2,4},{3,5},{4,2},{5,3},{6,0},{7,1},{8,14},{9,15},{10,... | collective-permute-start | bytes 98312 | tf_op jit(solution)/shard_map/ppermute | solution.py:194
  55.6 1.7 %collective-permute-start.32 = (bf16[64,256]{1,0:T(8,128)(2,1)S(1)}, bf16[64,256]{1,0:T(8,128)(2,1)S(1)}, u32[]{:S(2)}, u32[]{:S(2)}) collective-permute-start(bf16[64,256]{1,0:T(8,128)(2,1)S(1)} %shard_map.212.refs_0_.base_ref), channel_id=1, source_target_pairs={{0,2},{1,3},{2,0},{3,1},{4,6},{5,7},{6,4},{7,5},{8,10},{9,11},{10,... | collective-permute-start | bytes 98312 | tf_op jit(solution)/shard_map/ppermute | solution.py:194
  57.3 1.6 %collective-permute-done.37.refs_4_ = bf16[64,256]{1,0:T(8,128)(2,1)S(1)} collective-permute-done((bf16[64,256]{1,0:T(8,128)(2,1)S(1)}, bf16[64,256]{1,0:T(8,128)(2,1)S(1)}, u32[]{:S(2)}, u32[]{:S(2)}) %collective-permute-start.37) | collective-permute-done | bytes 32800 | tf_op jit(solution)/shard_map/ppermute | solution.py:194
  64.7 1.4 %collective-permute-start.41 = (bf16[64,256]{1,0:T(8,128)(2,1)S(1)}, bf16[64,256]{1,0:T(8,128)(2,1)S(1)}, u32[]{:S(2)}, u32[]{:S(2)}) collective-permute-start(bf16[64,256]{1,0:T(8,128)(2,1)S(1)} %get-tuple-element.57), channel_id=1, source_target_pairs={{0,4},{1,5},{2,6},{3,7},{4,0},{5,1},{6,2},{7,3},{8,12},{9,13},{10,... | collective-permute-start | bytes 98312 | tf_op jit(solution)/shard_map/ppermute | solution.py:194
  66.1 2.1 %collective-permute-start.42 = (bf16[64,256]{1,0:T(8,128)(2,1)S(1)}, bf16[64,256]{1,0:T(8,128)(2,1)S(1)}, u32[]{:S(2)}, u32[]{:S(2)}) collective-permute-start(bf16[64,256]{1,0:T(8,128)(2,1)S(1)} %get-tuple-element.58), channel_id=1, source_target_pairs={{0,6},{1,7},{2,4},{3,5},{4,2},{5,3},{6,0},{7,1},{8,14},{9,15},{10,... | collective-permute-start | bytes 98312 | tf_op jit(solution)/shard_map/ppermute | solution.py:194
  68.2 1.3 %shard_map.218 = f32[16,128,128]{2,1,0:T(8,128)} custom-call(f32[128,128]{1,0:T(8,128)S(1)} %get-tuple-element.59.update_ref, f32[128,128]{1,0:T(8,128)S(1)} %get-tuple-element.60.faded_ref, f32[128,128]{1,0:T(8,128)S(1)} %get-tuple-element.61.final_ref, f32[16,128,128]{2,1,0:T(8,128)S(1)} %bitcast.17), custom_call_target="tpu_custom_call" | custom-call | tf_op jit(solution)/shard_map/pallas_call | solution.py:178
  69.7 2.1 %collective-permute-done.42.refs_2_ = bf16[64,256]{1,0:T(8,128)(2,1)S(1)} collective-permute-done((bf16[64,256]{1,0:T(8,128)(2,1)S(1)}, bf16[64,256]{1,0:T(8,128)(2,1)S(1)}, u32[]{:S(2)}, u32[]{:S(2)}) %collective-permute-start.42) | collective-permute-done | bytes 32800 | tf_op jit(solution)/shard_map/ppermute | solution.py:194
  (127 shorter events, 21.6 us)
Async XLA Ops:
  0.7 7.2 %collective-permute-start.5 = (bf16[64,256]{1,0:T(8,128)(2,1)}, bf16[64,256]{1,0:T(8,128)(2,1)S(1)}, u32[]{:S(2)}, u32[]{:S(2)}) collective-permute-start(bf16[64,256]{1,0:T(8,128)(2,1)} %base_ref.1), channel_id=1, source_target_pairs={{0,6},{1,7},{2,4},{3,5},{4,2},{5,3},{6,0},{7,1},{8,14},{9,15},{10,... | collective-permute-start | bytes 98312 | tf_op jit(solution)/shard_map/ppermute | solution.py:194
  5.8 5.0 %collective-permute-start.2 = (bf16[64,256]{1,0:T(8,128)(2,1)}, bf16[64,256]{1,0:T(8,128)(2,1)S(1)}, u32[]{:S(2)}, u32[]{:S(2)}) collective-permute-start(bf16[64,256]{1,0:T(8,128)(2,1)} %base_ref.1), channel_id=1, source_target_pairs={{0,4},{1,5},{2,6},{3,7},{4,0},{5,1},{6,2},{7,3},{8,12},{9,13},{10,... | collective-permute-start | bytes 98312 | tf_op jit(solution)/shard_map/ppermute | solution.py:194
  5.8 5.0 %collective-permute-start = (bf16[64,256]{1,0:T(8,128)(2,1)}, bf16[64,256]{1,0:T(8,128)(2,1)S(1)}, u32[]{:S(2)}, u32[]{:S(2)}) collective-permute-start(bf16[64,256]{1,0:T(8,128)(2,1)} %base_ref.1), channel_id=1, source_target_pairs={{0,2},{1,3},{2,0},{3,1},{4,6},{5,7},{6,4},{7,5},{8,10},{9,11},{10,... | collective-permute-start | bytes 98312 | tf_op jit(solution)/shard_map/ppermute | solution.py:194
  6.4 4.9 %collective-permute-start.4 = (bf16[64,256]{1,0:T(8,128)(2,1)}, bf16[64,256]{1,0:T(8,128)(2,1)S(1)}, u32[]{:S(2)}, u32[]{:S(2)}) collective-permute-start(bf16[64,256]{1,0:T(8,128)(2,1)} %base_ref.1), channel_id=1, source_target_pairs={{0,1},{1,0},{2,3},{3,2},{4,5},{5,4},{6,7},{7,6},{8,9},{9,8},{10,11... | collective-permute-start | bytes 98312 | tf_op jit(solution)/shard_map/ppermute | solution.py:194
  16.1 4.5 %collective-permute-start.8 = (bf16[64,256]{1,0:T(8,128)(2,1)S(1)}, bf16[64,256]{1,0:T(8,128)(2,1)S(1)}, u32[]{:S(2)}, u32[]{:S(2)}) collective-permute-start(bf16[64,256]{1,0:T(8,128)(2,1)S(1)} %get-tuple-element.38), channel_id=1, source_target_pairs={{0,2},{1,3},{2,0},{3,1},{4,6},{5,7},{6,4},{7,5},{8,10},{9,11},{10,... | collective-permute-start | bytes 98312 | tf_op jit(solution)/shard_map/ppermute | solution.py:194
  16.2 4.9 %collective-permute-start.9 = (bf16[64,256]{1,0:T(8,128)(2,1)S(1)}, bf16[64,256]{1,0:T(8,128)(2,1)S(1)}, u32[]{:S(2)}, u32[]{:S(2)}) collective-permute-start(bf16[64,256]{1,0:T(8,128)(2,1)S(1)} %get-tuple-element.39), channel_id=1, source_target_pairs={{0,4},{1,5},{2,6},{3,7},{4,0},{5,1},{6,2},{7,3},{8,12},{9,13},{10,... | collective-permute-start | bytes 98312 | tf_op jit(solution)/shard_map/ppermute | solution.py:194
  18.3 5.7 %collective-permute-start.10 = (bf16[64,256]{1,0:T(8,128)(2,1)S(1)}, bf16[64,256]{1,0:T(8,128)(2,1)S(1)}, u32[]{:S(2)}, u32[]{:S(2)}) collective-permute-start(bf16[64,256]{1,0:T(8,128)(2,1)S(1)} %get-tuple-element.40), channel_id=1, source_target_pairs={{0,6},{1,7},{2,4},{3,5},{4,2},{5,3},{6,0},{7,1},{8,14},{9,15},{10,... | collective-permute-start | bytes 98312 | tf_op jit(solution)/shard_map/ppermute | solution.py:194
  24.1 5.9 %collective-permute-start.16 = (bf16[64,256]{1,0:T(8,128)(2,1)S(1)}, bf16[64,256]{1,0:T(8,128)(2,1)S(1)}, u32[]{:S(2)}, u32[]{:S(2)}) collective-permute-start(bf16[64,256]{1,0:T(8,128)(2,1)S(1)} %shard_map.208.refs_0_.refs_9_), channel_id=1, source_target_pairs={{0,6},{1,7},{2,4},{3,5},{4,2},{5,3},{6,0},{7,1},{8,14},{9,15},{10,... | collective-permute-start | bytes 98312 | tf_op jit(solution)/shard_map/ppermute | solution.py:194
  26.4 4.8 %collective-permute-start.13 = (bf16[64,256]{1,0:T(8,128)(2,1)S(1)}, bf16[64,256]{1,0:T(8,128)(2,1)S(1)}, u32[]{:S(2)}, u32[]{:S(2)}) collective-permute-start(bf16[64,256]{1,0:T(8,128)(2,1)S(1)} %shard_map.208.refs_0_.refs_9_), channel_id=1, source_target_pairs={{0,4},{1,5},{2,6},{3,7},{4,0},{5,1},{6,2},{7,3},{8,12},{9,13},{10,... | collective-permute-start | bytes 98312 | tf_op jit(solution)/shard_map/ppermute | solution.py:194
  26.4 4.8 %collective-permute-start.11 = (bf16[64,256]{1,0:T(8,128)(2,1)S(1)}, bf16[64,256]{1,0:T(8,128)(2,1)S(1)}, u32[]{:S(2)}, u32[]{:S(2)}) collective-permute-start(bf16[64,256]{1,0:T(8,128)(2,1)S(1)} %shard_map.208.refs_0_.refs_9_), channel_id=1, source_target_pairs={{0,2},{1,3},{2,0},{3,1},{4,6},{5,7},{6,4},{7,5},{8,10},{9,11},{10,... | collective-permute-start | bytes 98312 | tf_op jit(solution)/shard_map/ppermute | solution.py:194
  33.1 4.5 %collective-permute-start.19 = (bf16[16,1024]{1,0:T(8,128)(2,1)S(1)}, bf16[16,1024]{1,0:T(8,128)(2,1)S(1)}, u32[]{:S(2)}, u32[]{:S(2)}) collective-permute-start(bf16[16,1024]{1,0:T(8,128)(2,1)S(1)} %get-tuple-element.45), channel_id=1, source_target_pairs={{0,2},{1,3},{2,0},{3,1},{4,6},{5,7},{6,4},{7,5},{8,10},{9,11},{10,... | collective-permute-start | bytes 98312 | tf_op jit(solution)/shard_map/ppermute | solution.py:194
  34.1 5.1 %collective-permute-start.21 = (bf16[16,1024]{1,0:T(8,128)(2,1)S(1)}, bf16[16,1024]{1,0:T(8,128)(2,1)S(1)}, u32[]{:S(2)}, u32[]{:S(2)}) collective-permute-start(bf16[16,1024]{1,0:T(8,128)(2,1)S(1)} %get-tuple-element.46), channel_id=1, source_target_pairs={{0,4},{1,5},{2,6},{3,7},{4,0},{5,1},{6,2},{7,3},{8,12},{9,13},{10,... | collective-permute-start | bytes 98312 | tf_op jit(solution)/shard_map/ppermute | solution.py:194
  35.5 5.7 %collective-permute-start.23 = (bf16[16,1024]{1,0:T(8,128)(2,1)S(1)}, bf16[16,1024]{1,0:T(8,128)(2,1)S(1)}, u32[]{:S(2)}, u32[]{:S(2)}) collective-permute-start(bf16[16,1024]{1,0:T(8,128)(2,1)S(1)} %get-tuple-element.47), channel_id=1, source_target_pairs={{0,6},{1,7},{2,4},{3,5},{4,2},{5,3},{6,0},{7,1},{8,14},{9,15},{10,... | collective-permute-start | bytes 98312 | tf_op jit(solution)/shard_map/ppermute | solution.py:194
  37.6 4.2 %collective-permute-start.18 = (bf16[16,1024]{1,0:T(8,128)(2,1)S(1)}, bf16[16,1024]{1,0:T(8,128)(2,1)S(1)}, u32[]{:S(2)}, u32[]{:S(2)}) collective-permute-start(bf16[16,1024]{1,0:T(8,128)(2,1)S(1)} %get-tuple-element.44.refs_0_), channel_id=1, source_target_pairs={{0,1},{1,0},{2,3},{3,2},{4,5},{5,4},{6,7},{7,6},{8,9},{9,8},{10,11... | collective-permute-start | bytes 98312 | tf_op jit(solution)/shard_map/ppermute | solution.py:194
  37.6 4.3 %collective-permute-start.20 = (bf16[16,1024]{1,0:T(8,128)(2,1)S(1)}, bf16[16,1024]{1,0:T(8,128)(2,1)S(1)}, u32[]{:S(2)}, u32[]{:S(2)}) collective-permute-start(bf16[16,1024]{1,0:T(8,128)(2,1)S(1)} %collective-permute-done.19.refs_2_), channel_id=1, source_target_pairs={{0,1},{1,0},{2,3},{3,2},{4,5},{5,4},{6,7},{7,6},{8,9},{9,8},{10,11... | collective-permute-start | bytes 98312 | tf_op jit(solution)/shard_map/ppermute | solution.py:194
  44.1 5.8 %collective-permute-start.30 = (bf16[8,2048]{1,0:T(8,128)(2,1)S(1)}, bf16[8,2048]{1,0:T(8,128)(2,1)S(1)}, u32[]{:S(2)}, u32[]{:S(2)}) collective-permute-start(bf16[8,2048]{1,0:T(8,128)(2,1)S(1)} %get-tuple-element.49.refs_0_), channel_id=1, source_target_pairs={{0,6},{1,7},{2,4},{3,5},{4,2},{5,3},{6,0},{7,1},{8,14},{9,15},{10,... | collective-permute-start | bytes 98312 | tf_op jit(solution)/shard_map/ppermute | solution.py:194
  46.3 4.8 %collective-permute-start.28 = (bf16[8,2048]{1,0:T(8,128)(2,1)S(1)}, bf16[8,2048]{1,0:T(8,128)(2,1)S(1)}, u32[]{:S(2)}, u32[]{:S(2)}) collective-permute-start(bf16[8,2048]{1,0:T(8,128)(2,1)S(1)} %get-tuple-element.49.refs_0_), channel_id=1, source_target_pairs={{0,4},{1,5},{2,6},{3,7},{4,0},{5,1},{6,2},{7,3},{8,12},{9,13},{10,... | collective-permute-start | bytes 98312 | tf_op jit(solution)/shard_map/ppermute | solution.py:194
  46.3 4.8 %collective-permute-start.26 = (bf16[8,2048]{1,0:T(8,128)(2,1)S(1)}, bf16[8,2048]{1,0:T(8,128)(2,1)S(1)}, u32[]{:S(2)}, u32[]{:S(2)}) collective-permute-start(bf16[8,2048]{1,0:T(8,128)(2,1)S(1)} %get-tuple-element.49.refs_0_), channel_id=1, source_target_pairs={{0,2},{1,3},{2,0},{3,1},{4,6},{5,7},{6,4},{7,5},{8,10},{9,11},{10,... | collective-permute-start | bytes 98312 | tf_op jit(solution)/shard_map/ppermute | solution.py:194
  52.8 6.1 %collective-permute-start.37 = (bf16[64,256]{1,0:T(8,128)(2,1)S(1)}, bf16[64,256]{1,0:T(8,128)(2,1)S(1)}, u32[]{:S(2)}, u32[]{:S(2)}) collective-permute-start(bf16[64,256]{1,0:T(8,128)(2,1)S(1)} %shard_map.212.refs_0_.base_ref), channel_id=1, source_target_pairs={{0,6},{1,7},{2,4},{3,5},{4,2},{5,3},{6,0},{7,1},{8,14},{9,15},{10,... | collective-permute-start | bytes 98312 | tf_op jit(solution)/shard_map/ppermute | solution.py:194
  54.8 5.1 %collective-permute-start.34 = (bf16[64,256]{1,0:T(8,128)(2,1)S(1)}, bf16[64,256]{1,0:T(8,128)(2,1)S(1)}, u32[]{:S(2)}, u32[]{:S(2)}) collective-permute-start(bf16[64,256]{1,0:T(8,128)(2,1)S(1)} %shard_map.212.refs_0_.base_ref), channel_id=1, source_target_pairs={{0,4},{1,5},{2,6},{3,7},{4,0},{5,1},{6,2},{7,3},{8,12},{9,13},{10,... | collective-permute-start | bytes 98312 | tf_op jit(solution)/shard_map/ppermute | solution.py:194
  55.6 4.4 %collective-permute-start.32 = (bf16[64,256]{1,0:T(8,128)(2,1)S(1)}, bf16[64,256]{1,0:T(8,128)(2,1)S(1)}, u32[]{:S(2)}, u32[]{:S(2)}) collective-permute-start(bf16[64,256]{1,0:T(8,128)(2,1)S(1)} %shard_map.212.refs_0_.base_ref), channel_id=1, source_target_pairs={{0,2},{1,3},{2,0},{3,1},{4,6},{5,7},{6,4},{7,5},{8,10},{9,11},{10,... | collective-permute-start | bytes 98312 | tf_op jit(solution)/shard_map/ppermute | solution.py:194
  63.7 5.8 %collective-permute-start.40 = (bf16[64,256]{1,0:T(8,128)(2,1)S(1)}, bf16[64,256]{1,0:T(8,128)(2,1)S(1)}, u32[]{:S(2)}, u32[]{:S(2)}) collective-permute-start(bf16[64,256]{1,0:T(8,128)(2,1)S(1)} %get-tuple-element.56), channel_id=1, source_target_pairs={{0,2},{1,3},{2,0},{3,1},{4,6},{5,7},{6,4},{7,5},{8,10},{9,11},{10,... | collective-permute-start | bytes 98312 | tf_op jit(solution)/shard_map/ppermute | solution.py:194
  64.7 5.0 %collective-permute-start.41 = (bf16[64,256]{1,0:T(8,128)(2,1)S(1)}, bf16[64,256]{1,0:T(8,128)(2,1)S(1)}, u32[]{:S(2)}, u32[]{:S(2)}) collective-permute-start(bf16[64,256]{1,0:T(8,128)(2,1)S(1)} %get-tuple-element.57), channel_id=1, source_target_pairs={{0,4},{1,5},{2,6},{3,7},{4,0},{5,1},{6,2},{7,3},{8,12},{9,13},{10,... | collective-permute-start | bytes 98312 | tf_op jit(solution)/shard_map/ppermute | solution.py:194
  66.1 5.7 %collective-permute-start.42 = (bf16[64,256]{1,0:T(8,128)(2,1)S(1)}, bf16[64,256]{1,0:T(8,128)(2,1)S(1)}, u32[]{:S(2)}, u32[]{:S(2)}) collective-permute-start(bf16[64,256]{1,0:T(8,128)(2,1)S(1)} %get-tuple-element.58), channel_id=1, source_target_pairs={{0,6},{1,7},{2,4},{3,5},{4,2},{5,3},{6,0},{7,1},{8,14},{9,15},{10,... | collective-permute-start | bytes 98312 | tf_op jit(solution)/shard_map/ppermute | solution.py:194
  (42 other events, 565.6 us)

commit v4 on v3

--- a/solution.py
+++ b/solution.py
@@ -228,6 +228,26 @@
     )
 
 
+def stage_kernel(count, *refs):
+    sources, targets, sem = refs[:count], refs[count : 2 * count], refs[2 * count]
+    copies = [pltpu.make_async_copy(*pair, sem.at[i]) for i, pair in enumerate(zip(sources, targets))]
+    for copy in copies:
+        copy.start()
+    for copy in copies:
+        copy.wait()
+
+
+def stage(*arrays):
+    return call(
+        functools.partial(stage_kernel, len(arrays)),
+        [pltpu.VMEM(a.shape, a.dtype) for a in arrays],
+        [pltpu.with_memory_space_constraint(a, pltpu.HBM) for a in arrays],
+        in_specs=[HBM_SPEC] * len(arrays),
+        scratch=[pltpu.SemaphoreType.DMA((len(arrays),))],
+        limit=1 << 20,
+    )
+
+
 def core_span(units):
     tiles = units // 128
     span = -(-tiles // 2) * 128
@@ -346,12 +366,16 @@
     refs[-1][...] = (base_ref[...].astype(F32) + 0.5 * total).astype(BF16)
 
 
-def half_step(own, mark, count, gain, gate, up, down, last=False):
+def half_step(own, mark, count, gain, gate, up, down, first=False, last=False):
     rows, width = own.shape
     near = count // 2
     span, skip = core_span(down.shape[0])
-    blocks = gather_blocks(own, count)
     gain = gain.reshape(1, count * width)
+    near_own = own
+    if first:
+        own, gain = stage(own, gain)
+    received = far_swaps([near_own] * (near - 1), count)
+    blocks = pair_up([own, *received], count)
     early, late = early_masks(count)
     parts_early = call(
         functools.partial(ffn_early_kernel, early, span, skip),
@@ -448,36 +472,48 @@
     return total + lax.dot_general(left_high, right_high, dims, preferred_element_type=F32)
 
 
-def delta_kernel(count, *refs):
-    blocks = refs[:count]
-    pre_ref, rate_ref, length_ref, state_ref = refs[count : count + 4]
-    mixed_ref, update_ref, faded_ref, final_ref, ordered = refs[count + 4 :]
+def split_state_kernel(state_ref, length_ref, high_ref, low_ref, live_ref):
+    high_ref[...], low_ref[...] = parts(state_ref[...])
+    step_of = lax.broadcasted_iota(jnp.int32, live_ref.shape, 0)
+    live_ref[...] = (step_of < length_ref[...]).astype(F32)
+
+
+def delta_kernel(masks, count, *refs):
+    blocks = refs[: len(masks)]
+    pre_ref, rate_ref, live_ref, high_ref, low_ref = refs[len(masks) : len(masks) + 5]
+    mixed_ref, update_ref, faded_ref, final_ref = refs[len(masks) + 5 :]
     index = my_index()
     first_core = lax.axis_index("tp") == 0
-    for mask, block in enumerate(blocks):
-        both = block[...].astype(F32)
-        ordered[pl.ds(index ^ mask, 1)] = jnp.where(first_core, both[:BLK], both[BLK:])[None]
-    heads = rate_ref.shape[1]
-    size = state_ref.shape[-1]
-    per_block = heads // count
+    size = high_ref.shape[-1]
+    all_heads = rate_ref.shape[1]
+    per_block = all_heads // count
+    heads = per_block * len(masks)
     rows = heads * BLK
     width = per_block * size
+    taken = []
+    for block in blocks:
+        both = block[...].astype(F32)
+        taken.append(jnp.where(first_core, both[:BLK], both[BLK:]))
 
     def stack(place):
         found = []
-        for head in range(heads):
-            column = place * width + (head % per_block) * size
-            found.append(ordered[head // per_block, :, column : column + size])
+        for block in taken:
+            for head in range(per_block):
+                column = place * width + head * size
+                found.append(block[:, column : column + size])
         return jnp.concatenate(found, axis=0)
+
+    def head_at(head):
+        return (index ^ masks[head // per_block]) * per_block + head % per_block
 
     query, key_in, value, gating = (stack(place) for place in range(4))
     query_unit = query * lax.rsqrt(jnp.sum(query * query, axis=1, keepdims=True) + EPSILON) * (1.0 / math.sqrt(size))
     key_unit = key_in * lax.rsqrt(jnp.sum(key_in * key_in, axis=1, keepdims=True) + EPSILON)
-    step_of = lax.broadcasted_iota(jnp.int32, (BLK, heads), 0)
-    live = (step_of < length_ref[...]).astype(F32)
+    step_of = lax.broadcasted_iota(jnp.int32, (BLK, all_heads), 0)
+    live = live_ref[...]
     pre = pre_ref[...]
-    write_gate = jax.nn.sigmoid(pre[:, :heads]) * live
-    forget_in = pre[:, heads:]
+    write_gate = jax.nn.sigmoid(pre[:, :all_heads]) * live
+    forget_in = pre[:, all_heads:]
     softplus = jnp.maximum(forget_in, 0.0) + jnp.log1p(jnp.exp(-jnp.abs(forget_in)))
     forget = -jnp.exp(rate_ref[...]) * softplus * live
     cumulative = forget
@@ -486,9 +522,9 @@
         moved = pltpu.roll(cumulative, lower, 0)
         cumulative = cumulative + jnp.where(step_of >= lower, moved, 0.0)
         lower *= 2
-    final = jnp.broadcast_to(cumulative[BLK - 1 :, :], (BLK, heads))
-    row_head = lax.broadcasted_iota(jnp.int32, (rows, heads), 0) // BLK
-    picked = row_head == lax.broadcasted_iota(jnp.int32, (rows, heads), 1)
+    final = jnp.broadcast_to(cumulative[BLK - 1 :, :], (BLK, all_heads))
+    head_of = lax.broadcasted_iota(jnp.int32, (BLK, all_heads), 1)
+    picked = jnp.concatenate([head_of == head_at(head) for head in range(heads)], axis=0)
 
     def column_of(array):
         tall = jnp.concatenate([array] * heads, axis=0)
@@ -520,7 +556,7 @@
     for head in range(heads):
         at = slice(head * BLK, (head + 1) * BLK)
         both = jnp.concatenate([key_grown[at], query_grown[at]], axis=0)
-        found = dot_parts(parts(both), parts(state_ref[head]))
+        found = dot_parts(parts(both), (high_ref[head_at(head)], low_ref[head_at(head)]))
         from_key.append(found[:BLK])
         from_query.append(found[BLK:])
     target = write_col * (value - jnp.concatenate(from_key, axis=0))
@@ -535,18 +571,33 @@
     final_ref[...] = jnp.broadcast_to(jnp.exp(final_col), final_ref.shape)
 
 
-def state_kernel(update_ref, faded_ref, final_ref, state_ref, new_ref):
-    heads = state_ref.shape[0]
+def join_kernel(count, first_ref, second_ref, mixed_ref):
+    width = mixed_ref.shape[1] // count
+    index = my_index()
+    for mask in range(count):
+        source = second_ref if mask % 2 else first_ref
+        place = mask // 2
+        column = pl.multiple_of((index ^ mask) * width, width)
+        mixed_ref[:, pl.ds(column, width)] = source[:, place * width : (place + 1) * width]
+
+
+def state_kernel(groups, count, *refs):
+    state_ref, new_ref = refs[3 * len(groups) :]
+    per_block = state_ref.shape[0] // count
+    index = my_index()
     along = (((0,), (0,)), ((), ()))
-    for head in range(heads):
-        at = slice(head * BLK, (head + 1) * BLK)
-        left_high, left_low = parts(faded_ref[at])
-        right_high, right_low = parts(update_ref[at])
-        left = jnp.concatenate([left_high, left_high, left_low, left_low], axis=0)
-        right = jnp.concatenate([right_high, right_low, right_high, right_low], axis=0)
-        grown = lax.dot_general(left, right, along, preferred_element_type=F32)
-        scale = final_ref[head * BLK : head * BLK + 1, :]
-        new_ref[head] = scale * state_ref[head] + grown
+    for place, masks in enumerate(groups):
+        update_ref, faded_ref, final_ref = refs[3 * place : 3 * place + 3]
+        for head in range(per_block * len(masks)):
+            at = slice(head * BLK, (head + 1) * BLK)
+            left_high, left_low = parts(faded_ref[at])
+            right_high, right_low = parts(update_ref[at])
+            left = jnp.concatenate([left_high, left_high, left_low, left_low], axis=0)
+            right = jnp.concatenate([right_high, right_low, right_high, right_low], axis=0)
+            grown = lax.dot_general(left, right, along, preferred_element_type=F32)
+            scale = final_ref[head * BLK : head * BLK + 1, :]
+            owner = (index ^ masks[head // per_block]) * per_block + head % per_block
+            new_ref[pl.ds(owner, 1)] = (scale * state_ref[owner] + grown)[None]
 
 
 def out_kernel(count, *refs):
@@ -591,7 +642,9 @@
     channels = gain_first.shape[0]
     heads, size = state.shape[1], state.shape[2]
     mark = enter(first_gate, first_up, first_down)
-    after_first = half_step(tokens, mark, count, gain_first, first_gate, first_up, first_down)
+    after_first = half_step(
+        tokens, mark, count, gain_first, first_gate, first_up, first_down, first=True
+    )
     blocks = gather_blocks(after_first, count)
     columns = 4 * width
     near = count // 2
@@ -622,22 +675,38 @@
     )
     owned = pair_up([sends[0]] + far_swaps(sends[1:], count), count)
     matrices = state.reshape(heads, size, size)
-    mixed, update, faded, final = call(
-        functools.partial(delta_kernel, count),
-        [
-            pltpu.VMEM((BLK, channels), BF16),
-            pltpu.VMEM((heads * BLK, size), F32),
-            pltpu.VMEM((heads * BLK, size), F32),
-            pltpu.VMEM((heads * BLK, size), F32),
-        ],
-        [*owned, pre, forget_rate.reshape(1, heads), lengths.reshape(1, 1), matrices],
-        scratch=[pltpu.VMEM((count, BLK, columns), F32)],
+    high, low, live = call(
+        split_state_kernel,
+        [pltpu.VMEM(matrices.shape, BF16)] * 2 + [pltpu.VMEM((BLK, heads), F32)],
+        [matrices, lengths.reshape(1, 1)],
+        limit=3 << 20,
+    )
+    groups = [list(range(0, count, 2)), list(range(1, count, 2))]
+    mixed_parts, grown = [], []
+    for masks in groups:
+        tall = heads * BLK // 2
+        part, *rest = call(
+            functools.partial(delta_kernel, masks, count),
+            [pltpu.VMEM((BLK, channels // 2), BF16)] + [pltpu.VMEM((tall, size), F32)] * 3,
+            [
+                *(owned[m] for m in masks),
+                pre,
+                forget_rate.reshape(1, heads),
+                live,
+                high,
+                low,
+            ],
+        )
+        mixed_parts.append(part)
+        grown += rest
+    mixed = call(
+        functools.partial(join_kernel, count), pltpu.VMEM((BLK, channels), BF16), mixed_parts
     )
     head_blocks = gather_blocks(mixed, count)
     new_state = call(
-        state_kernel,
+        functools.partial(state_kernel, groups, count),
         jax.ShapeDtypeStruct((heads, size, size), F32),
-        [update, faded, final, matrices],
+        [*grown, matrices],
     )
     after_mix = call(
         functools.partial(out_kernel, count),

time: 72.7 us -> 76.4 us (1.051)
  Pallas kernels: 9.59 us -> 11.5 us
  waiting for transfers between devices: 24.2 us -> 25.8 us
  local copies, waits for them, and re-layouts: 1.58 us -> 2.43 us
    pallas_call x16 -> x20, Pallas kernels: 9.59 us -> 11.5 us  [call(): pl.pallas_call(body, out_shape=shapes, in_specs=in_specs or [VMEM_SPEC] *...]
    ppermute x43, waiting for transfers between devices: 24.2 us -> 25.8 us  [swap(): return lax.ppermute(value, GROUP, [(i, i ^ mask) for i in range(count)])]
    unnamed x46 -> x44, local copies, waits for them, and re-layouts: 1.58 us -> 2.43 us
  transfers between devices with their start and end apart: 43 -> 43, of which waited for: 19 -> 21; matrix products, arithmetic and copies ran while one was open for 0% -> 0% of each run, Pallas kernels for 7% -> 9%
where the time goes in v4:
time: 76.4 us; the launch traced here: 76.2 us
  starting transfers between devices  34.6 us (45%)
  waiting for transfers between devices  25.8 us (34%)
  Pallas kernels  11.5 us (15%)
  local copies, waits for them, and re-layouts  2.43 us (3%)
  between operations  1.82 us (2%)
    ppermute x43, starting transfers between devices, swap(): return lax.ppermute(value, GROUP, [(i, i ^ mask) for i in range(count)])  34.6 us
    ppermute x43, waiting for transfers between devices, swap(): return lax.ppermute(value, GROUP, [(i, i ^ mask) for i in range(count)])  25.8 us
    pallas_call x20, Pallas kernels, call(): pl.pallas_call(body, out_shape=shapes, in_specs=in_specs or [VMEM_SPEC] *...  11.5 us
    unnamed x44, local copies, waits for them, and re-layouts  2.43 us
  transfers between devices with their start and end apart: 43, of which 21 were waited for; matrix products, arithmetic and copies ran while one was open for 0% of the time, Pallas kernels for 9%

profile of v4, /device:TPU:0, one launch (start us, length us, event | category | flops | bytes accessed | tf_op | source)
XLA Modules:
  0.0 76.2 jit_solution(17691150021464812464)
XLA Ops:
  0.6 5.1 %collective-permute-start.5 = (bf16[64,256]{1,0:T(8,128)(2,1)}, bf16[64,256]{1,0:T(8,128)(2,1)S(1)}, u32[]{:S(2)}, u32[]{:S(2)}) collective-permute-start(bf16[64,256]{1,0:T(8,128)(2,1)} %refs_0_.1), channel_id=1, source_target_pairs={{0,6},{1,7},{2,4},{3,5},{4,2},{5,3},{6,0},{7,1},{8,14},{9,15},{10,... | collective-permute-start | bytes 98312 | tf_op jit(solution)/shard_map/ppermute | solution.py:194
  7.9 2.0 %collective-permute-done.refs_2_ = bf16[64,256]{1,0:T(8,128)(2,1)S(1)} collective-permute-done((bf16[64,256]{1,0:T(8,128)(2,1)}, bf16[64,256]{1,0:T(8,128)(2,1)S(1)}, u32[]{:S(2)}, u32[]{:S(2)}) %collective-permute-start) | collective-permute-done | bytes 32800 | tf_op jit(solution)/shard_map/ppermute | solution.py:194
  11.6 1.7 %copy-done = bf16[2048,1408]{1,0:T(8,128)(2,1)S(1)} copy-done((bf16[2048,1408]{1,0:T(8,128)(2,1)S(1)}, bf16[2048,1408]{1,0:T(8,128)(2,1)}, u32[]{:S(2)}) %copy-start) | copy-done | bytes 5767192
  16.5 1.5 %collective-permute-start.8 = (bf16[64,256]{1,0:T(8,128)(2,1)S(1)}, bf16[64,256]{1,0:T(8,128)(2,1)S(1)}, u32[]{:S(2)}, u32[]{:S(2)}) collective-permute-start(bf16[64,256]{1,0:T(8,128)(2,1)S(1)} %get-tuple-element.49), channel_id=1, source_target_pairs={{0,2},{1,3},{2,0},{3,1},{4,6},{5,7},{6,4},{7,5},{8,10},{9,11},{10,... | collective-permute-start | bytes 98312 | tf_op jit(solution)/shard_map/ppermute | solution.py:194
  18.0 2.9 %collective-permute-start.9 = (bf16[64,256]{1,0:T(8,128)(2,1)S(1)}, bf16[64,256]{1,0:T(8,128)(2,1)S(1)}, u32[]{:S(2)}, u32[]{:S(2)}) collective-permute-start(bf16[64,256]{1,0:T(8,128)(2,1)S(1)} %get-tuple-element.50), channel_id=1, source_target_pairs={{0,4},{1,5},{2,6},{3,7},{4,0},{5,1},{6,2},{7,3},{8,12},{9,13},{10,... | collective-permute-start | bytes 98312 | tf_op jit(solution)/shard_map/ppermute | solution.py:194
  21.0 2.5 %collective-permute-done.9.refs_1_ = bf16[64,256]{1,0:T(8,128)(2,1)S(1)} collective-permute-done((bf16[64,256]{1,0:T(8,128)(2,1)S(1)}, bf16[64,256]{1,0:T(8,128)(2,1)S(1)}, u32[]{:S(2)}, u32[]{:S(2)}) %collective-permute-start.9) | collective-permute-done | bytes 32800 | tf_op jit(solution)/shard_map/ppermute | solution.py:194
  23.5 3.2 %collective-permute-done.10.refs_2_ = bf16[64,256]{1,0:T(8,128)(2,1)S(1)} collective-permute-done((bf16[64,256]{1,0:T(8,128)(2,1)S(1)}, bf16[64,256]{1,0:T(8,128)(2,1)S(1)}, u32[]{:S(2)}, u32[]{:S(2)}) %collective-permute-start.10) | collective-permute-done | bytes 32800 | tf_op jit(solution)/shard_map/ppermute | solution.py:194
  27.1 4.1 %collective-permute-start.13 = (bf16[64,256]{1,0:T(8,128)(2,1)S(1)}, bf16[64,256]{1,0:T(8,128)(2,1)S(1)}, u32[]{:S(2)}, u32[]{:S(2)}) collective-permute-start(bf16[64,256]{1,0:T(8,128)(2,1)S(1)} %shard_map.209.refs_0_.refs_9_), channel_id=1, source_target_pairs={{0,4},{1,5},{2,6},{3,7},{4,0},{5,1},{6,2},{7,3},{8,12},{9,13},{10,... | collective-permute-start | bytes 98312 | tf_op jit(solution)/shard_map/ppermute | solution.py:194
  31.2 1.3 %collective-permute-done.16.refs_4_ = bf16[64,256]{1,0:T(8,128)(2,1)S(1)} collective-permute-done((bf16[64,256]{1,0:T(8,128)(2,1)S(1)}, bf16[64,256]{1,0:T(8,128)(2,1)S(1)}, u32[]{:S(2)}, u32[]{:S(2)}) %collective-permute-start.16) | collective-permute-done | bytes 32800 | tf_op jit(solution)/shard_map/ppermute | solution.py:194
  35.7 2.1 %collective-permute-start.19 = (bf16[16,1024]{1,0:T(8,128)(2,1)S(1)}, bf16[16,1024]{1,0:T(8,128)(2,1)S(1)}, u32[]{:S(2)}, u32[]{:S(2)}) collective-permute-start(bf16[16,1024]{1,0:T(8,128)(2,1)S(1)} %get-tuple-element.57), channel_id=1, source_target_pairs={{0,4},{1,5},{2,6},{3,7},{4,0},{5,1},{6,2},{7,3},{8,12},{9,13},{10,... | collective-permute-start | bytes 98312 | tf_op jit(solution)/shard_map/ppermute | solution.py:194
  37.8 1.8 %collective-permute-start.20 = (bf16[16,1024]{1,0:T(8,128)(2,1)S(1)}, bf16[16,1024]{1,0:T(8,128)(2,1)S(1)}, u32[]{:S(2)}, u32[]{:S(2)}) collective-permute-start(bf16[16,1024]{1,0:T(8,128)(2,1)S(1)} %get-tuple-element.58), channel_id=1, source_target_pairs={{0,6},{1,7},{2,4},{3,5},{4,2},{5,3},{6,0},{7,1},{8,14},{9,15},{10,... | collective-permute-start | bytes 98312 | tf_op jit(solution)/shard_map/ppermute | solution.py:194
  40.5 3.0 %collective-permute-done.20.refs_3_ = bf16[16,1024]{1,0:T(8,128)(2,1)S(1)} collective-permute-done((bf16[16,1024]{1,0:T(8,128)(2,1)S(1)}, bf16[16,1024]{1,0:T(8,128)(2,1)S(1)}, u32[]{:S(2)}, u32[]{:S(2)}) %collective-permute-start.20) | collective-permute-done | bytes 32800 | tf_op jit(solution)/shard_map/ppermute | solution.py:194
  44.4 1.3 %shard_map.213 = (bf16[8,1024]{1,0:T(8,128)(2,1)S(1)}, f32[64,128]{1,0:T(8,128)S(1)}, f32[64,128]{1,0:T(8,128)S(1)}, f32[64,128]{1,0:T(8,128)S(1)}) custom-call(bf16[16,1024]{1,0:T(8,128)(2,1)S(1)} %get-tuple-element.55.refs_0_, bf16[16,1024]{1,0:T(8,128)(2,1)S(1)} %collective-permute-done.18.refs_1_, bf16[16,1024]{1,0:T(8,128)(2,1)S(1)} %collective-permute-done.19.refs_2_, ...), custom_call_target="tpu_custom_call" | custom-call | tf_op jit(solution)/shard_map/pallas_call | solution.py:178
  45.7 1.3 %shard_map.214 = (bf16[8,1024]{1,0:T(8,128)(2,1)S(1)}, f32[64,128]{1,0:T(8,128)S(1)}, f32[64,128]{1,0:T(8,128)S(1)}, f32[64,128]{1,0:T(8,128)S(1)}) custom-call(bf16[16,1024]{1,0:T(8,128)(2,1)S(1)} %collective-permute-done.21.refs_0_, bf16[16,1024]{1,0:T(8,128)(2,1)S(1)} %collective-permute-done.22.refs_1_, ...), custom_call_target="tpu_custom_call" | custom-call | tf_op jit(solution)/shard_map/pallas_call | solution.py:178
  47.3 2.2 %collective-permute-start.28 = (bf16[8,2048]{1,0:T(8,128)(2,1)S(1)}, bf16[8,2048]{1,0:T(8,128)(2,1)S(1)}, u32[]{:S(2)}, u32[]{:S(2)}) collective-permute-start(bf16[8,2048]{1,0:T(8,128)(2,1)S(1)} %shard_map.215.refs_0_), channel_id=1, source_target_pairs={{0,4},{1,5},{2,6},{3,7},{4,0},{5,1},{6,2},{7,3},{8,12},{9,13},{10,... | collective-permute-start | bytes 98312 | tf_op jit(solution)/shard_map/ppermute | solution.py:194
  49.5 2.0 %collective-permute-start.30 = (bf16[8,2048]{1,0:T(8,128)(2,1)S(1)}, bf16[8,2048]{1,0:T(8,128)(2,1)S(1)}, u32[]{:S(2)}, u32[]{:S(2)}) collective-permute-start(bf16[8,2048]{1,0:T(8,128)(2,1)S(1)} %shard_map.215.refs_0_), channel_id=1, source_target_pairs={{0,6},{1,7},{2,4},{3,5},{4,2},{5,3},{6,0},{7,1},{8,14},{9,15},{10,... | collective-permute-start | bytes 98312 | tf_op jit(solution)/shard_map/ppermute | solution.py:194
  52.3 2.9 %collective-permute-done.30.refs_6_ = bf16[8,2048]{1,0:T(8,128)(2,1)S(1)} collective-permute-done((bf16[8,2048]{1,0:T(8,128)(2,1)S(1)}, bf16[8,2048]{1,0:T(8,128)(2,1)S(1)}, u32[]{:S(2)}, u32[]{:S(2)}) %collective-permute-start.30) | collective-permute-done | bytes 32800 | tf_op jit(solution)/shard_map/ppermute | solution.py:194
  56.8 2.1 %collective-permute-start.37 = (bf16[64,256]{1,0:T(8,128)(2,1)S(1)}, bf16[64,256]{1,0:T(8,128)(2,1)S(1)}, u32[]{:S(2)}, u32[]{:S(2)}) collective-permute-start(bf16[64,256]{1,0:T(8,128)(2,1)S(1)} %shard_map.216.refs_0_.base_ref), channel_id=1, source_target_pairs={{0,6},{1,7},{2,4},{3,5},{4,2},{5,3},{6,0},{7,1},{8,14},{9,15},{10,... | collective-permute-start | bytes 98312 | tf_op jit(solution)/shard_map/ppermute | solution.py:194
  58.8 2.4 %collective-permute-start.34 = (bf16[64,256]{1,0:T(8,128)(2,1)S(1)}, bf16[64,256]{1,0:T(8,128)(2,1)S(1)}, u32[]{:S(2)}, u32[]{:S(2)}) collective-permute-start(bf16[64,256]{1,0:T(8,128)(2,1)S(1)} %shard_map.216.refs_0_.base_ref), channel_id=1, source_target_pairs={{0,4},{1,5},{2,6},{3,7},{4,0},{5,1},{6,2},{7,3},{8,12},{9,13},{10,... | collective-permute-start | bytes 98312 | tf_op jit(solution)/shard_map/ppermute | solution.py:194
  61.2 1.4 %collective-permute-done.37.refs_4_ = bf16[64,256]{1,0:T(8,128)(2,1)S(1)} collective-permute-done((bf16[64,256]{1,0:T(8,128)(2,1)S(1)}, bf16[64,256]{1,0:T(8,128)(2,1)S(1)}, u32[]{:S(2)}, u32[]{:S(2)}) %collective-permute-start.37) | collective-permute-done | bytes 32800 | tf_op jit(solution)/shard_map/ppermute | solution.py:194
  67.4 1.7 %collective-permute-start.40 = (bf16[64,256]{1,0:T(8,128)(2,1)S(1)}, bf16[64,256]{1,0:T(8,128)(2,1)S(1)}, u32[]{:S(2)}, u32[]{:S(2)}) collective-permute-start(bf16[64,256]{1,0:T(8,128)(2,1)S(1)} %get-tuple-element.71), channel_id=1, source_target_pairs={{0,2},{1,3},{2,0},{3,1},{4,6},{5,7},{6,4},{7,5},{8,10},{9,11},{10,... | collective-permute-start | bytes 98312 | tf_op jit(solution)/shard_map/ppermute | solution.py:194
  69.9 2.0 %collective-permute-start.42 = (bf16[64,256]{1,0:T(8,128)(2,1)S(1)}, bf16[64,256]{1,0:T(8,128)(2,1)S(1)}, u32[]{:S(2)}, u32[]{:S(2)}) collective-permute-start(bf16[64,256]{1,0:T(8,128)(2,1)S(1)} %get-tuple-element.73), channel_id=1, source_target_pairs={{0,6},{1,7},{2,4},{3,5},{4,2},{5,3},{6,0},{7,1},{8,14},{9,15},{10,... | collective-permute-start | bytes 98312 | tf_op jit(solution)/shard_map/ppermute | solution.py:194
  71.9 1.3 %shard_map.222 = f32[16,128,128]{2,1,0:T(8,128)} custom-call(f32[64,128]{1,0:T(8,128)S(1)} %get-tuple-element.74.refs_0_, f32[64,128]{1,0:T(8,128)S(1)} %get-tuple-element.75.refs_1_, f32[64,128]{1,0:T(8,128)S(1)} %get-tuple-element.76.refs_2_, f32[64,128]{1,0:T(8,128)S(1)} %get-tuple-element.77.refs_3_, f32[64,128]{1,0:T(8,128)S(1)} %get-tuple-element.78.refs_4_, ...), custom_call_target="tpu_custom_call" | custom-call | tf_op jit(solution)/shard_map/pallas_call | solution.py:178
  73.2 1.6 %collective-permute-done.41.refs_1_ = bf16[64,256]{1,0:T(8,128)(2,1)S(1)} collective-permute-done((bf16[64,256]{1,0:T(8,128)(2,1)S(1)}, bf16[64,256]{1,0:T(8,128)(2,1)S(1)}, u32[]{:S(2)}, u32[]{:S(2)}) %collective-permute-start.41) | collective-permute-done | bytes 32800 | tf_op jit(solution)/shard_map/ppermute | solution.py:194
  (131 shorter events, 21.0 us)
Async XLA Ops:
  0.6 7.2 %collective-permute-start.5 = (bf16[64,256]{1,0:T(8,128)(2,1)}, bf16[64,256]{1,0:T(8,128)(2,1)S(1)}, u32[]{:S(2)}, u32[]{:S(2)}) collective-permute-start(bf16[64,256]{1,0:T(8,128)(2,1)} %refs_0_.1), channel_id=1, source_target_pairs={{0,6},{1,7},{2,4},{3,5},{4,2},{5,3},{6,0},{7,1},{8,14},{9,15},{10,... | collective-permute-start | bytes 98312 | tf_op jit(solution)/shard_map/ppermute | solution.py:194
  5.8 5.1 %collective-permute-start.2 = (bf16[64,256]{1,0:T(8,128)(2,1)}, bf16[64,256]{1,0:T(8,128)(2,1)S(1)}, u32[]{:S(2)}, u32[]{:S(2)}) collective-permute-start(bf16[64,256]{1,0:T(8,128)(2,1)} %refs_0_.1), channel_id=1, source_target_pairs={{0,4},{1,5},{2,6},{3,7},{4,0},{5,1},{6,2},{7,3},{8,12},{9,13},{10,... | collective-permute-start | bytes 98312 | tf_op jit(solution)/shard_map/ppermute | solution.py:194
  9.9 4.3 %collective-permute-start.1 = (bf16[64,256]{1,0:T(8,128)(2,1)S(1)}, bf16[64,256]{1,0:T(8,128)(2,1)S(1)}, u32[]{:S(2)}, u32[]{:S(2)}) collective-permute-start(bf16[64,256]{1,0:T(8,128)(2,1)S(1)} %collective-permute-done.refs_2_), channel_id=1, source_target_pairs={{0,1},{1,0},{2,3},{3,2},{4,5},{5,4},{6,7},{7,6},{8,9},{9,8},{10,11... | collective-permute-start | bytes 98312 | tf_op jit(solution)/shard_map/ppermute | solution.py:194
  16.5 4.5 %collective-permute-start.8 = (bf16[64,256]{1,0:T(8,128)(2,1)S(1)}, bf16[64,256]{1,0:T(8,128)(2,1)S(1)}, u32[]{:S(2)}, u32[]{:S(2)}) collective-permute-start(bf16[64,256]{1,0:T(8,128)(2,1)S(1)} %get-tuple-element.49), channel_id=1, source_target_pairs={{0,2},{1,3},{2,0},{3,1},{4,6},{5,7},{6,4},{7,5},{8,10},{9,11},{10,... | collective-permute-start | bytes 98312 | tf_op jit(solution)/shard_map/ppermute | solution.py:194
  18.0 5.5 %collective-permute-start.9 = (bf16[64,256]{1,0:T(8,128)(2,1)S(1)}, bf16[64,256]{1,0:T(8,128)(2,1)S(1)}, u32[]{:S(2)}, u32[]{:S(2)}) collective-permute-start(bf16[64,256]{1,0:T(8,128)(2,1)S(1)} %get-tuple-element.50), channel_id=1, source_target_pairs={{0,4},{1,5},{2,6},{3,7},{4,0},{5,1},{6,2},{7,3},{8,12},{9,13},{10,... | collective-permute-start | bytes 98312 | tf_op jit(solution)/shard_map/ppermute | solution.py:194
  20.9 5.8 %collective-permute-start.10 = (bf16[64,256]{1,0:T(8,128)(2,1)S(1)}, bf16[64,256]{1,0:T(8,128)(2,1)S(1)}, u32[]{:S(2)}, u32[]{:S(2)}) collective-permute-start(bf16[64,256]{1,0:T(8,128)(2,1)S(1)} %get-tuple-element.51), channel_id=1, source_target_pairs={{0,6},{1,7},{2,4},{3,5},{4,2},{5,3},{6,0},{7,1},{8,14},{9,15},{10,... | collective-permute-start | bytes 98312 | tf_op jit(solution)/shard_map/ppermute | solution.py:194
  26.7 5.8 %collective-permute-start.16 = (bf16[64,256]{1,0:T(8,128)(2,1)S(1)}, bf16[64,256]{1,0:T(8,128)(2,1)S(1)}, u32[]{:S(2)}, u32[]{:S(2)}) collective-permute-start(bf16[64,256]{1,0:T(8,128)(2,1)S(1)} %shard_map.209.refs_0_.refs_9_), channel_id=1, source_target_pairs={{0,6},{1,7},{2,4},{3,5},{4,2},{5,3},{6,0},{7,1},{8,14},{9,15},{10,... | collective-permute-start | bytes 98312 | tf_op jit(solution)/shard_map/ppermute | solution.py:194
  27.1 5.5 %collective-permute-start.11 = (bf16[64,256]{1,0:T(8,128)(2,1)S(1)}, bf16[64,256]{1,0:T(8,128)(2,1)S(1)}, u32[]{:S(2)}, u32[]{:S(2)}) collective-permute-start(bf16[64,256]{1,0:T(8,128)(2,1)S(1)} %shard_map.209.refs_0_.refs_9_), channel_id=1, source_target_pairs={{0,2},{1,3},{2,0},{3,1},{4,6},{5,7},{6,4},{7,5},{8,10},{9,11},{10,... | collective-permute-start | bytes 98312 | tf_op jit(solution)/shard_map/ppermute | solution.py:194
  27.1 6.0 %collective-permute-start.13 = (bf16[64,256]{1,0:T(8,128)(2,1)S(1)}, bf16[64,256]{1,0:T(8,128)(2,1)S(1)}, u32[]{:S(2)}, u32[]{:S(2)}) collective-permute-start(bf16[64,256]{1,0:T(8,128)(2,1)S(1)} %shard_map.209.refs_0_.refs_9_), channel_id=1, source_target_pairs={{0,4},{1,5},{2,6},{3,7},{4,0},{5,1},{6,2},{7,3},{8,12},{9,13},{10,... | collective-permute-start | bytes 98312 | tf_op jit(solution)/shard_map/ppermute | solution.py:194
  35.2 4.5 %collective-permute-start.18 = (bf16[16,1024]{1,0:T(8,128)(2,1)S(1)}, bf16[16,1024]{1,0:T(8,128)(2,1)S(1)}, u32[]{:S(2)}, u32[]{:S(2)}) collective-permute-start(bf16[16,1024]{1,0:T(8,128)(2,1)S(1)} %get-tuple-element.56), channel_id=1, source_target_pairs={{0,2},{1,3},{2,0},{3,1},{4,6},{5,7},{6,4},{7,5},{8,10},{9,11},{10,... | collective-permute-start | bytes 98312 | tf_op jit(solution)/shard_map/ppermute | solution.py:194
  35.7 4.8 %collective-permute-start.19 = (bf16[16,1024]{1,0:T(8,128)(2,1)S(1)}, bf16[16,1024]{1,0:T(8,128)(2,1)S(1)}, u32[]{:S(2)}, u32[]{:S(2)}) collective-permute-start(bf16[16,1024]{1,0:T(8,128)(2,1)S(1)} %get-tuple-element.57), channel_id=1, source_target_pairs={{0,4},{1,5},{2,6},{3,7},{4,0},{5,1},{6,2},{7,3},{8,12},{9,13},{10,... | collective-permute-start | bytes 98312 | tf_op jit(solution)/shard_map/ppermute | solution.py:194
  37.8 5.7 %collective-permute-start.20 = (bf16[16,1024]{1,0:T(8,128)(2,1)S(1)}, bf16[16,1024]{1,0:T(8,128)(2,1)S(1)}, u32[]{:S(2)}, u32[]{:S(2)}) collective-permute-start(bf16[16,1024]{1,0:T(8,128)(2,1)S(1)} %get-tuple-element.58), channel_id=1, source_target_pairs={{0,6},{1,7},{2,4},{3,5},{4,2},{5,3},{6,0},{7,1},{8,14},{9,15},{10,... | collective-permute-start | bytes 98312 | tf_op jit(solution)/shard_map/ppermute | solution.py:194
  39.6 6.1 %collective-permute-start.21 = (bf16[16,1024]{1,0:T(8,128)(2,1)S(1)}, bf16[16,1024]{1,0:T(8,128)(2,1)S(1)}, u32[]{:S(2)}, u32[]{:S(2)}) collective-permute-start(bf16[16,1024]{1,0:T(8,128)(2,1)S(1)} %get-tuple-element.55.refs_0_), channel_id=1, source_target_pairs={{0,1},{1,0},{2,3},{3,2},{4,5},{5,4},{6,7},{7,6},{8,9},{9,8},{10,11... | collective-permute-start | bytes 98312 | tf_op jit(solution)/shard_map/ppermute | solution.py:194
  39.6 6.1 %collective-permute-start.22 = (bf16[16,1024]{1,0:T(8,128)(2,1)S(1)}, bf16[16,1024]{1,0:T(8,128)(2,1)S(1)}, u32[]{:S(2)}, u32[]{:S(2)}) collective-permute-start(bf16[16,1024]{1,0:T(8,128)(2,1)S(1)} %collective-permute-done.18.refs_1_), channel_id=1, source_target_pairs={{0,1},{1,0},{2,3},{3,2},{4,5},{5,4},{6,7},{7,6},{8,9},{9,8},{10,11... | collective-permute-start | bytes 98312 | tf_op jit(solution)/shard_map/ppermute | solution.py:194
  40.5 5.2 %collective-permute-start.23 = (bf16[16,1024]{1,0:T(8,128)(2,1)S(1)}, bf16[16,1024]{1,0:T(8,128)(2,1)S(1)}, u32[]{:S(2)}, u32[]{:S(2)}) collective-permute-start(bf16[16,1024]{1,0:T(8,128)(2,1)S(1)} %collective-permute-done.19.refs_2_), channel_id=1, source_target_pairs={{0,1},{1,0},{2,3},{3,2},{4,5},{5,4},{6,7},{7,6},{8,9},{9,8},{10,11... | collective-permute-start | bytes 98312 | tf_op jit(solution)/shard_map/ppermute | solution.py:194
  47.1 4.5 %collective-permute-start.26 = (bf16[8,2048]{1,0:T(8,128)(2,1)S(1)}, bf16[8,2048]{1,0:T(8,128)(2,1)S(1)}, u32[]{:S(2)}, u32[]{:S(2)}) collective-permute-start(bf16[8,2048]{1,0:T(8,128)(2,1)S(1)} %shard_map.215.refs_0_), channel_id=1, source_target_pairs={{0,2},{1,3},{2,0},{3,1},{4,6},{5,7},{6,4},{7,5},{8,10},{9,11},{10,... | collective-permute-start | bytes 98312 | tf_op jit(solution)/shard_map/ppermute | solution.py:194
  47.3 5.1 %collective-permute-start.28 = (bf16[8,2048]{1,0:T(8,128)(2,1)S(1)}, bf16[8,2048]{1,0:T(8,128)(2,1)S(1)}, u32[]{:S(2)}, u32[]{:S(2)}) collective-permute-start(bf16[8,2048]{1,0:T(8,128)(2,1)S(1)} %shard_map.215.refs_0_), channel_id=1, source_target_pairs={{0,4},{1,5},{2,6},{3,7},{4,0},{5,1},{6,2},{7,3},{8,12},{9,13},{10,... | collective-permute-start | bytes 98312 | tf_op jit(solution)/shard_map/ppermute | solution.py:194
  49.5 5.7 %collective-permute-start.30 = (bf16[8,2048]{1,0:T(8,128)(2,1)S(1)}, bf16[8,2048]{1,0:T(8,128)(2,1)S(1)}, u32[]{:S(2)}, u32[]{:S(2)}) collective-permute-start(bf16[8,2048]{1,0:T(8,128)(2,1)S(1)} %shard_map.215.refs_0_), channel_id=1, source_target_pairs={{0,6},{1,7},{2,4},{3,5},{4,2},{5,3},{6,0},{7,1},{8,14},{9,15},{10,... | collective-permute-start | bytes 98312 | tf_op jit(solution)/shard_map/ppermute | solution.py:194
  56.8 5.8 %collective-permute-start.37 = (bf16[64,256]{1,0:T(8,128)(2,1)S(1)}, bf16[64,256]{1,0:T(8,128)(2,1)S(1)}, u32[]{:S(2)}, u32[]{:S(2)}) collective-permute-start(bf16[64,256]{1,0:T(8,128)(2,1)S(1)} %shard_map.216.refs_0_.base_ref), channel_id=1, source_target_pairs={{0,6},{1,7},{2,4},{3,5},{4,2},{5,3},{6,0},{7,1},{8,14},{9,15},{10,... | collective-permute-start | bytes 98312 | tf_op jit(solution)/shard_map/ppermute | solution.py:194
  58.8 4.4 %collective-permute-start.32 = (bf16[64,256]{1,0:T(8,128)(2,1)S(1)}, bf16[64,256]{1,0:T(8,128)(2,1)S(1)}, u32[]{:S(2)}, u32[]{:S(2)}) collective-permute-start(bf16[64,256]{1,0:T(8,128)(2,1)S(1)} %shard_map.216.refs_0_.base_ref), channel_id=1, source_target_pairs={{0,2},{1,3},{2,0},{3,1},{4,6},{5,7},{6,4},{7,5},{8,10},{9,11},{10,... | collective-permute-start | bytes 98312 | tf_op jit(solution)/shard_map/ppermute | solution.py:194
  58.8 5.2 %collective-permute-start.34 = (bf16[64,256]{1,0:T(8,128)(2,1)S(1)}, bf16[64,256]{1,0:T(8,128)(2,1)S(1)}, u32[]{:S(2)}, u32[]{:S(2)}) collective-permute-start(bf16[64,256]{1,0:T(8,128)(2,1)S(1)} %shard_map.216.refs_0_.base_ref), channel_id=1, source_target_pairs={{0,4},{1,5},{2,6},{3,7},{4,0},{5,1},{6,2},{7,3},{8,12},{9,13},{10,... | collective-permute-start | bytes 98312 | tf_op jit(solution)/shard_map/ppermute | solution.py:194
  67.4 5.8 %collective-permute-start.40 = (bf16[64,256]{1,0:T(8,128)(2,1)S(1)}, bf16[64,256]{1,0:T(8,128)(2,1)S(1)}, u32[]{:S(2)}, u32[]{:S(2)}) collective-permute-start(bf16[64,256]{1,0:T(8,128)(2,1)S(1)} %get-tuple-element.71), channel_id=1, source_target_pairs={{0,2},{1,3},{2,0},{3,1},{4,6},{5,7},{6,4},{7,5},{8,10},{9,11},{10,... | collective-permute-start | bytes 98312 | tf_op jit(solution)/shard_map/ppermute | solution.py:194
  69.1 5.6 %collective-permute-start.41 = (bf16[64,256]{1,0:T(8,128)(2,1)S(1)}, bf16[64,256]{1,0:T(8,128)(2,1)S(1)}, u32[]{:S(2)}, u32[]{:S(2)}) collective-permute-start(bf16[64,256]{1,0:T(8,128)(2,1)S(1)} %get-tuple-element.72), channel_id=1, source_target_pairs={{0,4},{1,5},{2,6},{3,7},{4,0},{5,1},{6,2},{7,3},{8,12},{9,13},{10,... | collective-permute-start | bytes 98312 | tf_op jit(solution)/shard_map/ppermute | solution.py:194
  69.9 5.7 %collective-permute-start.42 = (bf16[64,256]{1,0:T(8,128)(2,1)S(1)}, bf16[64,256]{1,0:T(8,128)(2,1)S(1)}, u32[]{:S(2)}, u32[]{:S(2)}) collective-permute-start(bf16[64,256]{1,0:T(8,128)(2,1)S(1)} %get-tuple-element.73), channel_id=1, source_target_pairs={{0,6},{1,7},{2,4},{3,5},{4,2},{5,3},{6,0},{7,1},{8,14},{9,15},{10,... | collective-permute-start | bytes 98312 | tf_op jit(solution)/shard_map/ppermute | solution.py:194
  (41 other events, 544.2 us)

commit v5 on v4

--- a/solution.py
+++ b/solution.py
@@ -501,74 +501,69 @@
             for head in range(per_block):
                 column = place * width + head * size
                 found.append(block[:, column : column + size])
-        return jnp.concatenate(found, axis=0)
+        return jnp.stack(found)
 
     def head_at(head):
         return (index ^ masks[head // per_block]) * per_block + head % per_block
 
+    def lane_sum(array):
+        return jnp.sum(array, axis=-1, keepdims=True)
+
     query, key_in, value, gating = (stack(place) for place in range(4))
-    query_unit = query * lax.rsqrt(jnp.sum(query * query, axis=1, keepdims=True) + EPSILON) * (1.0 / math.sqrt(size))
-    key_unit = key_in * lax.rsqrt(jnp.sum(key_in * key_in, axis=1, keepdims=True) + EPSILON)
+    query_unit = query * lax.rsqrt(lane_sum(query * query) + EPSILON) * (1.0 / math.sqrt(size))
+    key_unit = key_in * lax.rsqrt(lane_sum(key_in * key_in) + EPSILON)
     step_of = lax.broadcasted_iota(jnp.int32, (BLK, all_heads), 0)
+    head_of = lax.broadcasted_iota(jnp.int32, (BLK, all_heads), 1)
     live = live_ref[...]
     pre = pre_ref[...]
     write_gate = jax.nn.sigmoid(pre[:, :all_heads]) * live
     forget_in = pre[:, all_heads:]
     softplus = jnp.maximum(forget_in, 0.0) + jnp.log1p(jnp.exp(-jnp.abs(forget_in)))
-    forget = -jnp.exp(rate_ref[...]) * softplus * live
-    cumulative = forget
+    cumulative = -jnp.exp(rate_ref[...]) * softplus * live
     lower = 1
     while lower < BLK:
         moved = pltpu.roll(cumulative, lower, 0)
         cumulative = cumulative + jnp.where(step_of >= lower, moved, 0.0)
         lower *= 2
-    final = jnp.broadcast_to(cumulative[BLK - 1 :, :], (BLK, all_heads))
-    head_of = lax.broadcasted_iota(jnp.int32, (BLK, all_heads), 1)
-    picked = jnp.concatenate([head_of == head_at(head) for head in range(heads)], axis=0)
-
-    def column_of(array):
-        tall = jnp.concatenate([array] * heads, axis=0)
-        return jnp.sum(jnp.where(picked, tall, 0.0), axis=1, keepdims=True)
-
-    write_col, live_col = column_of(write_gate), column_of(live)
-    cum_col, final_col = column_of(cumulative), column_of(final)
-    down_at = lax.broadcasted_iota(jnp.int32, (rows, rows), 0)
-    over_at = lax.broadcasted_iota(jnp.int32, (rows, rows), 1)
-    same = (down_at // BLK) == (over_at // BLK)
-    diagonal = down_at == over_at
-    cum_row = jnp.sum(jnp.where(diagonal, cum_col, 0.0), axis=0, keepdims=True)
-    causal = same & (down_at >= over_at)
-    decay = jnp.where(causal, jnp.exp(jnp.minimum(cum_col - cum_row, 0.0)), 0.0)
-    across = (((1,), (1,)), ((), ()))
-    key_parts = parts(key_unit)
-    strict_part = jnp.where(diagonal, 0.0, write_col * decay * dot_parts(key_parts, key_parts, across))
-    scores = decay * dot_parts(parts(query_unit), key_parts, across)
-    identity = diagonal.astype(F32)
-    strict_split = parts(strict_part)
-    squared = dot_parts(strict_split, strict_split)
-    squared_split = parts(squared)
-    fourth = dot_parts(squared_split, squared_split)
-    inverse = identity - strict_part + squared - dot_parts(strict_split, squared_split)
-    inverse = inverse + dot_parts(parts(inverse), parts(fourth))
-    growth = jnp.exp(cum_col)
+
+    def columns_of(array):
+        found = [lane_sum(jnp.where(head_of == head_at(head), array, 0.0)) for head in range(heads)]
+        return jnp.broadcast_to(jnp.stack(found), (heads, BLK, size))
+
+    write_col, cum = columns_of(write_gate), columns_of(cumulative)
+    live_col = live[:, :1][None]
+    growth = jnp.exp(cum)
     key_grown, query_grown = key_unit * growth, query_unit * growth
     from_key, from_query = [], []
     for head in range(heads):
-        at = slice(head * BLK, (head + 1) * BLK)
-        both = jnp.concatenate([key_grown[at], query_grown[at]], axis=0)
+        both = jnp.concatenate([key_grown[head], query_grown[head]], axis=0)
         found = dot_parts(parts(both), (high_ref[head_at(head)], low_ref[head_at(head)]))
         from_key.append(found[:BLK])
         from_query.append(found[BLK:])
-    target = write_col * (value - jnp.concatenate(from_key, axis=0))
-    update = dot_parts(parts(inverse), parts(target))
-    attend = jnp.concatenate(from_query, axis=0) + dot_parts(parts(scores), parts(update))
-    normed = attend * lax.rsqrt(jnp.mean(attend * attend, axis=1, keepdims=True) + EPSILON)
+    update = write_col * (value - jnp.stack(from_key))
+    attend = jnp.stack(from_query)
+    row_at = lax.broadcasted_iota(jnp.int32, (heads, BLK, size), 1)
+    for step in range(BLK):
+
+        def row_of(array):
+            return jnp.broadcast_to(array[:, step : step + 1, :], array.shape)
+
+        key_row = row_of(key_unit)
+        decay = jnp.exp(jnp.minimum(cum - row_of(cum), 0.0))
+        score = jnp.where(row_at >= step, decay * lane_sum(query_unit * key_row), 0.0)
+        update_row = row_of(update)
+        attend = attend + score * update_row
+        if step < BLK - 1:
+            strict = jnp.where(row_at > step, write_col * decay * lane_sum(key_unit * key_row), 0.0)
+            update = update - strict * update_row
+    normed = attend * lax.rsqrt(lane_sum(attend * attend) / size + EPSILON)
     normed = (normed * (gating * jax.nn.sigmoid(gating)) * live_col).astype(BF16)
+    final = jnp.broadcast_to(cum[:, BLK - 1 :, :], cum.shape)
     for head in range(heads):
-        mixed_ref[:, head * size : (head + 1) * size] = normed[head * BLK : (head + 1) * BLK]
-    update_ref[...] = update
-    faded_ref[...] = key_unit * jnp.exp(final_col - cum_col)
-    final_ref[...] = jnp.broadcast_to(jnp.exp(final_col), final_ref.shape)
+        mixed_ref[:, head * size : (head + 1) * size] = normed[head]
+    update_ref[...] = update.reshape(rows, size)
+    faded_ref[...] = (key_unit * jnp.exp(final - cum)).reshape(rows, size)
+    final_ref[...] = jnp.exp(final).reshape(rows, size)
 
 
 def join_kernel(count, first_ref, second_ref, mixed_ref):

time: 76.4 us -> 75.5 us (0.988)
  Pallas kernels: 11.5 us -> 10.6 us
    pallas_call x20, Pallas kernels: 11.5 us -> 10.6 us  [call(): pl.pallas_call(body, out_shape=shapes, in_specs=in_specs or [VMEM_SPEC] *...]
where the time goes in v5:
time: 75.5 us; the launch traced here: 75.3 us
  starting transfers between devices  34.6 us (46%)
  waiting for transfers between devices  25.8 us (34%)
  Pallas kernels  10.6 us (14%)
  local copies, waits for them, and re-layouts  2.43 us (3%)
  between operations  1.82 us (2%)
    ppermute x43, starting transfers between devices, swap(): return lax.ppermute(value, GROUP, [(i, i ^ mask) for i in range(count)])  34.6 us
    ppermute x43, waiting for transfers between devices, swap(): return lax.ppermute(value, GROUP, [(i, i ^ mask) for i in range(count)])  25.8 us
    pallas_call x20, Pallas kernels, call(): pl.pallas_call(body, out_shape=shapes, in_specs=in_specs or [VMEM_SPEC] *...  10.6 us
    unnamed x44, local copies, waits for them, and re-layouts  2.43 us
  transfers between devices with their start and end apart: 43, of which 21 were waited for; matrix products, arithmetic and copies ran while one was open for 0% of the time, Pallas kernels for 9%

profile of v5, /device:TPU:0, one launch (start us, length us, event | category | flops | bytes accessed | tf_op | source)
XLA Modules:
  0.0 75.3 jit_solution(14882194889417976192)
XLA Ops:
  0.6 5.1 %collective-permute-start.5 = (bf16[64,256]{1,0:T(8,128)(2,1)}, bf16[64,256]{1,0:T(8,128)(2,1)S(1)}, u32[]{:S(2)}, u32[]{:S(2)}) collective-permute-start(bf16[64,256]{1,0:T(8,128)(2,1)} %refs_0_.1), channel_id=1, source_target_pairs={{0,6},{1,7},{2,4},{3,5},{4,2},{5,3},{6,0},{7,1},{8,14},{9,15},{10,... | collective-permute-start | bytes 98312 | tf_op jit(solution)/shard_map/ppermute | solution.py:194
  7.9 2.0 %collective-permute-done.refs_2_ = bf16[64,256]{1,0:T(8,128)(2,1)S(1)} collective-permute-done((bf16[64,256]{1,0:T(8,128)(2,1)}, bf16[64,256]{1,0:T(8,128)(2,1)S(1)}, u32[]{:S(2)}, u32[]{:S(2)}) %collective-permute-start) | collective-permute-done | bytes 32800 | tf_op jit(solution)/shard_map/ppermute | solution.py:194
  9.9 1.0 %collective-permute-done.2.refs_3_ = bf16[64,256]{1,0:T(8,128)(2,1)S(1)} collective-permute-done((bf16[64,256]{1,0:T(8,128)(2,1)}, bf16[64,256]{1,0:T(8,128)(2,1)S(1)}, u32[]{:S(2)}, u32[]{:S(2)}) %collective-permute-start.2) | collective-permute-done | bytes 32800 | tf_op jit(solution)/shard_map/ppermute | solution.py:194
  11.6 1.7 %copy-done = bf16[2048,1408]{1,0:T(8,128)(2,1)S(1)} copy-done((bf16[2048,1408]{1,0:T(8,128)(2,1)S(1)}, bf16[2048,1408]{1,0:T(8,128)(2,1)}, u32[]{:S(2)}) %copy-start) | copy-done | bytes 5767192
  16.5 1.5 %collective-permute-start.8 = (bf16[64,256]{1,0:T(8,128)(2,1)S(1)}, bf16[64,256]{1,0:T(8,128)(2,1)S(1)}, u32[]{:S(2)}, u32[]{:S(2)}) collective-permute-start(bf16[64,256]{1,0:T(8,128)(2,1)S(1)} %get-tuple-element.49), channel_id=1, source_target_pairs={{0,2},{1,3},{2,0},{3,1},{4,6},{5,7},{6,4},{7,5},{8,10},{9,11},{10,... | collective-permute-start | bytes 98312 | tf_op jit(solution)/shard_map/ppermute | solution.py:194
  18.0 2.9 %collective-permute-start.9 = (bf16[64,256]{1,0:T(8,128)(2,1)S(1)}, bf16[64,256]{1,0:T(8,128)(2,1)S(1)}, u32[]{:S(2)}, u32[]{:S(2)}) collective-permute-start(bf16[64,256]{1,0:T(8,128)(2,1)S(1)} %get-tuple-element.50), channel_id=1, source_target_pairs={{0,4},{1,5},{2,6},{3,7},{4,0},{5,1},{6,2},{7,3},{8,12},{9,13},{10,... | collective-permute-start | bytes 98312 | tf_op jit(solution)/shard_map/ppermute | solution.py:194
  21.0 2.5 %collective-permute-done.9.refs_1_ = bf16[64,256]{1,0:T(8,128)(2,1)S(1)} collective-permute-done((bf16[64,256]{1,0:T(8,128)(2,1)S(1)}, bf16[64,256]{1,0:T(8,128)(2,1)S(1)}, u32[]{:S(2)}, u32[]{:S(2)}) %collective-permute-start.9) | collective-permute-done | bytes 32800 | tf_op jit(solution)/shard_map/ppermute | solution.py:194
  23.5 3.2 %collective-permute-done.10.refs_2_ = bf16[64,256]{1,0:T(8,128)(2,1)S(1)} collective-permute-done((bf16[64,256]{1,0:T(8,128)(2,1)S(1)}, bf16[64,256]{1,0:T(8,128)(2,1)S(1)}, u32[]{:S(2)}, u32[]{:S(2)}) %collective-permute-start.10) | collective-permute-done | bytes 32800 | tf_op jit(solution)/shard_map/ppermute | solution.py:194
  27.1 4.1 %collective-permute-start.13 = (bf16[64,256]{1,0:T(8,128)(2,1)S(1)}, bf16[64,256]{1,0:T(8,128)(2,1)S(1)}, u32[]{:S(2)}, u32[]{:S(2)}) collective-permute-start(bf16[64,256]{1,0:T(8,128)(2,1)S(1)} %shard_map.209.refs_0_.refs_9_), channel_id=1, source_target_pairs={{0,4},{1,5},{2,6},{3,7},{4,0},{5,1},{6,2},{7,3},{8,12},{9,13},{10,... | collective-permute-start | bytes 98312 | tf_op jit(solution)/shard_map/ppermute | solution.py:194
  31.2 1.3 %collective-permute-done.16.refs_4_ = bf16[64,256]{1,0:T(8,128)(2,1)S(1)} collective-permute-done((bf16[64,256]{1,0:T(8,128)(2,1)S(1)}, bf16[64,256]{1,0:T(8,128)(2,1)S(1)}, u32[]{:S(2)}, u32[]{:S(2)}) %collective-permute-start.16) | collective-permute-done | bytes 32800 | tf_op jit(solution)/shard_map/ppermute | solution.py:194
  35.7 2.1 %collective-permute-start.19 = (bf16[16,1024]{1,0:T(8,128)(2,1)S(1)}, bf16[16,1024]{1,0:T(8,128)(2,1)S(1)}, u32[]{:S(2)}, u32[]{:S(2)}) collective-permute-start(bf16[16,1024]{1,0:T(8,128)(2,1)S(1)} %get-tuple-element.57), channel_id=1, source_target_pairs={{0,4},{1,5},{2,6},{3,7},{4,0},{5,1},{6,2},{7,3},{8,12},{9,13},{10,... | collective-permute-start | bytes 98312 | tf_op jit(solution)/shard_map/ppermute | solution.py:194
  37.8 1.8 %collective-permute-start.20 = (bf16[16,1024]{1,0:T(8,128)(2,1)S(1)}, bf16[16,1024]{1,0:T(8,128)(2,1)S(1)}, u32[]{:S(2)}, u32[]{:S(2)}) collective-permute-start(bf16[16,1024]{1,0:T(8,128)(2,1)S(1)} %get-tuple-element.58), channel_id=1, source_target_pairs={{0,6},{1,7},{2,4},{3,5},{4,2},{5,3},{6,0},{7,1},{8,14},{9,15},{10,... | collective-permute-start | bytes 98312 | tf_op jit(solution)/shard_map/ppermute | solution.py:194
  40.5 3.0 %collective-permute-done.20.refs_3_ = bf16[16,1024]{1,0:T(8,128)(2,1)S(1)} collective-permute-done((bf16[16,1024]{1,0:T(8,128)(2,1)S(1)}, bf16[16,1024]{1,0:T(8,128)(2,1)S(1)}, u32[]{:S(2)}, u32[]{:S(2)}) %collective-permute-start.20) | collective-permute-done | bytes 32800 | tf_op jit(solution)/shard_map/ppermute | solution.py:194
  46.4 2.2 %collective-permute-start.28 = (bf16[8,2048]{1,0:T(8,128)(2,1)S(1)}, bf16[8,2048]{1,0:T(8,128)(2,1)S(1)}, u32[]{:S(2)}, u32[]{:S(2)}) collective-permute-start(bf16[8,2048]{1,0:T(8,128)(2,1)S(1)} %shard_map.215.refs_0_), channel_id=1, source_target_pairs={{0,4},{1,5},{2,6},{3,7},{4,0},{5,1},{6,2},{7,3},{8,12},{9,13},{10,... | collective-permute-start | bytes 98312 | tf_op jit(solution)/shard_map/ppermute | solution.py:194
  48.6 2.0 %collective-permute-start.30 = (bf16[8,2048]{1,0:T(8,128)(2,1)S(1)}, bf16[8,2048]{1,0:T(8,128)(2,1)S(1)}, u32[]{:S(2)}, u32[]{:S(2)}) collective-permute-start(bf16[8,2048]{1,0:T(8,128)(2,1)S(1)} %shard_map.215.refs_0_), channel_id=1, source_target_pairs={{0,6},{1,7},{2,4},{3,5},{4,2},{5,3},{6,0},{7,1},{8,14},{9,15},{10,... | collective-permute-start | bytes 98312 | tf_op jit(solution)/shard_map/ppermute | solution.py:194
  51.4 2.9 %collective-permute-done.30.refs_6_ = bf16[8,2048]{1,0:T(8,128)(2,1)S(1)} collective-permute-done((bf16[8,2048]{1,0:T(8,128)(2,1)S(1)}, bf16[8,2048]{1,0:T(8,128)(2,1)S(1)}, u32[]{:S(2)}, u32[]{:S(2)}) %collective-permute-start.30) | collective-permute-done | bytes 32800 | tf_op jit(solution)/shard_map/ppermute | solution.py:194
  54.3 1.2 %collective-permute-done.31.refs_7_ = bf16[8,2048]{1,0:T(8,128)(2,1)S(1)} collective-permute-done((bf16[8,2048]{1,0:T(8,128)(2,1)S(1)}, bf16[8,2048]{1,0:T(8,128)(2,1)S(1)}, u32[]{:S(2)}, u32[]{:S(2)}) %collective-permute-start.31) | collective-permute-done | bytes 32800 | tf_op jit(solution)/shard_map/ppermute | solution.py:194
  55.8 2.1 %collective-permute-start.37 = (bf16[64,256]{1,0:T(8,128)(2,1)S(1)}, bf16[64,256]{1,0:T(8,128)(2,1)S(1)}, u32[]{:S(2)}, u32[]{:S(2)}) collective-permute-start(bf16[64,256]{1,0:T(8,128)(2,1)S(1)} %shard_map.216.refs_0_.base_ref), channel_id=1, source_target_pairs={{0,6},{1,7},{2,4},{3,5},{4,2},{5,3},{6,0},{7,1},{8,14},{9,15},{10,... | collective-permute-start | bytes 98312 | tf_op jit(solution)/shard_map/ppermute | solution.py:194
  57.9 2.4 %collective-permute-start.34 = (bf16[64,256]{1,0:T(8,128)(2,1)S(1)}, bf16[64,256]{1,0:T(8,128)(2,1)S(1)}, u32[]{:S(2)}, u32[]{:S(2)}) collective-permute-start(bf16[64,256]{1,0:T(8,128)(2,1)S(1)} %shard_map.216.refs_0_.base_ref), channel_id=1, source_target_pairs={{0,4},{1,5},{2,6},{3,7},{4,0},{5,1},{6,2},{7,3},{8,12},{9,13},{10,... | collective-permute-start | bytes 98312 | tf_op jit(solution)/shard_map/ppermute | solution.py:194
  60.3 1.4 %collective-permute-done.37.refs_4_ = bf16[64,256]{1,0:T(8,128)(2,1)S(1)} collective-permute-done((bf16[64,256]{1,0:T(8,128)(2,1)S(1)}, bf16[64,256]{1,0:T(8,128)(2,1)S(1)}, u32[]{:S(2)}, u32[]{:S(2)}) %collective-permute-start.37) | collective-permute-done | bytes 32800 | tf_op jit(solution)/shard_map/ppermute | solution.py:194
  66.5 1.7 %collective-permute-start.40 = (bf16[64,256]{1,0:T(8,128)(2,1)S(1)}, bf16[64,256]{1,0:T(8,128)(2,1)S(1)}, u32[]{:S(2)}, u32[]{:S(2)}) collective-permute-start(bf16[64,256]{1,0:T(8,128)(2,1)S(1)} %get-tuple-element.71), channel_id=1, source_target_pairs={{0,2},{1,3},{2,0},{3,1},{4,6},{5,7},{6,4},{7,5},{8,10},{9,11},{10,... | collective-permute-start | bytes 98312 | tf_op jit(solution)/shard_map/ppermute | solution.py:194
  68.9 2.0 %collective-permute-start.42 = (bf16[64,256]{1,0:T(8,128)(2,1)S(1)}, bf16[64,256]{1,0:T(8,128)(2,1)S(1)}, u32[]{:S(2)}, u32[]{:S(2)}) collective-permute-start(bf16[64,256]{1,0:T(8,128)(2,1)S(1)} %get-tuple-element.73), channel_id=1, source_target_pairs={{0,6},{1,7},{2,4},{3,5},{4,2},{5,3},{6,0},{7,1},{8,14},{9,15},{10,... | collective-permute-start | bytes 98312 | tf_op jit(solution)/shard_map/ppermute | solution.py:194
  70.9 1.3 %shard_map.222 = f32[16,128,128]{2,1,0:T(8,128)} custom-call(f32[64,128]{1,0:T(8,128)S(1)} %get-tuple-element.74.refs_0_, f32[64,128]{1,0:T(8,128)S(1)} %get-tuple-element.75.refs_1_, f32[64,128]{1,0:T(8,128)S(1)} %get-tuple-element.76.refs_2_, f32[64,128]{1,0:T(8,128)S(1)} %get-tuple-element.77.refs_3_, f32[64,128]{1,0:T(8,128)S(1)} %get-tuple-element.78.refs_4_, ...), custom_call_target="tpu_custom_call" | custom-call | tf_op jit(solution)/shard_map/pallas_call | solution.py:178
  72.3 1.6 %collective-permute-done.41.refs_1_ = bf16[64,256]{1,0:T(8,128)(2,1)S(1)} collective-permute-done((bf16[64,256]{1,0:T(8,128)(2,1)S(1)}, bf16[64,256]{1,0:T(8,128)(2,1)S(1)}, u32[]{:S(2)}, u32[]{:S(2)}) %collective-permute-start.41) | collective-permute-done | bytes 32800 | tf_op jit(solution)/shard_map/ppermute | solution.py:194
  (131 shorter events, 20.4 us)
Async XLA Ops:
  0.6 7.2 %collective-permute-start.5 = (bf16[64,256]{1,0:T(8,128)(2,1)}, bf16[64,256]{1,0:T(8,128)(2,1)S(1)}, u32[]{:S(2)}, u32[]{:S(2)}) collective-permute-start(bf16[64,256]{1,0:T(8,128)(2,1)} %refs_0_.1), channel_id=1, source_target_pairs={{0,6},{1,7},{2,4},{3,5},{4,2},{5,3},{6,0},{7,1},{8,14},{9,15},{10,... | collective-permute-start | bytes 98312 | tf_op jit(solution)/shard_map/ppermute | solution.py:194
  5.8 5.1 %collective-permute-start.2 = (bf16[64,256]{1,0:T(8,128)(2,1)}, bf16[64,256]{1,0:T(8,128)(2,1)S(1)}, u32[]{:S(2)}, u32[]{:S(2)}) collective-permute-start(bf16[64,256]{1,0:T(8,128)(2,1)} %refs_0_.1), channel_id=1, source_target_pairs={{0,4},{1,5},{2,6},{3,7},{4,0},{5,1},{6,2},{7,3},{8,12},{9,13},{10,... | collective-permute-start | bytes 98312 | tf_op jit(solution)/shard_map/ppermute | solution.py:194
  9.9 4.3 %collective-permute-start.1 = (bf16[64,256]{1,0:T(8,128)(2,1)S(1)}, bf16[64,256]{1,0:T(8,128)(2,1)S(1)}, u32[]{:S(2)}, u32[]{:S(2)}) collective-permute-start(bf16[64,256]{1,0:T(8,128)(2,1)S(1)} %collective-permute-done.refs_2_), channel_id=1, source_target_pairs={{0,1},{1,0},{2,3},{3,2},{4,5},{5,4},{6,7},{7,6},{8,9},{9,8},{10,11... | collective-permute-start | bytes 98312 | tf_op jit(solution)/shard_map/ppermute | solution.py:194
  16.5 4.5 %collective-permute-start.8 = (bf16[64,256]{1,0:T(8,128)(2,1)S(1)}, bf16[64,256]{1,0:T(8,128)(2,1)S(1)}, u32[]{:S(2)}, u32[]{:S(2)}) collective-permute-start(bf16[64,256]{1,0:T(8,128)(2,1)S(1)} %get-tuple-element.49), channel_id=1, source_target_pairs={{0,2},{1,3},{2,0},{3,1},{4,6},{5,7},{6,4},{7,5},{8,10},{9,11},{10,... | collective-permute-start | bytes 98312 | tf_op jit(solution)/shard_map/ppermute | solution.py:194
  18.0 5.5 %collective-permute-start.9 = (bf16[64,256]{1,0:T(8,128)(2,1)S(1)}, bf16[64,256]{1,0:T(8,128)(2,1)S(1)}, u32[]{:S(2)}, u32[]{:S(2)}) collective-permute-start(bf16[64,256]{1,0:T(8,128)(2,1)S(1)} %get-tuple-element.50), channel_id=1, source_target_pairs={{0,4},{1,5},{2,6},{3,7},{4,0},{5,1},{6,2},{7,3},{8,12},{9,13},{10,... | collective-permute-start | bytes 98312 | tf_op jit(solution)/shard_map/ppermute | solution.py:194
  20.9 5.8 %collective-permute-start.10 = (bf16[64,256]{1,0:T(8,128)(2,1)S(1)}, bf16[64,256]{1,0:T(8,128)(2,1)S(1)}, u32[]{:S(2)}, u32[]{:S(2)}) collective-permute-start(bf16[64,256]{1,0:T(8,128)(2,1)S(1)} %get-tuple-element.51), channel_id=1, source_target_pairs={{0,6},{1,7},{2,4},{3,5},{4,2},{5,3},{6,0},{7,1},{8,14},{9,15},{10,... | collective-permute-start | bytes 98312 | tf_op jit(solution)/shard_map/ppermute | solution.py:194
  26.7 5.8 %collective-permute-start.16 = (bf16[64,256]{1,0:T(8,128)(2,1)S(1)}, bf16[64,256]{1,0:T(8,128)(2,1)S(1)}, u32[]{:S(2)}, u32[]{:S(2)}) collective-permute-start(bf16[64,256]{1,0:T(8,128)(2,1)S(1)} %shard_map.209.refs_0_.refs_9_), channel_id=1, source_target_pairs={{0,6},{1,7},{2,4},{3,5},{4,2},{5,3},{6,0},{7,1},{8,14},{9,15},{10,... | collective-permute-start | bytes 98312 | tf_op jit(solution)/shard_map/ppermute | solution.py:194
  27.1 5.5 %collective-permute-start.11 = (bf16[64,256]{1,0:T(8,128)(2,1)S(1)}, bf16[64,256]{1,0:T(8,128)(2,1)S(1)}, u32[]{:S(2)}, u32[]{:S(2)}) collective-permute-start(bf16[64,256]{1,0:T(8,128)(2,1)S(1)} %shard_map.209.refs_0_.refs_9_), channel_id=1, source_target_pairs={{0,2},{1,3},{2,0},{3,1},{4,6},{5,7},{6,4},{7,5},{8,10},{9,11},{10,... | collective-permute-start | bytes 98312 | tf_op jit(solution)/shard_map/ppermute | solution.py:194
  27.1 6.0 %collective-permute-start.13 = (bf16[64,256]{1,0:T(8,128)(2,1)S(1)}, bf16[64,256]{1,0:T(8,128)(2,1)S(1)}, u32[]{:S(2)}, u32[]{:S(2)}) collective-permute-start(bf16[64,256]{1,0:T(8,128)(2,1)S(1)} %shard_map.209.refs_0_.refs_9_), channel_id=1, source_target_pairs={{0,4},{1,5},{2,6},{3,7},{4,0},{5,1},{6,2},{7,3},{8,12},{9,13},{10,... | collective-permute-start | bytes 98312 | tf_op jit(solution)/shard_map/ppermute | solution.py:194
  35.2 4.5 %collective-permute-start.18 = (bf16[16,1024]{1,0:T(8,128)(2,1)S(1)}, bf16[16,1024]{1,0:T(8,128)(2,1)S(1)}, u32[]{:S(2)}, u32[]{:S(2)}) collective-permute-start(bf16[16,1024]{1,0:T(8,128)(2,1)S(1)} %get-tuple-element.56), channel_id=1, source_target_pairs={{0,2},{1,3},{2,0},{3,1},{4,6},{5,7},{6,4},{7,5},{8,10},{9,11},{10,... | collective-permute-start | bytes 98312 | tf_op jit(solution)/shard_map/ppermute | solution.py:194
  35.7 4.8 %collective-permute-start.19 = (bf16[16,1024]{1,0:T(8,128)(2,1)S(1)}, bf16[16,1024]{1,0:T(8,128)(2,1)S(1)}, u32[]{:S(2)}, u32[]{:S(2)}) collective-permute-start(bf16[16,1024]{1,0:T(8,128)(2,1)S(1)} %get-tuple-element.57), channel_id=1, source_target_pairs={{0,4},{1,5},{2,6},{3,7},{4,0},{5,1},{6,2},{7,3},{8,12},{9,13},{10,... | collective-permute-start | bytes 98312 | tf_op jit(solution)/shard_map/ppermute | solution.py:194
  37.8 5.7 %collective-permute-start.20 = (bf16[16,1024]{1,0:T(8,128)(2,1)S(1)}, bf16[16,1024]{1,0:T(8,128)(2,1)S(1)}, u32[]{:S(2)}, u32[]{:S(2)}) collective-permute-start(bf16[16,1024]{1,0:T(8,128)(2,1)S(1)} %get-tuple-element.58), channel_id=1, source_target_pairs={{0,6},{1,7},{2,4},{3,5},{4,2},{5,3},{6,0},{7,1},{8,14},{9,15},{10,... | collective-permute-start | bytes 98312 | tf_op jit(solution)/shard_map/ppermute | solution.py:194
  39.6 5.6 %collective-permute-start.21 = (bf16[16,1024]{1,0:T(8,128)(2,1)S(1)}, bf16[16,1024]{1,0:T(8,128)(2,1)S(1)}, u32[]{:S(2)}, u32[]{:S(2)}) collective-permute-start(bf16[16,1024]{1,0:T(8,128)(2,1)S(1)} %get-tuple-element.55.refs_0_), channel_id=1, source_target_pairs={{0,1},{1,0},{2,3},{3,2},{4,5},{5,4},{6,7},{7,6},{8,9},{9,8},{10,11... | collective-permute-start | bytes 98312 | tf_op jit(solution)/shard_map/ppermute | solution.py:194
  39.6 5.6 %collective-permute-start.22 = (bf16[16,1024]{1,0:T(8,128)(2,1)S(1)}, bf16[16,1024]{1,0:T(8,128)(2,1)S(1)}, u32[]{:S(2)}, u32[]{:S(2)}) collective-permute-start(bf16[16,1024]{1,0:T(8,128)(2,1)S(1)} %collective-permute-done.18.refs_1_), channel_id=1, source_target_pairs={{0,1},{1,0},{2,3},{3,2},{4,5},{5,4},{6,7},{7,6},{8,9},{9,8},{10,11... | collective-permute-start | bytes 98312 | tf_op jit(solution)/shard_map/ppermute | solution.py:194
  40.5 4.7 %collective-permute-start.23 = (bf16[16,1024]{1,0:T(8,128)(2,1)S(1)}, bf16[16,1024]{1,0:T(8,128)(2,1)S(1)}, u32[]{:S(2)}, u32[]{:S(2)}) collective-permute-start(bf16[16,1024]{1,0:T(8,128)(2,1)S(1)} %collective-permute-done.19.refs_2_), channel_id=1, source_target_pairs={{0,1},{1,0},{2,3},{3,2},{4,5},{5,4},{6,7},{7,6},{8,9},{9,8},{10,11... | collective-permute-start | bytes 98312 | tf_op jit(solution)/shard_map/ppermute | solution.py:194
  46.1 4.5 %collective-permute-start.26 = (bf16[8,2048]{1,0:T(8,128)(2,1)S(1)}, bf16[8,2048]{1,0:T(8,128)(2,1)S(1)}, u32[]{:S(2)}, u32[]{:S(2)}) collective-permute-start(bf16[8,2048]{1,0:T(8,128)(2,1)S(1)} %shard_map.215.refs_0_), channel_id=1, source_target_pairs={{0,2},{1,3},{2,0},{3,1},{4,6},{5,7},{6,4},{7,5},{8,10},{9,11},{10,... | collective-permute-start | bytes 98312 | tf_op jit(solution)/shard_map/ppermute | solution.py:194
  46.4 5.1 %collective-permute-start.28 = (bf16[8,2048]{1,0:T(8,128)(2,1)S(1)}, bf16[8,2048]{1,0:T(8,128)(2,1)S(1)}, u32[]{:S(2)}, u32[]{:S(2)}) collective-permute-start(bf16[8,2048]{1,0:T(8,128)(2,1)S(1)} %shard_map.215.refs_0_), channel_id=1, source_target_pairs={{0,4},{1,5},{2,6},{3,7},{4,0},{5,1},{6,2},{7,3},{8,12},{9,13},{10,... | collective-permute-start | bytes 98312 | tf_op jit(solution)/shard_map/ppermute | solution.py:194
  48.6 5.7 %collective-permute-start.30 = (bf16[8,2048]{1,0:T(8,128)(2,1)S(1)}, bf16[8,2048]{1,0:T(8,128)(2,1)S(1)}, u32[]{:S(2)}, u32[]{:S(2)}) collective-permute-start(bf16[8,2048]{1,0:T(8,128)(2,1)S(1)} %shard_map.215.refs_0_), channel_id=1, source_target_pairs={{0,6},{1,7},{2,4},{3,5},{4,2},{5,3},{6,0},{7,1},{8,14},{9,15},{10,... | collective-permute-start | bytes 98312 | tf_op jit(solution)/shard_map/ppermute | solution.py:194
  55.8 5.8 %collective-permute-start.37 = (bf16[64,256]{1,0:T(8,128)(2,1)S(1)}, bf16[64,256]{1,0:T(8,128)(2,1)S(1)}, u32[]{:S(2)}, u32[]{:S(2)}) collective-permute-start(bf16[64,256]{1,0:T(8,128)(2,1)S(1)} %shard_map.216.refs_0_.base_ref), channel_id=1, source_target_pairs={{0,6},{1,7},{2,4},{3,5},{4,2},{5,3},{6,0},{7,1},{8,14},{9,15},{10,... | collective-permute-start | bytes 98312 | tf_op jit(solution)/shard_map/ppermute | solution.py:194
  57.9 4.4 %collective-permute-start.32 = (bf16[64,256]{1,0:T(8,128)(2,1)S(1)}, bf16[64,256]{1,0:T(8,128)(2,1)S(1)}, u32[]{:S(2)}, u32[]{:S(2)}) collective-permute-start(bf16[64,256]{1,0:T(8,128)(2,1)S(1)} %shard_map.216.refs_0_.base_ref), channel_id=1, source_target_pairs={{0,2},{1,3},{2,0},{3,1},{4,6},{5,7},{6,4},{7,5},{8,10},{9,11},{10,... | collective-permute-start | bytes 98312 | tf_op jit(solution)/shard_map/ppermute | solution.py:194
  57.9 5.2 %collective-permute-start.34 = (bf16[64,256]{1,0:T(8,128)(2,1)S(1)}, bf16[64,256]{1,0:T(8,128)(2,1)S(1)}, u32[]{:S(2)}, u32[]{:S(2)}) collective-permute-start(bf16[64,256]{1,0:T(8,128)(2,1)S(1)} %shard_map.216.refs_0_.base_ref), channel_id=1, source_target_pairs={{0,4},{1,5},{2,6},{3,7},{4,0},{5,1},{6,2},{7,3},{8,12},{9,13},{10,... | collective-permute-start | bytes 98312 | tf_op jit(solution)/shard_map/ppermute | solution.py:194
  66.5 5.8 %collective-permute-start.40 = (bf16[64,256]{1,0:T(8,128)(2,1)S(1)}, bf16[64,256]{1,0:T(8,128)(2,1)S(1)}, u32[]{:S(2)}, u32[]{:S(2)}) collective-permute-start(bf16[64,256]{1,0:T(8,128)(2,1)S(1)} %get-tuple-element.71), channel_id=1, source_target_pairs={{0,2},{1,3},{2,0},{3,1},{4,6},{5,7},{6,4},{7,5},{8,10},{9,11},{10,... | collective-permute-start | bytes 98312 | tf_op jit(solution)/shard_map/ppermute | solution.py:194
  68.2 5.6 %collective-permute-start.41 = (bf16[64,256]{1,0:T(8,128)(2,1)S(1)}, bf16[64,256]{1,0:T(8,128)(2,1)S(1)}, u32[]{:S(2)}, u32[]{:S(2)}) collective-permute-start(bf16[64,256]{1,0:T(8,128)(2,1)S(1)} %get-tuple-element.72), channel_id=1, source_target_pairs={{0,4},{1,5},{2,6},{3,7},{4,0},{5,1},{6,2},{7,3},{8,12},{9,13},{10,... | collective-permute-start | bytes 98312 | tf_op jit(solution)/shard_map/ppermute | solution.py:194
  68.9 5.7 %collective-permute-start.42 = (bf16[64,256]{1,0:T(8,128)(2,1)S(1)}, bf16[64,256]{1,0:T(8,128)(2,1)S(1)}, u32[]{:S(2)}, u32[]{:S(2)}) collective-permute-start(bf16[64,256]{1,0:T(8,128)(2,1)S(1)} %get-tuple-element.73), channel_id=1, source_target_pairs={{0,6},{1,7},{2,4},{3,5},{4,2},{5,3},{6,0},{7,1},{8,14},{9,15},{10,... | collective-permute-start | bytes 98312 | tf_op jit(solution)/shard_map/ppermute | solution.py:194
  (41 other events, 536.3 us)

commit v6 on v5

--- a/solution.py
+++ b/solution.py
@@ -169,6 +169,7 @@
 VMEM_SPEC = pl.BlockSpec(memory_space=pltpu.VMEM)
 HBM_SPEC = pl.BlockSpec(memory_space=pltpu.HBM)
 GROUP = ("kv", "tp")
+LIVE_HALVES = 7
 F32, BF16 = jnp.float32, jnp.bfloat16
 
 
@@ -213,37 +214,31 @@
     return pair_up(near, count)
 
 
-def entry_kernel(gate_hbm, up_hbm, down_hbm, mark_ref):
-    mark_ref[...] = jnp.zeros_like(mark_ref)
-
-
-def enter(*weights):
-    arrays = [pltpu.with_memory_space_constraint(a, pltpu.HBM) for a in weights]
+def entry_kernel(length_ref, tokens_hbm, gain_hbm, gate_hbm, up_hbm, down_hbm, *refs):
+    tokens_ref, gain_ref, sem = refs
+    rows = tokens_hbm.shape[0]
+    copies = [
+        pltpu.make_async_copy(tokens_hbm, tokens_ref.at[pl.ds(0, rows)], sem.at[0]),
+        pltpu.make_async_copy(gain_hbm, gain_ref, sem.at[1]),
+    ]
+    for copy in copies:
+        copy.start()
+    tail = (BLK, tokens_ref.shape[1])
+    tokens_ref[pl.ds(rows, BLK), :] = jnp.full(tail, length_ref[0].astype(F32)).astype(BF16)
+    for copy in copies:
+        copy.wait()
+
+
+def enter(tokens, gain, lengths, *weights):
+    arrays = [tokens, gain, *weights]
+    arrays = [pltpu.with_memory_space_constraint(a, pltpu.HBM) for a in arrays]
+    rows, width = tokens.shape
     return call(
         entry_kernel,
-        pltpu.VMEM((8, 128), F32),
-        arrays,
-        in_specs=[HBM_SPEC] * len(arrays),
-        limit=1 << 20,
-    )
-
-
-def stage_kernel(count, *refs):
-    sources, targets, sem = refs[:count], refs[count : 2 * count], refs[2 * count]
-    copies = [pltpu.make_async_copy(*pair, sem.at[i]) for i, pair in enumerate(zip(sources, targets))]
-    for copy in copies:
-        copy.start()
-    for copy in copies:
-        copy.wait()
-
-
-def stage(*arrays):
-    return call(
-        functools.partial(stage_kernel, len(arrays)),
-        [pltpu.VMEM(a.shape, a.dtype) for a in arrays],
-        [pltpu.with_memory_space_constraint(a, pltpu.HBM) for a in arrays],
-        in_specs=[HBM_SPEC] * len(arrays),
-        scratch=[pltpu.SemaphoreType.DMA((len(arrays),))],
+        [pltpu.VMEM((rows + BLK, width), BF16), pltpu.VMEM(gain.shape, F32)],
+        [lengths, *arrays],
+        in_specs=[pl.BlockSpec(memory_space=pltpu.SMEM)] + [HBM_SPEC] * len(arrays),
+        scratch=[pltpu.SemaphoreType.DMA((2,))],
         limit=1 << 20,
     )
 
@@ -278,29 +273,9 @@
     return [m for m in range(count) if m not in late], list(late)
 
 
-def entry_kernel(gate_hbm, up_hbm, down_hbm, mark_ref):
-    mark_ref[...] = jnp.zeros_like(mark_ref)
-
-
-def enter(*weights):
-    arrays = [pltpu.with_memory_space_constraint(a, pltpu.HBM) for a in weights]
-    return call(
-        entry_kernel,
-        pltpu.VMEM((8, 128), F32),
-        arrays,
-        in_specs=[HBM_SPEC] * len(arrays),
-        limit=1 << 20,
-    )
-
-
-def core_span(units):
-    tiles = units // 128
-    span = -(-tiles // 2) * 128
-    return span, units - span
-
-
-def units_of(blocks, masks, gain_ref, gate_ref, up_ref, span, skip):
+def units_of(blocks, masks, gain_ref, gate_ref, up_ref, span, skip, row_count):
     index = my_index()
+    blocks = [block.at[pl.ds(0, row_count)] for block in blocks]
     start = pl.multiple_of(lax.axis_index("tp") * skip, 128)
     gate_acc = up_acc = squares = None
     for mask, block in zip(masks, blocks):
@@ -317,9 +292,9 @@
 
 def ffn_early_kernel(masks, span, skip, *refs):
     blocks = refs[: len(masks)]
-    gain_ref, gate_ref, up_ref, _, _, gate_out, up_out, squares_out = refs[len(masks) :]
+    gain_ref, gate_ref, up_ref, _, gate_out, up_out, squares_out = refs[len(masks) :]
     gate_out[...], up_out[...], squares_out[...] = units_of(
-        blocks, masks, gain_ref, gate_ref, up_ref, span, skip
+        blocks, masks, gain_ref, gate_ref, up_ref, span, skip, gate_out.shape[0]
     )
 
 
@@ -327,7 +302,9 @@
     blocks = refs[: len(masks)]
     gain_ref, gate_ref, up_ref, down_ref, gate_in, up_in, squares_in = refs[len(masks) : len(masks) + 7]
     hidden_ref, cross_ref = refs[len(masks) + 7 :]
-    gate_acc, up_acc, squares = units_of(blocks, masks, gain_ref, gate_ref, up_ref, span, skip)
+    gate_acc, up_acc, squares = units_of(
+        blocks, masks, gain_ref, gate_ref, up_ref, span, skip, gate_in.shape[0]
+    )
     channels = gate_ref.shape[0]
     row_scale = scale_of_rows(squares + squares_in[...], channels)
     gate_act = (gate_acc + gate_in[...]) * row_scale
@@ -366,21 +343,78 @@
     refs[-1][...] = (base_ref[...].astype(F32) + 0.5 * total).astype(BF16)
 
 
-def half_step(own, mark, count, gain, gate, up, down, first=False, last=False):
-    rows, width = own.shape
+def live_kernel(count, rows, *refs):
+    blocks, pick_ref = refs[:count], refs[count]
+    index = my_index()
+    lane = lax.broadcasted_iota(jnp.int32, (BLK, rows), 1)
+    lengths = jnp.zeros((BLK, rows), F32)
+    for mask, block in enumerate(blocks):
+        length = block[pl.ds(rows, BLK), :rows].astype(F32)
+        lengths = jnp.where(lane // BLK == (index ^ mask), length, lengths)
+    live = (lane % BLK).astype(F32) < lengths
+    before = lax.broadcasted_iota(jnp.int32, (rows, rows), 0) < lax.broadcasted_iota(
+        jnp.int32, (rows, rows), 1
+    )
+    rank = jnp.dot(live.astype(BF16), before.astype(BF16), preferred_element_type=F32)
+    rank = jnp.where(live, rank, -1.0)[:1]
+    wanted = lax.broadcasted_iota(jnp.int32, pick_ref.shape, 0).astype(F32)
+    pick_ref[...] = (rank == wanted).astype(F32).astype(BF16)
+
+
+def spread_kernel(near, pick_ref, own_ref, cross_ref, mine_ref, kept_ref, *sends):
+    pick = pick_ref[...]
+    packed = pick.shape[0]
+    rows = own_ref.shape[1]
+    whole, chosen = [], []
+    for step in range(near):
+        total = own_ref[step] + cross_ref[step].astype(F32)
+        if step == 0:
+            mine_ref[...] = total
+        high, low = parts(total)
+        upper = jnp.dot(pick, high, preferred_element_type=F32)
+        whole.append(high)
+        chosen.append(upper.astype(BF16))
+        if step:
+            kept_ref[step - 1] = upper + jnp.dot(pick, low, preferred_element_type=F32)
+    for step, send in enumerate(sends, 1):
+        send[pl.ds(0, rows), :] = whole[step]
+        others = [other for other in range(near) if other != step]
+        for place, other in enumerate(others):
+            send[pl.ds(rows + place * packed, packed), :] = chosen[other]
+
+
+def collect_kernel(near, *refs):
+    pick_ref, mine_ref, kept_ref = refs[:3]
+    tokens, received = refs[3 : 3 + near], refs[3 + near : 2 + 2 * near]
+    after_ref, near_ref = refs[2 + 2 * near :]
+    pick = pick_ref[...]
+    packed = pick.shape[0]
+    rows = mine_ref.shape[0]
+    total = mine_ref[...]
+    for part in received:
+        total = total + part[pl.ds(0, rows), :].astype(F32)
+    base = tokens[0][pl.ds(0, rows), :].astype(F32)
+    after = (base + 0.5 * total).astype(BF16)
+    after_ref[...] = after
+    near_ref[0] = jnp.dot(pick, after, preferred_element_type=F32).astype(BF16)
+    for step in range(1, near):
+        total = kept_ref[step - 1]
+        for sender, part in enumerate(received, 1):
+            place = [other for other in range(near) if other != sender].index(sender ^ step)
+            total = total + part[pl.ds(rows + place * packed, packed), :].astype(F32)
+        base = jnp.dot(pick, tokens[step][pl.ds(0, rows), :], preferred_element_type=F32)
+        near_ref[step] = (base + 0.5 * total).astype(BF16)
+
+
+def hidden_sums(blocks, rows, count, gain, gate, up, down):
     near = count // 2
+    width = blocks[0].shape[1]
     span, skip = core_span(down.shape[0])
-    gain = gain.reshape(1, count * width)
-    near_own = own
-    if first:
-        own, gain = stage(own, gain)
-    received = far_swaps([near_own] * (near - 1), count)
-    blocks = pair_up([own, *received], count)
     early, late = early_masks(count)
     parts_early = call(
         functools.partial(ffn_early_kernel, early, span, skip),
         [pltpu.VMEM((rows, span), F32)] * 2 + [pltpu.VMEM((rows, 128), F32)],
-        [*(blocks[m] for m in early), gain, gate, up, down, mark],
+        [*(blocks[m] for m in early), gain, gate, up, down],
     )
     hidden, cross_part = call(
         functools.partial(ffn_late_kernel, late, count, span, skip),
@@ -393,14 +427,48 @@
         pltpu.VMEM((near, rows, width), F32),
         [hidden, down],
     )
+    return own_part, cross_sum
+
+
+def first_half_step(tokens, rows, count, gain, gate, up, down):
+    near = count // 2
+    width = tokens.shape[1]
+    blocks = gather_blocks(tokens, count)
+    own_part, cross_sum = hidden_sums(blocks, rows, count, gain, gate, up, down)
+    live_rows = count * LIVE_HALVES // 2
+    packed = -(-live_rows // 16) * 16
+    pick = call(
+        functools.partial(live_kernel, count, rows), pltpu.VMEM((packed, rows), BF16), blocks
+    )
+    sent = rows + (near - 1) * packed
+    mine, kept, *sends = call(
+        functools.partial(spread_kernel, near),
+        [pltpu.VMEM((rows, width), F32), pltpu.VMEM((near - 1, packed, width), F32)]
+        + [pltpu.VMEM((sent, width), BF16)] * (near - 1),
+        [pick, own_part, cross_sum],
+    )
+    received = far_swaps(sends, count)
+    after, near_live = call(
+        functools.partial(collect_kernel, near),
+        [pltpu.VMEM((rows, width), BF16), pltpu.VMEM((near, packed, width), BF16)],
+        [pick, mine, kept, *blocks[::2], *received],
+    )
+    return after, near_live, pick
+
+
+def second_half_step(own, count, gain, gate, up, down):
+    rows, width = own.shape
+    near = count // 2
+    gain = gain.reshape(1, count * width)
+    blocks = gather_blocks(own, count)
+    own_part, cross_sum = hidden_sums(blocks, rows, count, gain, gate, up, down)
     mine, *sends = call(
         pair_sum_kernel,
         [pltpu.VMEM((rows, width), F32)] + [pltpu.VMEM((rows, width), BF16)] * (near - 1),
         [own_part, cross_sum],
     )
     received = far_swaps(sends, count)
-    shape = jax.ShapeDtypeStruct if last else pltpu.VMEM
-    return call(residual_kernel, shape((rows, width), BF16), [own, mine, *received])
+    return call(residual_kernel, jax.ShapeDtypeStruct((rows, width), BF16), [own, mine, *received])
 
 
 def mixes_of(blocks, masks, gain_ref, weights, thin):
@@ -423,10 +491,9 @@
     return wide, narrow, squares
 
 
-def project_early_kernel(masks, *refs):
-    blocks = refs[: len(masks)]
-    gain_ref, *weights = refs[len(masks) : len(masks) + 7]
-    result, pre, squares_out = refs[len(masks) + 7 :]
+def project_early_kernel(masks, near_ref, gain_ref, *refs):
+    weights, (result, pre, squares_out) = refs[:6], refs[6:]
+    blocks = [near_ref.at[place] for place in range(len(masks))]
     wide, narrow, squares_out[...] = mixes_of(blocks, masks, gain_ref, weights[:4], weights[4:])
     for place, part in enumerate(wide):
         width = part.shape[1]
@@ -436,21 +503,27 @@
         pre[:, place * width : (place + 1) * width] = part
 
 
-def project_late_kernel(masks, *refs):
-    blocks = refs[: len(masks)]
-    gain_ref, *weights = refs[len(masks) : len(masks) + 7]
-    result_in, pre_in, squares_in = refs[len(masks) + 7 : len(masks) + 10]
-    *sends, pre_ref, result, pre_scratch = refs[len(masks) + 10 :]
+def project_late_kernel(masks, near_ref, gain_ref, *refs):
+    weights, (result_in, pre_in, squares_in, pick_ref) = refs[:6], refs[6:10]
+    *sends, pre_ref, result, pre_scratch = refs[10:]
+    blocks = [near_ref.at[place] for place in range(len(masks))]
     wide, narrow, squares = mixes_of(blocks, masks, gain_ref, weights[:4], weights[4:])
     row_scale = scale_of_rows(squares + squares_in[...], weights[0].shape[0])
+    pick = pick_ref[...]
+    back = (((0,), (0,)), ((), ()))
     for place, part in enumerate(wide):
         width = part.shape[1]
         columns = slice(place * width, (place + 1) * width)
-        result[:, columns] = (part + result_in[:, columns]) * row_scale
+        rounded = ((part + result_in[:, columns]) * row_scale).astype(BF16)
+        result[:, columns] = lax.dot_general(pick, rounded, back, preferred_element_type=F32)
     for place, part in enumerate(narrow):
         width = part.shape[1]
         columns = slice(place * width, (place + 1) * width)
-        pre_scratch[:, columns] = (part + pre_in[:, columns]) * row_scale
+        high, low = parts((part + pre_in[:, columns]) * row_scale)
+        total = lax.dot_general(pick, high, back, preferred_element_type=F32)
+        pre_scratch[:, columns] = total + lax.dot_general(
+            pick, low, back, preferred_element_type=F32
+        )
     for step, send in enumerate(sends):
         rows = send.shape[0]
         row = pl.multiple_of((lax.axis_index("kv") ^ step) * rows, rows)
@@ -636,14 +709,17 @@
     rows, width = tokens.shape
     channels = gain_first.shape[0]
     heads, size = state.shape[1], state.shape[2]
-    mark = enter(first_gate, first_up, first_down)
-    after_first = half_step(
-        tokens, mark, count, gain_first, first_gate, first_up, first_down, first=True
-    )
-    blocks = gather_blocks(after_first, count)
+    entered, gain_ready = enter(
+        tokens, gain_first.reshape(1, channels), lengths, first_gate, first_up, first_down
+    )
+    after_first, near_live, pick = first_half_step(
+        entered, rows, count, gain_ready, first_gate, first_up, first_down
+    )
+    cross_live = swap(near_live, 1, count)
+    packed = pick.shape[0]
     columns = 4 * width
     near = count // 2
-    early, late = early_masks(count)
+    near_masks, cross_masks = list(range(0, count, 2)), list(range(1, count, 2))
     mixers = [
         gain_mix.reshape(1, channels),
         query_weight,
@@ -654,18 +730,18 @@
         forget_weight.T,
     ]
     parts_early = call(
-        functools.partial(project_early_kernel, early),
+        functools.partial(project_early_kernel, near_masks),
         [
-            pltpu.VMEM((rows, columns), F32),
-            pltpu.VMEM((rows, 2 * heads), F32),
-            pltpu.VMEM((rows, 128), F32),
+            pltpu.VMEM((packed, columns), F32),
+            pltpu.VMEM((packed, 2 * heads), F32),
+            pltpu.VMEM((packed, 128), F32),
         ],
-        [*(blocks[m] for m in early), *mixers],
+        [near_live, *mixers],
     )
     *sends, pre = call(
-        functools.partial(project_late_kernel, late),
+        functools.partial(project_late_kernel, cross_masks),
         [pltpu.VMEM((rows // near, columns), BF16)] * near + [pltpu.VMEM((BLK, 2 * heads), F32)],
-        [*(blocks[m] for m in late), *mixers, *parts_early],
+        [cross_live, *mixers, *parts_early, pick],
         scratch=[pltpu.VMEM((rows, columns), F32), pltpu.VMEM((rows, 2 * heads), F32)],
     )
     owned = pair_up([sends[0]] + far_swaps(sends[1:], count), count)
@@ -709,8 +785,8 @@
         [*head_blocks, out_weight, after_first],
         scratch=[pltpu.VMEM((rows, width), F32)],
     )
-    mixed_out = half_step(
-        after_mix, mark, count, gain_second, second_gate, second_up, second_down, last=True
+    mixed_out = second_half_step(
+        after_mix, count, gain_second, second_gate, second_up, second_down
     )
     return (mixed_out, new_state.reshape(state.shape))
 

time: 75.5 us -> 68.9 us (0.913)
  starting transfers between devices: 34.6 us -> 30.4 us
  local copies, waits for them, and re-layouts: 2.43 us -> 0.11 us
    ppermute x43 -> x37, starting transfers between devices: 34.6 us -> 30.4 us  [swap(): return lax.ppermute(value, GROUP, [(i, i ^ mask) for i in range(count)])]
    unnamed x44 -> x40, local copies, waits for them, and re-layouts: 2.43 us -> 0.11 us
    ppermute x43 -> x37, waiting for transfers between devices: 25.8 us -> 25.3 us  [swap(): return lax.ppermute(value, GROUP, [(i, i ^ mask) for i in range(count)])]
  transfers between devices with their start and end apart: 43 -> 37, of which waited for: 21 -> 21; matrix products, arithmetic and copies ran while one was open for 0% -> 0% of each run, Pallas kernels for 9% -> 8%
where the time goes in v6:
time: 68.9 us; the launch traced here: 68.7 us
  starting transfers between devices  30.4 us (44%)
  waiting for transfers between devices  25.3 us (37%)
  Pallas kernels  11.1 us (16%)
  between operations  1.73 us (3%)
    ppermute x37, starting transfers between devices, swap(): return lax.ppermute(value, GROUP, [(i, i ^ mask) for i in range(count)])  30.4 us
    ppermute x37, waiting for transfers between devices, swap(): return lax.ppermute(value, GROUP, [(i, i ^ mask) for i in range(count)])  25.3 us
    pallas_call x20, Pallas kernels, call(): pl.pallas_call(body, out_shape=shapes, in_specs=in_specs or [VMEM_SPEC] *...  11.1 us
  transfers between devices with their start and end apart: 37, of which 21 were waited for; matrix products, arithmetic and copies ran while one was open for 0% of the time, Pallas kernels for 8%

profile of v6, /device:TPU:0, one launch (start us, length us, event | category | flops | bytes accessed | tf_op | source)
XLA Modules:
  0.0 68.7 jit_solution(3431174868363159908)
XLA Ops:
  2.2 5.1 %collective-permute-start.5 = (bf16[72,256]{1,0:T(8,128)(2,1)S(1)}, bf16[72,256]{1,0:T(8,128)(2,1)S(1)}, u32[]{:S(2)}, u32[]{:S(2)}) collective-permute-start(bf16[72,256]{1,0:T(8,128)(2,1)S(1)} %get-tuple-element.44.refs_0_.refs_3_), channel_id=1, source_target_pairs={{0,6},{1,7},{2,4},{3,5},{4,2},{5,3},{6,0},{7,1},{8,14},{9,15},{10,... | collective-permute-start | bytes 110600 | tf_op jit(solution)/shard_map/ppermute | solution.py:195
  8.0 1.3 %collective-permute-done.5.refs_6_.refs_4_ = bf16[72,256]{1,0:T(8,128)(2,1)S(1)} collective-permute-done((bf16[72,256]{1,0:T(8,128)(2,1)S(1)}, bf16[72,256]{1,0:T(8,128)(2,1)S(1)}, u32[]{:S(2)}, u32[]{:S(2)}) %collective-permute-start.5) | collective-permute-done | bytes 36896 | tf_op jit(solution)/shard_map/ppermute | solution.py:195
  9.3 2.0 %collective-permute-done.1.refs_2_.refs_4_ = bf16[72,256]{1,0:T(8,128)(2,1)S(1)} collective-permute-done((bf16[72,256]{1,0:T(8,128)(2,1)S(1)}, bf16[72,256]{1,0:T(8,128)(2,1)S(1)}, u32[]{:S(2)}, u32[]{:S(2)}) %collective-permute-start.1) | collective-permute-done | bytes 36896 | tf_op jit(solution)/shard_map/ppermute | solution.py:195
  11.3 1.1 %collective-permute-done.3.refs_4_.refs_3_.refs_5_ = bf16[72,256]{1,0:T(8,128)(2,1)S(1)} collective-permute-done((bf16[72,256]{1,0:T(8,128)(2,1)S(1)}, bf16[72,256]{1,0:T(8,128)(2,1)S(1)}, u32[]{:S(2)}, u32[]{:S(2)}) %collective-permute-start.3) | collective-permute-done | bytes 36896 | tf_op jit(solution)/shard_map/ppermute | solution.py:195
  16.0 1.9 %collective-permute-start.8 = (bf16[160,256]{1,0:T(8,128)(2,1)S(1)}, bf16[160,256]{1,0:T(8,128)(2,1)S(1)}, u32[]{:S(2)}, u32[]{:S(2)}) collective-permute-start(bf16[160,256]{1,0:T(8,128)(2,1)S(1)} %get-tuple-element.53), channel_id=1, source_target_pairs={{0,2},{1,3},{2,0},{3,1},{4,6},{5,7},{6,4},{7,5},{8,10},{9,11},{10,... | collective-permute-start | bytes 245768 | tf_op jit(solution)/shard_map/ppermute | solution.py:195
  18.5 2.0 %collective-permute-start.10 = (bf16[160,256]{1,0:T(8,128)(2,1)S(1)}, bf16[160,256]{1,0:T(8,128)(2,1)S(1)}, u32[]{:S(2)}, u32[]{:S(2)}) collective-permute-start(bf16[160,256]{1,0:T(8,128)(2,1)S(1)} %get-tuple-element.55), channel_id=1, source_target_pairs={{0,6},{1,7},{2,4},{3,5},{4,2},{5,3},{6,0},{7,1},{8,14},{9,15},{10,... | collective-permute-start | bytes 245768 | tf_op jit(solution)/shard_map/ppermute | solution.py:195
  20.9 5.7 %collective-permute-done.9.refs_8_ = bf16[160,256]{1,0:T(8,128)(2,1)S(1)} collective-permute-done((bf16[160,256]{1,0:T(8,128)(2,1)S(1)}, bf16[160,256]{1,0:T(8,128)(2,1)S(1)}, u32[]{:S(2)}, u32[]{:S(2)}) %collective-permute-start.9) | collective-permute-done | bytes 81952 | tf_op jit(solution)/shard_map/ppermute | solution.py:195
  28.9 2.3 %collective-permute-start.12 = (bf16[16,1024]{1,0:T(8,128)(2,1)S(1)}, bf16[16,1024]{1,0:T(8,128)(2,1)S(1)}, u32[]{:S(2)}, u32[]{:S(2)}) collective-permute-start(bf16[16,1024]{1,0:T(8,128)(2,1)S(1)} %get-tuple-element.61), channel_id=1, source_target_pairs={{0,2},{1,3},{2,0},{3,1},{4,6},{5,7},{6,4},{7,5},{8,10},{9,11},{10,... | collective-permute-start | bytes 98312 | tf_op jit(solution)/shard_map/ppermute | solution.py:195
  31.2 2.4 %collective-permute-start.14 = (bf16[16,1024]{1,0:T(8,128)(2,1)S(1)}, bf16[16,1024]{1,0:T(8,128)(2,1)S(1)}, u32[]{:S(2)}, u32[]{:S(2)}) collective-permute-start(bf16[16,1024]{1,0:T(8,128)(2,1)S(1)} %get-tuple-element.63), channel_id=1, source_target_pairs={{0,6},{1,7},{2,4},{3,5},{4,2},{5,3},{6,0},{7,1},{8,14},{9,15},{10,... | collective-permute-start | bytes 98312 | tf_op jit(solution)/shard_map/ppermute | solution.py:195
  34.1 2.3 %collective-permute-done.13.refs_2_ = bf16[16,1024]{1,0:T(8,128)(2,1)S(1)} collective-permute-done((bf16[16,1024]{1,0:T(8,128)(2,1)S(1)}, bf16[16,1024]{1,0:T(8,128)(2,1)S(1)}, u32[]{:S(2)}, u32[]{:S(2)}) %collective-permute-start.13) | collective-permute-done | bytes 32800 | tf_op jit(solution)/shard_map/ppermute | solution.py:195
  39.8 2.2 %collective-permute-start.22 = (bf16[8,2048]{1,0:T(8,128)(2,1)S(1)}, bf16[8,2048]{1,0:T(8,128)(2,1)S(1)}, u32[]{:S(2)}, u32[]{:S(2)}) collective-permute-start(bf16[8,2048]{1,0:T(8,128)(2,1)S(1)} %shard_map.215.refs_0_), channel_id=1, source_target_pairs={{0,4},{1,5},{2,6},{3,7},{4,0},{5,1},{6,2},{7,3},{8,12},{9,13},{10,... | collective-permute-start | bytes 98312 | tf_op jit(solution)/shard_map/ppermute | solution.py:195
  42.0 1.5 %collective-permute-start.24 = (bf16[8,2048]{1,0:T(8,128)(2,1)S(1)}, bf16[8,2048]{1,0:T(8,128)(2,1)S(1)}, u32[]{:S(2)}, u32[]{:S(2)}) collective-permute-start(bf16[8,2048]{1,0:T(8,128)(2,1)S(1)} %shard_map.215.refs_0_), channel_id=1, source_target_pairs={{0,6},{1,7},{2,4},{3,5},{4,2},{5,3},{6,0},{7,1},{8,14},{9,15},{10,... | collective-permute-start | bytes 98312 | tf_op jit(solution)/shard_map/ppermute | solution.py:195
  44.0 1.6 %collective-permute-done.22.refs_4_ = bf16[8,2048]{1,0:T(8,128)(2,1)S(1)} collective-permute-done((bf16[8,2048]{1,0:T(8,128)(2,1)S(1)}, bf16[8,2048]{1,0:T(8,128)(2,1)S(1)}, u32[]{:S(2)}, u32[]{:S(2)}) %collective-permute-start.22) | collective-permute-done | bytes 32800 | tf_op jit(solution)/shard_map/ppermute | solution.py:195
  45.6 2.1 %collective-permute-done.24.refs_6_ = bf16[8,2048]{1,0:T(8,128)(2,1)S(1)} collective-permute-done((bf16[8,2048]{1,0:T(8,128)(2,1)S(1)}, bf16[8,2048]{1,0:T(8,128)(2,1)S(1)}, u32[]{:S(2)}, u32[]{:S(2)}) %collective-permute-start.24) | collective-permute-done | bytes 32800 | tf_op jit(solution)/shard_map/ppermute | solution.py:195
  47.8 1.2 %collective-permute-done.25.refs_7_ = bf16[8,2048]{1,0:T(8,128)(2,1)S(1)} collective-permute-done((bf16[8,2048]{1,0:T(8,128)(2,1)S(1)}, bf16[8,2048]{1,0:T(8,128)(2,1)S(1)}, u32[]{:S(2)}, u32[]{:S(2)}) %collective-permute-start.25) | collective-permute-done | bytes 32800 | tf_op jit(solution)/shard_map/ppermute | solution.py:195
  49.3 1.6 %collective-permute-start.31 = (bf16[64,256]{1,0:T(8,128)(2,1)S(1)}, bf16[64,256]{1,0:T(8,128)(2,1)S(1)}, u32[]{:S(2)}, u32[]{:S(2)}) collective-permute-start(bf16[64,256]{1,0:T(8,128)(2,1)S(1)} %shard_map.216.refs_0_.base_ref), channel_id=1, source_target_pairs={{0,6},{1,7},{2,4},{3,5},{4,2},{5,3},{6,0},{7,1},{8,14},{9,15},{10,... | collective-permute-start | bytes 98312 | tf_op jit(solution)/shard_map/ppermute | solution.py:195
  50.8 2.9 %collective-permute-start.28 = (bf16[64,256]{1,0:T(8,128)(2,1)S(1)}, bf16[64,256]{1,0:T(8,128)(2,1)S(1)}, u32[]{:S(2)}, u32[]{:S(2)}) collective-permute-start(bf16[64,256]{1,0:T(8,128)(2,1)S(1)} %shard_map.216.refs_0_.base_ref), channel_id=1, source_target_pairs={{0,4},{1,5},{2,6},{3,7},{4,0},{5,1},{6,2},{7,3},{8,12},{9,13},{10,... | collective-permute-start | bytes 98312 | tf_op jit(solution)/shard_map/ppermute | solution.py:195
  53.7 1.3 %collective-permute-done.31.refs_4_ = bf16[64,256]{1,0:T(8,128)(2,1)S(1)} collective-permute-done((bf16[64,256]{1,0:T(8,128)(2,1)S(1)}, bf16[64,256]{1,0:T(8,128)(2,1)S(1)}, u32[]{:S(2)}, u32[]{:S(2)}) %collective-permute-start.31) | collective-permute-done | bytes 32800 | tf_op jit(solution)/shard_map/ppermute | solution.py:195
  59.5 1.6 %collective-permute-start.34 = (bf16[64,256]{1,0:T(8,128)(2,1)S(1)}, bf16[64,256]{1,0:T(8,128)(2,1)S(1)}, u32[]{:S(2)}, u32[]{:S(2)}) collective-permute-start(bf16[64,256]{1,0:T(8,128)(2,1)S(1)} %get-tuple-element.77), channel_id=1, source_target_pairs={{0,2},{1,3},{2,0},{3,1},{4,6},{5,7},{6,4},{7,5},{8,10},{9,11},{10,... | collective-permute-start | bytes 98312 | tf_op jit(solution)/shard_map/ppermute | solution.py:195
  61.1 1.2 %collective-permute-start.35 = (bf16[64,256]{1,0:T(8,128)(2,1)S(1)}, bf16[64,256]{1,0:T(8,128)(2,1)S(1)}, u32[]{:S(2)}, u32[]{:S(2)}) collective-permute-start(bf16[64,256]{1,0:T(8,128)(2,1)S(1)} %get-tuple-element.78), channel_id=1, source_target_pairs={{0,4},{1,5},{2,6},{3,7},{4,0},{5,1},{6,2},{7,3},{8,12},{9,13},{10,... | collective-permute-start | bytes 98312 | tf_op jit(solution)/shard_map/ppermute | solution.py:195
  62.4 1.6 %collective-permute-start.36 = (bf16[64,256]{1,0:T(8,128)(2,1)S(1)}, bf16[64,256]{1,0:T(8,128)(2,1)S(1)}, u32[]{:S(2)}, u32[]{:S(2)}) collective-permute-start(bf16[64,256]{1,0:T(8,128)(2,1)S(1)} %get-tuple-element.79), channel_id=1, source_target_pairs={{0,6},{1,7},{2,4},{3,5},{4,2},{5,3},{6,0},{7,1},{8,14},{9,15},{10,... | collective-permute-start | bytes 98312 | tf_op jit(solution)/shard_map/ppermute | solution.py:195
  64.0 1.3 %shard_map.222 = f32[16,128,128]{2,1,0:T(8,128)} custom-call(f32[64,128]{1,0:T(8,128)S(1)} %get-tuple-element.80.refs_0_, f32[64,128]{1,0:T(8,128)S(1)} %get-tuple-element.81.refs_1_, f32[64,128]{1,0:T(8,128)S(1)} %get-tuple-element.82.refs_2_, f32[64,128]{1,0:T(8,128)S(1)} %get-tuple-element.83.refs_3_, f32[64,128]{1,0:T(8,128)S(1)} %get-tuple-element.84.refs_4_, ...), custom_call_target="tpu_custom_call" | custom-call | tf_op jit(solution)/shard_map/pallas_call | solution.py:179
  65.3 1.2 %collective-permute-done.35.refs_1_ = bf16[64,256]{1,0:T(8,128)(2,1)S(1)} collective-permute-done((bf16[64,256]{1,0:T(8,128)(2,1)S(1)}, bf16[64,256]{1,0:T(8,128)(2,1)S(1)}, u32[]{:S(2)}, u32[]{:S(2)}) %collective-permute-start.35) | collective-permute-done | bytes 32800 | tf_op jit(solution)/shard_map/ppermute | solution.py:195
  66.5 1.6 %collective-permute-done.36.refs_2_ = bf16[64,256]{1,0:T(8,128)(2,1)S(1)} collective-permute-done((bf16[64,256]{1,0:T(8,128)(2,1)S(1)}, bf16[64,256]{1,0:T(8,128)(2,1)S(1)}, u32[]{:S(2)}, u32[]{:S(2)}) %collective-permute-start.36) | collective-permute-done | bytes 32800 | tf_op jit(solution)/shard_map/ppermute | solution.py:195
  (113 shorter events, 17.8 us)
Async XLA Ops:
  2.2 7.1 %collective-permute-start.5 = (bf16[72,256]{1,0:T(8,128)(2,1)S(1)}, bf16[72,256]{1,0:T(8,128)(2,1)S(1)}, u32[]{:S(2)}, u32[]{:S(2)}) collective-permute-start(bf16[72,256]{1,0:T(8,128)(2,1)S(1)} %get-tuple-element.44.refs_0_.refs_3_), channel_id=1, source_target_pairs={{0,6},{1,7},{2,4},{3,5},{4,2},{5,3},{6,0},{7,1},{8,14},{9,15},{10,... | collective-permute-start | bytes 110600 | tf_op jit(solution)/shard_map/ppermute | solution.py:195
  7.4 4.0 %collective-permute-start.1 = (bf16[72,256]{1,0:T(8,128)(2,1)S(1)}, bf16[72,256]{1,0:T(8,128)(2,1)S(1)}, u32[]{:S(2)}, u32[]{:S(2)}) collective-permute-start(bf16[72,256]{1,0:T(8,128)(2,1)S(1)} %get-tuple-element.44.refs_0_.refs_3_), channel_id=1, source_target_pairs={{0,2},{1,3},{2,0},{3,1},{4,6},{5,7},{6,4},{7,5},{8,10},{9,11},{10,... | collective-permute-start | bytes 110600 | tf_op jit(solution)/shard_map/ppermute | solution.py:195
  7.4 5.0 %collective-permute-start.3 = (bf16[72,256]{1,0:T(8,128)(2,1)S(1)}, bf16[72,256]{1,0:T(8,128)(2,1)S(1)}, u32[]{:S(2)}, u32[]{:S(2)}) collective-permute-start(bf16[72,256]{1,0:T(8,128)(2,1)S(1)} %get-tuple-element.44.refs_0_.refs_3_), channel_id=1, source_target_pairs={{0,4},{1,5},{2,6},{3,7},{4,0},{5,1},{6,2},{7,3},{8,12},{9,13},{10,... | collective-permute-start | bytes 110600 | tf_op jit(solution)/shard_map/ppermute | solution.py:195
  8.0 4.4 %collective-permute-start = (bf16[72,256]{1,0:T(8,128)(2,1)S(1)}, bf16[72,256]{1,0:T(8,128)(2,1)S(1)}, u32[]{:S(2)}, u32[]{:S(2)}) collective-permute-start(bf16[72,256]{1,0:T(8,128)(2,1)S(1)} %get-tuple-element.44.refs_0_.refs_3_), channel_id=1, source_target_pairs={{0,1},{1,0},{2,3},{3,2},{4,5},{5,4},{6,7},{7,6},{8,9},{9,8},{10,11... | collective-permute-start | bytes 110600 | tf_op jit(solution)/shard_map/ppermute | solution.py:195
  9.3 3.1 %collective-permute-start.6 = (bf16[72,256]{1,0:T(8,128)(2,1)S(1)}, bf16[72,256]{1,0:T(8,128)(2,1)S(1)}, u32[]{:S(2)}, u32[]{:S(2)}) collective-permute-start(bf16[72,256]{1,0:T(8,128)(2,1)S(1)} %collective-permute-done.5.refs_6_.refs_4_), channel_id=1, source_target_pairs={{0,1},{1,0},{2,3},{3,2},{4,5},{5,4},{6,7},{7,6},{8,9},{9,8},{10,11... | collective-permute-start | bytes 110600 | tf_op jit(solution)/shard_map/ppermute | solution.py:195
  16.0 4.9 %collective-permute-start.8 = (bf16[160,256]{1,0:T(8,128)(2,1)S(1)}, bf16[160,256]{1,0:T(8,128)(2,1)S(1)}, u32[]{:S(2)}, u32[]{:S(2)}) collective-permute-start(bf16[160,256]{1,0:T(8,128)(2,1)S(1)} %get-tuple-element.53), channel_id=1, source_target_pairs={{0,2},{1,3},{2,0},{3,1},{4,6},{5,7},{6,4},{7,5},{8,10},{9,11},{10,... | collective-permute-start | bytes 245768 | tf_op jit(solution)/shard_map/ppermute | solution.py:195
  18.0 8.7 %collective-permute-start.9 = (bf16[160,256]{1,0:T(8,128)(2,1)S(1)}, bf16[160,256]{1,0:T(8,128)(2,1)S(1)}, u32[]{:S(2)}, u32[]{:S(2)}) collective-permute-start(bf16[160,256]{1,0:T(8,128)(2,1)S(1)} %get-tuple-element.54), channel_id=1, source_target_pairs={{0,4},{1,5},{2,6},{3,7},{4,0},{5,1},{6,2},{7,3},{8,12},{9,13},{10,... | collective-permute-start | bytes 245768 | tf_op jit(solution)/shard_map/ppermute | solution.py:195
  18.5 8.2 %collective-permute-start.10 = (bf16[160,256]{1,0:T(8,128)(2,1)S(1)}, bf16[160,256]{1,0:T(8,128)(2,1)S(1)}, u32[]{:S(2)}, u32[]{:S(2)}) collective-permute-start(bf16[160,256]{1,0:T(8,128)(2,1)S(1)} %get-tuple-element.55), channel_id=1, source_target_pairs={{0,6},{1,7},{2,4},{3,5},{4,2},{5,3},{6,0},{7,1},{8,14},{9,15},{10,... | collective-permute-start | bytes 245768 | tf_op jit(solution)/shard_map/ppermute | solution.py:195
  28.9 4.7 %collective-permute-start.12 = (bf16[16,1024]{1,0:T(8,128)(2,1)S(1)}, bf16[16,1024]{1,0:T(8,128)(2,1)S(1)}, u32[]{:S(2)}, u32[]{:S(2)}) collective-permute-start(bf16[16,1024]{1,0:T(8,128)(2,1)S(1)} %get-tuple-element.61), channel_id=1, source_target_pairs={{0,2},{1,3},{2,0},{3,1},{4,6},{5,7},{6,4},{7,5},{8,10},{9,11},{10,... | collective-permute-start | bytes 98312 | tf_op jit(solution)/shard_map/ppermute | solution.py:195
  31.2 5.3 %collective-permute-start.13 = (bf16[16,1024]{1,0:T(8,128)(2,1)S(1)}, bf16[16,1024]{1,0:T(8,128)(2,1)S(1)}, u32[]{:S(2)}, u32[]{:S(2)}) collective-permute-start(bf16[16,1024]{1,0:T(8,128)(2,1)S(1)} %get-tuple-element.62), channel_id=1, source_target_pairs={{0,4},{1,5},{2,6},{3,7},{4,0},{5,1},{6,2},{7,3},{8,12},{9,13},{10,... | collective-permute-start | bytes 98312 | tf_op jit(solution)/shard_map/ppermute | solution.py:195
  31.2 5.8 %collective-permute-start.14 = (bf16[16,1024]{1,0:T(8,128)(2,1)S(1)}, bf16[16,1024]{1,0:T(8,128)(2,1)S(1)}, u32[]{:S(2)}, u32[]{:S(2)}) collective-permute-start(bf16[16,1024]{1,0:T(8,128)(2,1)S(1)} %get-tuple-element.63), channel_id=1, source_target_pairs={{0,6},{1,7},{2,4},{3,5},{4,2},{5,3},{6,0},{7,1},{8,14},{9,15},{10,... | collective-permute-start | bytes 98312 | tf_op jit(solution)/shard_map/ppermute | solution.py:195
  33.6 4.5 %collective-permute-start.15 = (bf16[16,1024]{1,0:T(8,128)(2,1)S(1)}, bf16[16,1024]{1,0:T(8,128)(2,1)S(1)}, u32[]{:S(2)}, u32[]{:S(2)}) collective-permute-start(bf16[16,1024]{1,0:T(8,128)(2,1)S(1)} %get-tuple-element.60.refs_0_), channel_id=1, source_target_pairs={{0,1},{1,0},{2,3},{3,2},{4,5},{5,4},{6,7},{7,6},{8,9},{9,8},{10,11... | collective-permute-start | bytes 98312 | tf_op jit(solution)/shard_map/ppermute | solution.py:195
  33.6 4.5 %collective-permute-start.16 = (bf16[16,1024]{1,0:T(8,128)(2,1)S(1)}, bf16[16,1024]{1,0:T(8,128)(2,1)S(1)}, u32[]{:S(2)}, u32[]{:S(2)}) collective-permute-start(bf16[16,1024]{1,0:T(8,128)(2,1)S(1)} %collective-permute-done.12.refs_1_), channel_id=1, source_target_pairs={{0,1},{1,0},{2,3},{3,2},{4,5},{5,4},{6,7},{7,6},{8,9},{9,8},{10,11... | collective-permute-start | bytes 98312 | tf_op jit(solution)/shard_map/ppermute | solution.py:195
  39.1 4.5 %collective-permute-start.20 = (bf16[8,2048]{1,0:T(8,128)(2,1)S(1)}, bf16[8,2048]{1,0:T(8,128)(2,1)S(1)}, u32[]{:S(2)}, u32[]{:S(2)}) collective-permute-start(bf16[8,2048]{1,0:T(8,128)(2,1)S(1)} %shard_map.215.refs_0_), channel_id=1, source_target_pairs={{0,2},{1,3},{2,0},{3,1},{4,6},{5,7},{6,4},{7,5},{8,10},{9,11},{10,... | collective-permute-start | bytes 98312 | tf_op jit(solution)/shard_map/ppermute | solution.py:195
  39.8 5.8 %collective-permute-start.22 = (bf16[8,2048]{1,0:T(8,128)(2,1)S(1)}, bf16[8,2048]{1,0:T(8,128)(2,1)S(1)}, u32[]{:S(2)}, u32[]{:S(2)}) collective-permute-start(bf16[8,2048]{1,0:T(8,128)(2,1)S(1)} %shard_map.215.refs_0_), channel_id=1, source_target_pairs={{0,4},{1,5},{2,6},{3,7},{4,0},{5,1},{6,2},{7,3},{8,12},{9,13},{10,... | collective-permute-start | bytes 98312 | tf_op jit(solution)/shard_map/ppermute | solution.py:195
  42.0 5.7 %collective-permute-start.24 = (bf16[8,2048]{1,0:T(8,128)(2,1)S(1)}, bf16[8,2048]{1,0:T(8,128)(2,1)S(1)}, u32[]{:S(2)}, u32[]{:S(2)}) collective-permute-start(bf16[8,2048]{1,0:T(8,128)(2,1)S(1)} %shard_map.215.refs_0_), channel_id=1, source_target_pairs={{0,6},{1,7},{2,4},{3,5},{4,2},{5,3},{6,0},{7,1},{8,14},{9,15},{10,... | collective-permute-start | bytes 98312 | tf_op jit(solution)/shard_map/ppermute | solution.py:195
  43.5 4.2 %collective-permute-start.19 = (bf16[8,2048]{1,0:T(8,128)(2,1)S(1)}, bf16[8,2048]{1,0:T(8,128)(2,1)S(1)}, u32[]{:S(2)}, u32[]{:S(2)}) collective-permute-start(bf16[8,2048]{1,0:T(8,128)(2,1)S(1)} %shard_map.215.refs_0_), channel_id=1, source_target_pairs={{0,1},{1,0},{2,3},{3,2},{4,5},{5,4},{6,7},{7,6},{8,9},{9,8},{10,11... | collective-permute-start | bytes 98312 | tf_op jit(solution)/shard_map/ppermute | solution.py:195
  43.5 4.2 %collective-permute-start.21 = (bf16[8,2048]{1,0:T(8,128)(2,1)S(1)}, bf16[8,2048]{1,0:T(8,128)(2,1)S(1)}, u32[]{:S(2)}, u32[]{:S(2)}) collective-permute-start(bf16[8,2048]{1,0:T(8,128)(2,1)S(1)} %collective-permute-done.20.refs_2_), channel_id=1, source_target_pairs={{0,1},{1,0},{2,3},{3,2},{4,5},{5,4},{6,7},{7,6},{8,9},{9,8},{10,11... | collective-permute-start | bytes 98312 | tf_op jit(solution)/shard_map/ppermute | solution.py:195
  49.3 5.8 %collective-permute-start.31 = (bf16[64,256]{1,0:T(8,128)(2,1)S(1)}, bf16[64,256]{1,0:T(8,128)(2,1)S(1)}, u32[]{:S(2)}, u32[]{:S(2)}) collective-permute-start(bf16[64,256]{1,0:T(8,128)(2,1)S(1)} %shard_map.216.refs_0_.base_ref), channel_id=1, source_target_pairs={{0,6},{1,7},{2,4},{3,5},{4,2},{5,3},{6,0},{7,1},{8,14},{9,15},{10,... | collective-permute-start | bytes 98312 | tf_op jit(solution)/shard_map/ppermute | solution.py:195
  50.8 4.5 %collective-permute-start.26 = (bf16[64,256]{1,0:T(8,128)(2,1)S(1)}, bf16[64,256]{1,0:T(8,128)(2,1)S(1)}, u32[]{:S(2)}, u32[]{:S(2)}) collective-permute-start(bf16[64,256]{1,0:T(8,128)(2,1)S(1)} %shard_map.216.refs_0_.base_ref), channel_id=1, source_target_pairs={{0,2},{1,3},{2,0},{3,1},{4,6},{5,7},{6,4},{7,5},{8,10},{9,11},{10,... | collective-permute-start | bytes 98312 | tf_op jit(solution)/shard_map/ppermute | solution.py:195
  50.8 5.2 %collective-permute-start.28 = (bf16[64,256]{1,0:T(8,128)(2,1)S(1)}, bf16[64,256]{1,0:T(8,128)(2,1)S(1)}, u32[]{:S(2)}, u32[]{:S(2)}) collective-permute-start(bf16[64,256]{1,0:T(8,128)(2,1)S(1)} %shard_map.216.refs_0_.base_ref), channel_id=1, source_target_pairs={{0,4},{1,5},{2,6},{3,7},{4,0},{5,1},{6,2},{7,3},{8,12},{9,13},{10,... | collective-permute-start | bytes 98312 | tf_op jit(solution)/shard_map/ppermute | solution.py:195
  59.5 5.8 %collective-permute-start.34 = (bf16[64,256]{1,0:T(8,128)(2,1)S(1)}, bf16[64,256]{1,0:T(8,128)(2,1)S(1)}, u32[]{:S(2)}, u32[]{:S(2)}) collective-permute-start(bf16[64,256]{1,0:T(8,128)(2,1)S(1)} %get-tuple-element.77), channel_id=1, source_target_pairs={{0,2},{1,3},{2,0},{3,1},{4,6},{5,7},{6,4},{7,5},{8,10},{9,11},{10,... | collective-permute-start | bytes 98312 | tf_op jit(solution)/shard_map/ppermute | solution.py:195
  61.1 5.4 %collective-permute-start.35 = (bf16[64,256]{1,0:T(8,128)(2,1)S(1)}, bf16[64,256]{1,0:T(8,128)(2,1)S(1)}, u32[]{:S(2)}, u32[]{:S(2)}) collective-permute-start(bf16[64,256]{1,0:T(8,128)(2,1)S(1)} %get-tuple-element.78), channel_id=1, source_target_pairs={{0,4},{1,5},{2,6},{3,7},{4,0},{5,1},{6,2},{7,3},{8,12},{9,13},{10,... | collective-permute-start | bytes 98312 | tf_op jit(solution)/shard_map/ppermute | solution.py:195
  62.4 5.7 %collective-permute-start.36 = (bf16[64,256]{1,0:T(8,128)(2,1)S(1)}, bf16[64,256]{1,0:T(8,128)(2,1)S(1)}, u32[]{:S(2)}, u32[]{:S(2)}) collective-permute-start(bf16[64,256]{1,0:T(8,128)(2,1)S(1)} %get-tuple-element.79), channel_id=1, source_target_pairs={{0,6},{1,7},{2,4},{3,5},{4,2},{5,3},{6,0},{7,1},{8,14},{9,15},{10,... | collective-permute-start | bytes 98312 | tf_op jit(solution)/shard_map/ppermute | solution.py:195
  (33 other events, 448.1 us)

commit v7 on v6

--- a/solution.py
+++ b/solution.py
@@ -169,6 +169,7 @@
 VMEM_SPEC = pl.BlockSpec(memory_space=pltpu.VMEM)
 HBM_SPEC = pl.BlockSpec(memory_space=pltpu.HBM)
 GROUP = ("kv", "tp")
+CROSSED = ("ex_e",)
 LIVE_HALVES = 7
 F32, BF16 = jnp.float32, jnp.bfloat16
 
@@ -202,16 +203,26 @@
     return received
 
 
-def pair_up(near, count):
+def pair_up(near, count, known=()):
     blocks = []
-    for block in near:
+    for step, block in enumerate(near):
+        if step in known:
+            blocks += [block, known[step]]
+            continue
         blocks += [block, swap(block, 1, count)]
     return blocks
 
 
-def gather_blocks(own, count):
-    near = [own] + far_swaps([own] * (count // 2 - 1), count)
-    return pair_up(near, count)
+def exchange_blocks(sends, count, label):
+    near = [sends[0]] + far_swaps(sends[1:], count)
+    if label not in CROSSED:
+        return pair_up(near, count)
+    nearest = swap(sends[1], 3, count)
+    return pair_up(near, count, {1: nearest})
+
+
+def gather_blocks(own, count, label):
+    return exchange_blocks([own] * (count // 2), count, label)
 
 
 def entry_kernel(length_ref, tokens_hbm, gain_hbm, gate_hbm, up_hbm, down_hbm, *refs):
@@ -268,9 +279,8 @@
     return part if total is None else total + part
 
 
-def early_masks(count):
-    late = (3, 5) if count > 4 else (3,)
-    return [m for m in range(count) if m not in late], list(late)
+def mask_groups(count):
+    return [], [m for m in range(count) if m not in (3, 5)], [3, 5]
 
 
 def units_of(blocks, masks, gain_ref, gate_ref, up_ref, span, skip, row_count):
@@ -292,10 +302,13 @@
 
 def ffn_early_kernel(masks, span, skip, *refs):
     blocks = refs[: len(masks)]
-    gain_ref, gate_ref, up_ref, _, gate_out, up_out, squares_out = refs[len(masks) :]
-    gate_out[...], up_out[...], squares_out[...] = units_of(
-        blocks, masks, gain_ref, gate_ref, up_ref, span, skip, gate_out.shape[0]
-    )
+    gain_ref, gate_ref, up_ref, _, *carried = refs[len(masks) :]
+    outs, before = carried[-3:], carried[:-3]
+    found = units_of(
+        blocks, masks, gain_ref, gate_ref, up_ref, span, skip, outs[0].shape[0]
+    )
+    for place, (out, part) in enumerate(zip(outs, found)):
+        out[...] = part + before[place][...] if before else part
 
 
 def ffn_late_kernel(masks, count, span, skip, *refs):
@@ -361,7 +374,8 @@
     pick_ref[...] = (rank == wanted).astype(F32).astype(BF16)
 
 
-def spread_kernel(near, pick_ref, own_ref, cross_ref, mine_ref, kept_ref, *sends):
+def spread_kernel(near, live_rows, pick_ref, own_ref, cross_ref, mine_ref, kept_ref, *sends):
+    *sends, packed_ref = sends
     pick = pick_ref[...]
     packed = pick.shape[0]
     rows = own_ref.shape[1]
@@ -373,17 +387,18 @@
         high, low = parts(total)
         upper = jnp.dot(pick, high, preferred_element_type=F32)
         whole.append(high)
-        chosen.append(upper.astype(BF16))
+        chosen.append(upper)
         if step:
             kept_ref[step - 1] = upper + jnp.dot(pick, low, preferred_element_type=F32)
     for step, send in enumerate(sends, 1):
         send[pl.ds(0, rows), :] = whole[step]
         others = [other for other in range(near) if other != step]
         for place, other in enumerate(others):
-            send[pl.ds(rows + place * packed, packed), :] = chosen[other]
-
-
-def collect_kernel(near, *refs):
+            packed_ref[pl.ds(place * live_rows, packed), :] = chosen[other]
+        send[pl.ds(rows, packed_ref.shape[0]), :] = packed_ref[...].astype(BF16)
+
+
+def collect_kernel(near, live_rows, *refs):
     pick_ref, mine_ref, kept_ref = refs[:3]
     tokens, received = refs[3 : 3 + near], refs[3 + near : 2 + 2 * near]
     after_ref, near_ref = refs[2 + 2 * near :]
@@ -397,11 +412,12 @@
     after = (base + 0.5 * total).astype(BF16)
     after_ref[...] = after
     near_ref[0] = jnp.dot(pick, after, preferred_element_type=F32).astype(BF16)
+    tails = [part[pl.ds(rows, part.shape[0] - rows), :].astype(F32) for part in received]
     for step in range(1, near):
         total = kept_ref[step - 1]
-        for sender, part in enumerate(received, 1):
+        for sender, tail in enumerate(tails, 1):
             place = [other for other in range(near) if other != sender].index(sender ^ step)
-            total = total + part[pl.ds(rows + place * packed, packed), :].astype(F32)
+            total = total + tail[place * live_rows : place * live_rows + packed]
         base = jnp.dot(pick, tokens[step][pl.ds(0, rows), :], preferred_element_type=F32)
         near_ref[step] = (base + 0.5 * total).astype(BF16)
 
@@ -410,12 +426,14 @@
     near = count // 2
     width = blocks[0].shape[1]
     span, skip = core_span(down.shape[0])
-    early, late = early_masks(count)
-    parts_early = call(
-        functools.partial(ffn_early_kernel, early, span, skip),
-        [pltpu.VMEM((rows, span), F32)] * 2 + [pltpu.VMEM((rows, 128), F32)],
-        [*(blocks[m] for m in early), gain, gate, up, down],
-    )
+    _, early, late = mask_groups(count)
+    parts_early = []
+    for masks in (early,):
+        parts_early = call(
+            functools.partial(ffn_early_kernel, masks, span, skip),
+            [pltpu.VMEM((rows, span), F32)] * 2 + [pltpu.VMEM((rows, 128), F32)],
+            [*(blocks[m] for m in masks), gain, gate, up, down, *parts_early],
+        )
     hidden, cross_part = call(
         functools.partial(ffn_late_kernel, late, count, span, skip),
         [pltpu.VMEM((rows, span), BF16), pltpu.VMEM((near, rows, width), BF16)],
@@ -433,23 +451,27 @@
 def first_half_step(tokens, rows, count, gain, gate, up, down):
     near = count // 2
     width = tokens.shape[1]
-    blocks = gather_blocks(tokens, count)
+    blocks = gather_blocks(tokens, count, "ex_a")
     own_part, cross_sum = hidden_sums(blocks, rows, count, gain, gate, up, down)
     live_rows = count * LIVE_HALVES // 2
     packed = -(-live_rows // 16) * 16
     pick = call(
-        functools.partial(live_kernel, count, rows), pltpu.VMEM((packed, rows), BF16), blocks
-    )
-    sent = rows + (near - 1) * packed
+        functools.partial(live_kernel, count, rows),
+        pltpu.VMEM((packed, rows), BF16),
+        blocks,
+    )
+    tail = -(-((near - 2) * live_rows + packed) // BLK) * BLK
+    sent = rows + tail
     mine, kept, *sends = call(
-        functools.partial(spread_kernel, near),
+        functools.partial(spread_kernel, near, live_rows),
         [pltpu.VMEM((rows, width), F32), pltpu.VMEM((near - 1, packed, width), F32)]
         + [pltpu.VMEM((sent, width), BF16)] * (near - 1),
         [pick, own_part, cross_sum],
+        scratch=[pltpu.VMEM((tail, width), F32)],
     )
     received = far_swaps(sends, count)
     after, near_live = call(
-        functools.partial(collect_kernel, near),
+        functools.partial(collect_kernel, near, live_rows),
         [pltpu.VMEM((rows, width), BF16), pltpu.VMEM((near, packed, width), BF16)],
         [pick, mine, kept, *blocks[::2], *received],
     )
@@ -460,7 +482,7 @@
     rows, width = own.shape
     near = count // 2
     gain = gain.reshape(1, count * width)
-    blocks = gather_blocks(own, count)
+    blocks = gather_blocks(own, count, "ex_f")
     own_part, cross_sum = hidden_sums(blocks, rows, count, gain, gate, up, down)
     mine, *sends = call(
         pair_sum_kernel,
@@ -468,7 +490,11 @@
         [own_part, cross_sum],
     )
     received = far_swaps(sends, count)
-    return call(residual_kernel, jax.ShapeDtypeStruct((rows, width), BF16), [own, mine, *received])
+    return call(
+        residual_kernel,
+        jax.ShapeDtypeStruct((rows, width), BF16),
+        [own, mine, *received],
+    )
 
 
 def mixes_of(blocks, masks, gain_ref, weights, thin):
@@ -551,10 +577,10 @@
     live_ref[...] = (step_of < length_ref[...]).astype(F32)
 
 
-def delta_kernel(masks, count, *refs):
+def delta_kernel(masks, count, joined, *refs):
     blocks = refs[: len(masks)]
     pre_ref, rate_ref, live_ref, high_ref, low_ref = refs[len(masks) : len(masks) + 5]
-    mixed_ref, update_ref, faded_ref, final_ref = refs[len(masks) + 5 :]
+    *before, mixed_ref, update_ref, faded_ref, final_ref = refs[len(masks) + 5 :]
     index = my_index()
     first_core = lax.axis_index("tp") == 0
     size = high_ref.shape[-1]
@@ -632,21 +658,17 @@
     normed = attend * lax.rsqrt(lane_sum(attend * attend) / size + EPSILON)
     normed = (normed * (gating * jax.nn.sigmoid(gating)) * live_col).astype(BF16)
     final = jnp.broadcast_to(cum[:, BLK - 1 :, :], cum.shape)
-    for head in range(heads):
-        mixed_ref[:, head * size : (head + 1) * size] = normed[head]
+    for place, mask in enumerate(masks):
+        block = jnp.concatenate([normed[place * per_block + e] for e in range(per_block)], axis=1)
+        if not joined:
+            mixed_ref[:, place * width : (place + 1) * width] = block
+            continue
+        mixed_ref[:, pl.ds(pl.multiple_of((index ^ mask) * width, width), width)] = block
+        column = pl.multiple_of((index ^ mask ^ 1) * width, width)
+        mixed_ref[:, pl.ds(column, width)] = before[0][:, place * width : (place + 1) * width]
     update_ref[...] = update.reshape(rows, size)
     faded_ref[...] = (key_unit * jnp.exp(final - cum)).reshape(rows, size)
     final_ref[...] = jnp.exp(final).reshape(rows, size)
-
-
-def join_kernel(count, first_ref, second_ref, mixed_ref):
-    width = mixed_ref.shape[1] // count
-    index = my_index()
-    for mask in range(count):
-        source = second_ref if mask % 2 else first_ref
-        place = mask // 2
-        column = pl.multiple_of((index ^ mask) * width, width)
-        mixed_ref[:, pl.ds(column, width)] = source[:, place * width : (place + 1) * width]
 
 
 def state_kernel(groups, count, *refs):
@@ -744,7 +766,7 @@
         [cross_live, *mixers, *parts_early, pick],
         scratch=[pltpu.VMEM((rows, columns), F32), pltpu.VMEM((rows, 2 * heads), F32)],
     )
-    owned = pair_up([sends[0]] + far_swaps(sends[1:], count), count)
+    owned = exchange_blocks(sends, count, "ex_d")
     matrices = state.reshape(heads, size, size)
     high, low, live = call(
         split_state_kernel,
@@ -754,11 +776,11 @@
     )
     groups = [list(range(0, count, 2)), list(range(1, count, 2))]
     mixed_parts, grown = [], []
-    for masks in groups:
+    for place, masks in enumerate(groups):
         tall = heads * BLK // 2
         part, *rest = call(
-            functools.partial(delta_kernel, masks, count),
-            [pltpu.VMEM((BLK, channels // 2), BF16)] + [pltpu.VMEM((tall, size), F32)] * 3,
+            functools.partial(delta_kernel, masks, count, bool(place)),
+            [pltpu.VMEM((BLK, channels // (2 - place)), BF16)] + [pltpu.VMEM((tall, size), F32)] * 3,
             [
                 *(owned[m] for m in masks),
                 pre,
@@ -766,14 +788,13 @@
                 live,
                 high,
                 low,
+                *mixed_parts,
             ],
         )
         mixed_parts.append(part)
         grown += rest
-    mixed = call(
-        functools.partial(join_kernel, count), pltpu.VMEM((BLK, channels), BF16), mixed_parts
-    )
-    head_blocks = gather_blocks(mixed, count)
+    mixed = mixed_parts[1]
+    head_blocks = gather_blocks(mixed, count, "ex_e")
     new_state = call(
         functools.partial(state_kernel, groups, count),
         jax.ShapeDtypeStruct((heads, size, size), F32),

time: 68.9 us -> 66.9 us (0.971)
  waiting for transfers between devices: 25.3 us -> 23.4 us
    ppermute x37, waiting for transfers between devices: 25.3 us -> 23.4 us  [swap(): return lax.ppermute(value, GROUP, [(i, i ^ mask) for i in range(count)])]
    pallas_call x20 -> x19, Pallas kernels: 11.1 us -> 11.1 us  [call(): pl.pallas_call(body, out_shape=shapes, in_specs=in_specs or [VMEM_SPEC] *...]
  transfers between devices with their start and end apart: 37 -> 37, of which waited for: 21 -> 20; matrix products, arithmetic and copies ran while one was open for 0% -> 0% of each run, Pallas kernels for 8% -> 9%
where the time goes in v7:
time: 66.9 us; the launch traced here: 66.7 us
  starting transfers between devices  30.4 us (45%)
  waiting for transfers between devices  23.4 us (35%)
  Pallas kernels  11.1 us (17%)
  between operations  1.73 us (3%)
    ppermute x37, starting transfers between devices, swap(): return lax.ppermute(value, GROUP, [(i, i ^ mask) for i in range(count)])  30.4 us
    ppermute x37, waiting for transfers between devices, swap(): return lax.ppermute(value, GROUP, [(i, i ^ mask) for i in range(count)])  23.4 us
    pallas_call x19, Pallas kernels, call(): pl.pallas_call(body, out_shape=shapes, in_specs=in_specs or [VMEM_SPEC] *...  11.1 us
  transfers between devices with their start and end apart: 37, of which 20 were waited for; matrix products, arithmetic and copies ran while one was open for 0% of the time, Pallas kernels for 9%

profile of v7, /device:TPU:0, one launch (start us, length us, event | category | flops | bytes accessed | tf_op | source)
XLA Modules:
  0.0 66.7 jit_solution(17928943618316253708)
XLA Ops:
  2.2 5.1 %collective-permute-start.5 = (bf16[72,256]{1,0:T(8,128)(2,1)S(1)}, bf16[72,256]{1,0:T(8,128)(2,1)S(1)}, u32[]{:S(2)}, u32[]{:S(2)}) collective-permute-start(bf16[72,256]{1,0:T(8,128)(2,1)S(1)} %get-tuple-element.44.refs_0_.refs_3_), channel_id=1, source_target_pairs={{0,6},{1,7},{2,4},{3,5},{4,2},{5,3},{6,0},{7,1},{8,14},{9,15},{10,... | collective-permute-start | bytes 110600 | tf_op jit(solution)/shard_map/ppermute | solution.py:196
  8.0 1.3 %collective-permute-done.5.refs_6_.refs_4_ = bf16[72,256]{1,0:T(8,128)(2,1)S(1)} collective-permute-done((bf16[72,256]{1,0:T(8,128)(2,1)S(1)}, bf16[72,256]{1,0:T(8,128)(2,1)S(1)}, u32[]{:S(2)}, u32[]{:S(2)}) %collective-permute-start.5) | collective-permute-done | bytes 36896 | tf_op jit(solution)/shard_map/ppermute | solution.py:196
  9.3 2.9 %collective-permute-done.3.refs_4_.refs_3_.refs_5_ = bf16[72,256]{1,0:T(8,128)(2,1)S(1)} collective-permute-done((bf16[72,256]{1,0:T(8,128)(2,1)S(1)}, bf16[72,256]{1,0:T(8,128)(2,1)S(1)}, u32[]{:S(2)}, u32[]{:S(2)}) %collective-permute-start.3) | collective-permute-done | bytes 36896 | tf_op jit(solution)/shard_map/ppermute | solution.py:196
  16.3 2.2 %collective-permute-start.9 = (bf16[152,256]{1,0:T(8,128)(2,1)S(1)}, bf16[152,256]{1,0:T(8,128)(2,1)S(1)}, u32[]{:S(2)}, u32[]{:S(2)}) collective-permute-start(bf16[152,256]{1,0:T(8,128)(2,1)S(1)} %get-tuple-element.54), channel_id=1, source_target_pairs={{0,4},{1,5},{2,6},{3,7},{4,0},{5,1},{6,2},{7,3},{8,12},{9,13},{10,... | collective-permute-start | bytes 233480 | tf_op jit(solution)/shard_map/ppermute | solution.py:196
  18.5 2.2 %collective-permute-start.10 = (bf16[152,256]{1,0:T(8,128)(2,1)S(1)}, bf16[152,256]{1,0:T(8,128)(2,1)S(1)}, u32[]{:S(2)}, u32[]{:S(2)}) collective-permute-start(bf16[152,256]{1,0:T(8,128)(2,1)S(1)} %get-tuple-element.55), channel_id=1, source_target_pairs={{0,6},{1,7},{2,4},{3,5},{4,2},{5,3},{6,0},{7,1},{8,14},{9,15},{10,... | collective-permute-start | bytes 233480 | tf_op jit(solution)/shard_map/ppermute | solution.py:196
  20.7 1.7 %collective-permute-done.8.refs_7_ = bf16[152,256]{1,0:T(8,128)(2,1)S(1)} collective-permute-done((bf16[152,256]{1,0:T(8,128)(2,1)S(1)}, bf16[152,256]{1,0:T(8,128)(2,1)S(1)}, u32[]{:S(2)}, u32[]{:S(2)}) %collective-permute-start.8) | collective-permute-done | bytes 77856 | tf_op jit(solution)/shard_map/ppermute | solution.py:196
  22.5 2.9 %collective-permute-done.10.refs_9_ = bf16[152,256]{1,0:T(8,128)(2,1)S(1)} collective-permute-done((bf16[152,256]{1,0:T(8,128)(2,1)S(1)}, bf16[152,256]{1,0:T(8,128)(2,1)S(1)}, u32[]{:S(2)}, u32[]{:S(2)}) %collective-permute-start.10) | collective-permute-done | bytes 77856 | tf_op jit(solution)/shard_map/ppermute | solution.py:196
  27.7 1.9 %collective-permute-start.13 = (bf16[16,1024]{1,0:T(8,128)(2,1)S(1)}, bf16[16,1024]{1,0:T(8,128)(2,1)S(1)}, u32[]{:S(2)}, u32[]{:S(2)}) collective-permute-start(bf16[16,1024]{1,0:T(8,128)(2,1)S(1)} %get-tuple-element.61), channel_id=1, source_target_pairs={{0,2},{1,3},{2,0},{3,1},{4,6},{5,7},{6,4},{7,5},{8,10},{9,11},{10,... | collective-permute-start | bytes 98312 | tf_op jit(solution)/shard_map/ppermute | solution.py:196
  29.6 1.3 %collective-permute-start.15 = (bf16[16,1024]{1,0:T(8,128)(2,1)S(1)}, bf16[16,1024]{1,0:T(8,128)(2,1)S(1)}, u32[]{:S(2)}, u32[]{:S(2)}) collective-permute-start(bf16[16,1024]{1,0:T(8,128)(2,1)S(1)} %get-tuple-element.62), channel_id=1, source_target_pairs={{0,4},{1,5},{2,6},{3,7},{4,0},{5,1},{6,2},{7,3},{8,12},{9,13},{10,... | collective-permute-start | bytes 98312 | tf_op jit(solution)/shard_map/ppermute | solution.py:196
  31.0 1.4 %collective-permute-start.17 = (bf16[16,1024]{1,0:T(8,128)(2,1)S(1)}, bf16[16,1024]{1,0:T(8,128)(2,1)S(1)}, u32[]{:S(2)}, u32[]{:S(2)}) collective-permute-start(bf16[16,1024]{1,0:T(8,128)(2,1)S(1)} %get-tuple-element.63), channel_id=1, source_target_pairs={{0,6},{1,7},{2,4},{3,5},{4,2},{5,3},{6,0},{7,1},{8,14},{9,15},{10,... | collective-permute-start | bytes 98312 | tf_op jit(solution)/shard_map/ppermute | solution.py:196
  32.9 2.0 %collective-permute-done.15.refs_2_ = bf16[16,1024]{1,0:T(8,128)(2,1)S(1)} collective-permute-done((bf16[16,1024]{1,0:T(8,128)(2,1)S(1)}, bf16[16,1024]{1,0:T(8,128)(2,1)S(1)}, u32[]{:S(2)}, u32[]{:S(2)}) %collective-permute-start.15) | collective-permute-done | bytes 32800 | tf_op jit(solution)/shard_map/ppermute | solution.py:196
  34.9 1.8 %collective-permute-done.17.refs_3_ = bf16[16,1024]{1,0:T(8,128)(2,1)S(1)} collective-permute-done((bf16[16,1024]{1,0:T(8,128)(2,1)S(1)}, bf16[16,1024]{1,0:T(8,128)(2,1)S(1)}, u32[]{:S(2)}, u32[]{:S(2)}) %collective-permute-start.17) | collective-permute-done | bytes 32800 | tf_op jit(solution)/shard_map/ppermute | solution.py:196
  38.7 1.6 %collective-permute-start.24 = (bf16[8,2048]{1,0:T(8,128)(2,1)S(1)}, bf16[8,2048]{1,0:T(8,128)(2,1)S(1)}, u32[]{:S(2)}, u32[]{:S(2)}) collective-permute-start(bf16[8,2048]{1,0:T(8,128)(2,1)S(1)} %get-tuple-element.69.refs_0_), channel_id=1, source_target_pairs={{0,6},{1,7},{2,4},{3,5},{4,2},{5,3},{6,0},{7,1},{8,14},{9,15},{10,... | collective-permute-start | bytes 98312 | tf_op jit(solution)/shard_map/ppermute | solution.py:196
  40.4 2.3 %collective-permute-start.21 = (bf16[8,2048]{1,0:T(8,128)(2,1)S(1)}, bf16[8,2048]{1,0:T(8,128)(2,1)S(1)}, u32[]{:S(2)}, u32[]{:S(2)}) collective-permute-start(bf16[8,2048]{1,0:T(8,128)(2,1)S(1)} %get-tuple-element.69.refs_0_), channel_id=1, source_target_pairs={{0,3},{1,2},{2,1},{3,0},{4,7},{5,6},{6,5},{7,4},{8,11},{9,10},{10,... | collective-permute-start | bytes 98312 | tf_op jit(solution)/shard_map/ppermute | solution.py:196
  43.3 1.4 %collective-permute-done.24.refs_6_ = bf16[8,2048]{1,0:T(8,128)(2,1)S(1)} collective-permute-done((bf16[8,2048]{1,0:T(8,128)(2,1)S(1)}, bf16[8,2048]{1,0:T(8,128)(2,1)S(1)}, u32[]{:S(2)}, u32[]{:S(2)}) %collective-permute-start.24) | collective-permute-done | bytes 32800 | tf_op jit(solution)/shard_map/ppermute | solution.py:196
  47.2 1.8 %collective-permute-start.31 = (bf16[64,256]{1,0:T(8,128)(2,1)S(1)}, bf16[64,256]{1,0:T(8,128)(2,1)S(1)}, u32[]{:S(2)}, u32[]{:S(2)}) collective-permute-start(bf16[64,256]{1,0:T(8,128)(2,1)S(1)} %shard_map.215.refs_0_.base_ref), channel_id=1, source_target_pairs={{0,6},{1,7},{2,4},{3,5},{4,2},{5,3},{6,0},{7,1},{8,14},{9,15},{10,... | collective-permute-start | bytes 98312 | tf_op jit(solution)/shard_map/ppermute | solution.py:196
  49.4 2.3 %collective-permute-start.26 = (bf16[64,256]{1,0:T(8,128)(2,1)S(1)}, bf16[64,256]{1,0:T(8,128)(2,1)S(1)}, u32[]{:S(2)}, u32[]{:S(2)}) collective-permute-start(bf16[64,256]{1,0:T(8,128)(2,1)S(1)} %shard_map.215.refs_0_.base_ref), channel_id=1, source_target_pairs={{0,2},{1,3},{2,0},{3,1},{4,6},{5,7},{6,4},{7,5},{8,10},{9,11},{10,... | collective-permute-start | bytes 98312 | tf_op jit(solution)/shard_map/ppermute | solution.py:196
  51.7 1.3 %collective-permute-done.31.refs_4_ = bf16[64,256]{1,0:T(8,128)(2,1)S(1)} collective-permute-done((bf16[64,256]{1,0:T(8,128)(2,1)S(1)}, bf16[64,256]{1,0:T(8,128)(2,1)S(1)}, u32[]{:S(2)}, u32[]{:S(2)}) %collective-permute-start.31) | collective-permute-done | bytes 32800 | tf_op jit(solution)/shard_map/ppermute | solution.py:196
  57.7 1.3 %collective-permute-start.34 = (bf16[64,256]{1,0:T(8,128)(2,1)S(1)}, bf16[64,256]{1,0:T(8,128)(2,1)S(1)}, u32[]{:S(2)}, u32[]{:S(2)}) collective-permute-start(bf16[64,256]{1,0:T(8,128)(2,1)S(1)} %get-tuple-element.77), channel_id=1, source_target_pairs={{0,2},{1,3},{2,0},{3,1},{4,6},{5,7},{6,4},{7,5},{8,10},{9,11},{10,... | collective-permute-start | bytes 98312 | tf_op jit(solution)/shard_map/ppermute | solution.py:196
  59.1 1.3 %collective-permute-start.35 = (bf16[64,256]{1,0:T(8,128)(2,1)S(1)}, bf16[64,256]{1,0:T(8,128)(2,1)S(1)}, u32[]{:S(2)}, u32[]{:S(2)}) collective-permute-start(bf16[64,256]{1,0:T(8,128)(2,1)S(1)} %get-tuple-element.78), channel_id=1, source_target_pairs={{0,4},{1,5},{2,6},{3,7},{4,0},{5,1},{6,2},{7,3},{8,12},{9,13},{10,... | collective-permute-start | bytes 98312 | tf_op jit(solution)/shard_map/ppermute | solution.py:196
  60.3 1.8 %collective-permute-start.36 = (bf16[64,256]{1,0:T(8,128)(2,1)S(1)}, bf16[64,256]{1,0:T(8,128)(2,1)S(1)}, u32[]{:S(2)}, u32[]{:S(2)}) collective-permute-start(bf16[64,256]{1,0:T(8,128)(2,1)S(1)} %get-tuple-element.79), channel_id=1, source_target_pairs={{0,6},{1,7},{2,4},{3,5},{4,2},{5,3},{6,0},{7,1},{8,14},{9,15},{10,... | collective-permute-start | bytes 98312 | tf_op jit(solution)/shard_map/ppermute | solution.py:196
  62.2 1.3 %shard_map.221 = f32[16,128,128]{2,1,0:T(8,128)} custom-call(f32[64,128]{1,0:T(8,128)S(1)} %get-tuple-element.80.refs_0_, f32[64,128]{1,0:T(8,128)S(1)} %get-tuple-element.81.refs_1_, f32[64,128]{1,0:T(8,128)S(1)} %get-tuple-element.82.refs_2_, f32[64,128]{1,0:T(8,128)S(1)} %get-tuple-element.83.refs_3_, f32[64,128]{1,0:T(8,128)S(1)} %get-tuple-element.84.refs_4_, ...), custom_call_target="tpu_custom_call" | custom-call | tf_op jit(solution)/shard_map/pallas_call | solution.py:180
  63.5 1.2 %collective-permute-done.35.refs_1_ = bf16[64,256]{1,0:T(8,128)(2,1)S(1)} collective-permute-done((bf16[64,256]{1,0:T(8,128)(2,1)S(1)}, bf16[64,256]{1,0:T(8,128)(2,1)S(1)}, u32[]{:S(2)}, u32[]{:S(2)}) %collective-permute-start.35) | collective-permute-done | bytes 32800 | tf_op jit(solution)/shard_map/ppermute | solution.py:196
  64.8 1.3 %collective-permute-done.36.refs_2_ = bf16[64,256]{1,0:T(8,128)(2,1)S(1)} collective-permute-done((bf16[64,256]{1,0:T(8,128)(2,1)S(1)}, bf16[64,256]{1,0:T(8,128)(2,1)S(1)}, u32[]{:S(2)}, u32[]{:S(2)}) %collective-permute-start.36) | collective-permute-done | bytes 32800 | tf_op jit(solution)/shard_map/ppermute | solution.py:196
  (112 shorter events, 19.2 us)
Async XLA Ops:
  2.2 7.1 %collective-permute-start.5 = (bf16[72,256]{1,0:T(8,128)(2,1)S(1)}, bf16[72,256]{1,0:T(8,128)(2,1)S(1)}, u32[]{:S(2)}, u32[]{:S(2)}) collective-permute-start(bf16[72,256]{1,0:T(8,128)(2,1)S(1)} %get-tuple-element.44.refs_0_.refs_3_), channel_id=1, source_target_pairs={{0,6},{1,7},{2,4},{3,5},{4,2},{5,3},{6,0},{7,1},{8,14},{9,15},{10,... | collective-permute-start | bytes 110600 | tf_op jit(solution)/shard_map/ppermute | solution.py:196
  7.4 4.9 %collective-permute-start.3 = (bf16[72,256]{1,0:T(8,128)(2,1)S(1)}, bf16[72,256]{1,0:T(8,128)(2,1)S(1)}, u32[]{:S(2)}, u32[]{:S(2)}) collective-permute-start(bf16[72,256]{1,0:T(8,128)(2,1)S(1)} %get-tuple-element.44.refs_0_.refs_3_), channel_id=1, source_target_pairs={{0,4},{1,5},{2,6},{3,7},{4,0},{5,1},{6,2},{7,3},{8,12},{9,13},{10,... | collective-permute-start | bytes 110600 | tf_op jit(solution)/shard_map/ppermute | solution.py:196
  7.4 4.9 %collective-permute-start.1 = (bf16[72,256]{1,0:T(8,128)(2,1)S(1)}, bf16[72,256]{1,0:T(8,128)(2,1)S(1)}, u32[]{:S(2)}, u32[]{:S(2)}) collective-permute-start(bf16[72,256]{1,0:T(8,128)(2,1)S(1)} %get-tuple-element.44.refs_0_.refs_3_), channel_id=1, source_target_pairs={{0,2},{1,3},{2,0},{3,1},{4,6},{5,7},{6,4},{7,5},{8,10},{9,11},{10,... | collective-permute-start | bytes 110600 | tf_op jit(solution)/shard_map/ppermute | solution.py:196
  8.0 4.7 %collective-permute-start = (bf16[72,256]{1,0:T(8,128)(2,1)S(1)}, bf16[72,256]{1,0:T(8,128)(2,1)S(1)}, u32[]{:S(2)}, u32[]{:S(2)}) collective-permute-start(bf16[72,256]{1,0:T(8,128)(2,1)S(1)} %get-tuple-element.44.refs_0_.refs_3_), channel_id=1, source_target_pairs={{0,1},{1,0},{2,3},{3,2},{4,5},{5,4},{6,7},{7,6},{8,9},{9,8},{10,11... | collective-permute-start | bytes 110600 | tf_op jit(solution)/shard_map/ppermute | solution.py:196
  9.3 3.4 %collective-permute-start.6 = (bf16[72,256]{1,0:T(8,128)(2,1)S(1)}, bf16[72,256]{1,0:T(8,128)(2,1)S(1)}, u32[]{:S(2)}, u32[]{:S(2)}) collective-permute-start(bf16[72,256]{1,0:T(8,128)(2,1)S(1)} %collective-permute-done.5.refs_6_.refs_4_), channel_id=1, source_target_pairs={{0,1},{1,0},{2,3},{3,2},{4,5},{5,4},{6,7},{7,6},{8,9},{9,8},{10,11... | collective-permute-start | bytes 110600 | tf_op jit(solution)/shard_map/ppermute | solution.py:196
  16.2 6.1 %collective-permute-start.8 = (bf16[152,256]{1,0:T(8,128)(2,1)S(1)}, bf16[152,256]{1,0:T(8,128)(2,1)S(1)}, u32[]{:S(2)}, u32[]{:S(2)}) collective-permute-start(bf16[152,256]{1,0:T(8,128)(2,1)S(1)} %get-tuple-element.53), channel_id=1, source_target_pairs={{0,2},{1,3},{2,0},{3,1},{4,6},{5,7},{6,4},{7,5},{8,10},{9,11},{10,... | collective-permute-start | bytes 233480 | tf_op jit(solution)/shard_map/ppermute | solution.py:196
  16.3 6.2 %collective-permute-start.9 = (bf16[152,256]{1,0:T(8,128)(2,1)S(1)}, bf16[152,256]{1,0:T(8,128)(2,1)S(1)}, u32[]{:S(2)}, u32[]{:S(2)}) collective-permute-start(bf16[152,256]{1,0:T(8,128)(2,1)S(1)} %get-tuple-element.54), channel_id=1, source_target_pairs={{0,4},{1,5},{2,6},{3,7},{4,0},{5,1},{6,2},{7,3},{8,12},{9,13},{10,... | collective-permute-start | bytes 233480 | tf_op jit(solution)/shard_map/ppermute | solution.py:196
  18.5 7.0 %collective-permute-start.10 = (bf16[152,256]{1,0:T(8,128)(2,1)S(1)}, bf16[152,256]{1,0:T(8,128)(2,1)S(1)}, u32[]{:S(2)}, u32[]{:S(2)}) collective-permute-start(bf16[152,256]{1,0:T(8,128)(2,1)S(1)} %get-tuple-element.55), channel_id=1, source_target_pairs={{0,6},{1,7},{2,4},{3,5},{4,2},{5,3},{6,0},{7,1},{8,14},{9,15},{10,... | collective-permute-start | bytes 233480 | tf_op jit(solution)/shard_map/ppermute | solution.py:196
  27.7 4.7 %collective-permute-start.13 = (bf16[16,1024]{1,0:T(8,128)(2,1)S(1)}, bf16[16,1024]{1,0:T(8,128)(2,1)S(1)}, u32[]{:S(2)}, u32[]{:S(2)}) collective-permute-start(bf16[16,1024]{1,0:T(8,128)(2,1)S(1)} %get-tuple-element.61), channel_id=1, source_target_pairs={{0,2},{1,3},{2,0},{3,1},{4,6},{5,7},{6,4},{7,5},{8,10},{9,11},{10,... | collective-permute-start | bytes 98312 | tf_op jit(solution)/shard_map/ppermute | solution.py:196
  29.6 5.3 %collective-permute-start.15 = (bf16[16,1024]{1,0:T(8,128)(2,1)S(1)}, bf16[16,1024]{1,0:T(8,128)(2,1)S(1)}, u32[]{:S(2)}, u32[]{:S(2)}) collective-permute-start(bf16[16,1024]{1,0:T(8,128)(2,1)S(1)} %get-tuple-element.62), channel_id=1, source_target_pairs={{0,4},{1,5},{2,6},{3,7},{4,0},{5,1},{6,2},{7,3},{8,12},{9,13},{10,... | collective-permute-start | bytes 98312 | tf_op jit(solution)/shard_map/ppermute | solution.py:196
  31.0 5.7 %collective-permute-start.17 = (bf16[16,1024]{1,0:T(8,128)(2,1)S(1)}, bf16[16,1024]{1,0:T(8,128)(2,1)S(1)}, u32[]{:S(2)}, u32[]{:S(2)}) collective-permute-start(bf16[16,1024]{1,0:T(8,128)(2,1)S(1)} %get-tuple-element.63), channel_id=1, source_target_pairs={{0,6},{1,7},{2,4},{3,5},{4,2},{5,3},{6,0},{7,1},{8,14},{9,15},{10,... | collective-permute-start | bytes 98312 | tf_op jit(solution)/shard_map/ppermute | solution.py:196
  32.3 5.4 %collective-permute-start.12 = (bf16[16,1024]{1,0:T(8,128)(2,1)S(1)}, bf16[16,1024]{1,0:T(8,128)(2,1)S(1)}, u32[]{:S(2)}, u32[]{:S(2)}) collective-permute-start(bf16[16,1024]{1,0:T(8,128)(2,1)S(1)} %get-tuple-element.60.refs_0_), channel_id=1, source_target_pairs={{0,1},{1,0},{2,3},{3,2},{4,5},{5,4},{6,7},{7,6},{8,9},{9,8},{10,11... | collective-permute-start | bytes 98312 | tf_op jit(solution)/shard_map/ppermute | solution.py:196
  32.3 5.4 %collective-permute-start.14 = (bf16[16,1024]{1,0:T(8,128)(2,1)S(1)}, bf16[16,1024]{1,0:T(8,128)(2,1)S(1)}, u32[]{:S(2)}, u32[]{:S(2)}) collective-permute-start(bf16[16,1024]{1,0:T(8,128)(2,1)S(1)} %collective-permute-done.13.refs_1_), channel_id=1, source_target_pairs={{0,1},{1,0},{2,3},{3,2},{4,5},{5,4},{6,7},{7,6},{8,9},{9,8},{10,11... | collective-permute-start | bytes 98312 | tf_op jit(solution)/shard_map/ppermute | solution.py:196
  38.7 6.0 %collective-permute-start.24 = (bf16[8,2048]{1,0:T(8,128)(2,1)S(1)}, bf16[8,2048]{1,0:T(8,128)(2,1)S(1)}, u32[]{:S(2)}, u32[]{:S(2)}) collective-permute-start(bf16[8,2048]{1,0:T(8,128)(2,1)S(1)} %get-tuple-element.69.refs_0_), channel_id=1, source_target_pairs={{0,6},{1,7},{2,4},{3,5},{4,2},{5,3},{6,0},{7,1},{8,14},{9,15},{10,... | collective-permute-start | bytes 98312 | tf_op jit(solution)/shard_map/ppermute | solution.py:196
  40.3 5.4 %collective-permute-start.22 = (bf16[8,2048]{1,0:T(8,128)(2,1)S(1)}, bf16[8,2048]{1,0:T(8,128)(2,1)S(1)}, u32[]{:S(2)}, u32[]{:S(2)}) collective-permute-start(bf16[8,2048]{1,0:T(8,128)(2,1)S(1)} %get-tuple-element.69.refs_0_), channel_id=1, source_target_pairs={{0,4},{1,5},{2,6},{3,7},{4,0},{5,1},{6,2},{7,3},{8,12},{9,13},{10,... | collective-permute-start | bytes 98312 | tf_op jit(solution)/shard_map/ppermute | solution.py:196
  40.4 5.4 %collective-permute-start.21 = (bf16[8,2048]{1,0:T(8,128)(2,1)S(1)}, bf16[8,2048]{1,0:T(8,128)(2,1)S(1)}, u32[]{:S(2)}, u32[]{:S(2)}) collective-permute-start(bf16[8,2048]{1,0:T(8,128)(2,1)S(1)} %get-tuple-element.69.refs_0_), channel_id=1, source_target_pairs={{0,3},{1,2},{2,1},{3,0},{4,7},{5,6},{6,5},{7,4},{8,11},{9,10},{10,... | collective-permute-start | bytes 98312 | tf_op jit(solution)/shard_map/ppermute | solution.py:196
  42.6 3.9 %collective-permute-start.20 = (bf16[8,2048]{1,0:T(8,128)(2,1)S(1)}, bf16[8,2048]{1,0:T(8,128)(2,1)S(1)}, u32[]{:S(2)}, u32[]{:S(2)}) collective-permute-start(bf16[8,2048]{1,0:T(8,128)(2,1)S(1)} %get-tuple-element.69.refs_0_), channel_id=1, source_target_pairs={{0,2},{1,3},{2,0},{3,1},{4,6},{5,7},{6,4},{7,5},{8,10},{9,11},{10,... | collective-permute-start | bytes 98312 | tf_op jit(solution)/shard_map/ppermute | solution.py:196
  43.2 3.4 %collective-permute-start.19 = (bf16[8,2048]{1,0:T(8,128)(2,1)S(1)}, bf16[8,2048]{1,0:T(8,128)(2,1)S(1)}, u32[]{:S(2)}, u32[]{:S(2)}) collective-permute-start(bf16[8,2048]{1,0:T(8,128)(2,1)S(1)} %get-tuple-element.69.refs_0_), channel_id=1, source_target_pairs={{0,1},{1,0},{2,3},{3,2},{4,5},{5,4},{6,7},{7,6},{8,9},{9,8},{10,11... | collective-permute-start | bytes 98312 | tf_op jit(solution)/shard_map/ppermute | solution.py:196
  47.2 5.8 %collective-permute-start.31 = (bf16[64,256]{1,0:T(8,128)(2,1)S(1)}, bf16[64,256]{1,0:T(8,128)(2,1)S(1)}, u32[]{:S(2)}, u32[]{:S(2)}) collective-permute-start(bf16[64,256]{1,0:T(8,128)(2,1)S(1)} %shard_map.215.refs_0_.base_ref), channel_id=1, source_target_pairs={{0,6},{1,7},{2,4},{3,5},{4,2},{5,3},{6,0},{7,1},{8,14},{9,15},{10,... | collective-permute-start | bytes 98312 | tf_op jit(solution)/shard_map/ppermute | solution.py:196
  49.0 5.0 %collective-permute-start.28 = (bf16[64,256]{1,0:T(8,128)(2,1)S(1)}, bf16[64,256]{1,0:T(8,128)(2,1)S(1)}, u32[]{:S(2)}, u32[]{:S(2)}) collective-permute-start(bf16[64,256]{1,0:T(8,128)(2,1)S(1)} %shard_map.215.refs_0_.base_ref), channel_id=1, source_target_pairs={{0,4},{1,5},{2,6},{3,7},{4,0},{5,1},{6,2},{7,3},{8,12},{9,13},{10,... | collective-permute-start | bytes 98312 | tf_op jit(solution)/shard_map/ppermute | solution.py:196
  49.4 4.7 %collective-permute-start.26 = (bf16[64,256]{1,0:T(8,128)(2,1)S(1)}, bf16[64,256]{1,0:T(8,128)(2,1)S(1)}, u32[]{:S(2)}, u32[]{:S(2)}) collective-permute-start(bf16[64,256]{1,0:T(8,128)(2,1)S(1)} %shard_map.215.refs_0_.base_ref), channel_id=1, source_target_pairs={{0,2},{1,3},{2,0},{3,1},{4,6},{5,7},{6,4},{7,5},{8,10},{9,11},{10,... | collective-permute-start | bytes 98312 | tf_op jit(solution)/shard_map/ppermute | solution.py:196
  57.7 5.8 %collective-permute-start.34 = (bf16[64,256]{1,0:T(8,128)(2,1)S(1)}, bf16[64,256]{1,0:T(8,128)(2,1)S(1)}, u32[]{:S(2)}, u32[]{:S(2)}) collective-permute-start(bf16[64,256]{1,0:T(8,128)(2,1)S(1)} %get-tuple-element.77), channel_id=1, source_target_pairs={{0,2},{1,3},{2,0},{3,1},{4,6},{5,7},{6,4},{7,5},{8,10},{9,11},{10,... | collective-permute-start | bytes 98312 | tf_op jit(solution)/shard_map/ppermute | solution.py:196
  59.1 5.7 %collective-permute-start.35 = (bf16[64,256]{1,0:T(8,128)(2,1)S(1)}, bf16[64,256]{1,0:T(8,128)(2,1)S(1)}, u32[]{:S(2)}, u32[]{:S(2)}) collective-permute-start(bf16[64,256]{1,0:T(8,128)(2,1)S(1)} %get-tuple-element.78), channel_id=1, source_target_pairs={{0,4},{1,5},{2,6},{3,7},{4,0},{5,1},{6,2},{7,3},{8,12},{9,13},{10,... | collective-permute-start | bytes 98312 | tf_op jit(solution)/shard_map/ppermute | solution.py:196
  60.3 5.7 %collective-permute-start.36 = (bf16[64,256]{1,0:T(8,128)(2,1)S(1)}, bf16[64,256]{1,0:T(8,128)(2,1)S(1)}, u32[]{:S(2)}, u32[]{:S(2)}) collective-permute-start(bf16[64,256]{1,0:T(8,128)(2,1)S(1)} %get-tuple-element.79), channel_id=1, source_target_pairs={{0,6},{1,7},{2,4},{3,5},{4,2},{5,3},{6,0},{7,1},{8,14},{9,15},{10,... | collective-permute-start | bytes 98312 | tf_op jit(solution)/shard_map/ppermute | solution.py:196
  (33 other events, 431.3 us)
